TPU v7x, 512 devices: a whole 4x4x16 slice. The times are simulated.
512 devices in a mesh: sp: 16 (over z), tp: 32 (over y, x, core).
Axes of the slice: x: 4, y: 4, z: 16, core: 2. Of those that a mesh axis runs over, the one named last changes fastest.
Arguments:
- target_rows: bfloat16 [3072, 2048], P(('sp', 'tp')), may hold values from -6 to 6
- source_rows: bfloat16 [16384, 2048], P(('sp', 'tp')), may hold values from -6 to 6
- target_gain: float32 [2048], replicated, may hold values from 0.55 to 9
- source_gain: float32 [2048], replicated, may hold values from 0.55 to 9
- query_weight: bfloat16 [2048, 2048], P(None, 'tp'), may hold values from -0.125 to 0.125
- key_weight: bfloat16 [2048, 512], P('tp'), may hold values from -0.125 to 0.125
- value_weight: bfloat16 [2048, 512], P('tp'), may hold values from -0.125 to 0.125
- out_weight: bfloat16 [2048, 2048], P('tp'), may hold values from -0.125 to 0.125
- out_cotangent: bfloat16 [3072, 2048], P(('sp', 'tp')), may hold values from -6 to 6
Outputs:
- target_grad: float32 [3072, 2048], P(('sp', 'tp'))
- source_grad: float32 [16384, 2048], P(('sp', 'tp'))
- out_weight_grad: float32 [2048, 2048], P('tp')
All inputs are finite; a program needn't handle non-finite values.
Results may differ from a plain program's by a relative error of at most 0.03.
Values may be sent and summed in bfloat16 or wider, within the bound.
A program may use at most 64 MiB of HBM per device.

v0:
```python
import jax
import jax.numpy as jnp
from jax import lax
from jax.sharding import PartitionSpec as P

HEAD_DIM = 64
KV_HEADS = 8


EPSILON = 1e-06
NEGATIVE = -1e30


def in_one_piece(arrays, axis, dim, along):
    ends, at = ([], 0)
    for a in arrays[:-1]:
        at += a.shape[along]
        ends.append(at)
    both = jnp.concatenate(arrays, axis=along)
    return tuple(jnp.split(lax.all_gather(both, axis, axis=dim, tiled=True), ends, axis=along))


def side_by_side(arrays, axis, split_dim, concat_dim, along):
    ends, at = ([], 0)
    for a in arrays[:-1]:
        at += a.shape[along]
        ends.append(at)
    both = jnp.concatenate(arrays, axis=along)
    return tuple(
        jnp.split(
            lax.all_to_all(both, axis, split_axis=split_dim, concat_axis=concat_dim, tiled=True),
            ends,
            axis=along,
        )
    )


def joined_along(blocks, dim):
    lengths = list(blocks.shape[1:])
    lengths[dim] *= blocks.shape[0]
    return jnp.moveaxis(blocks, 0, dim).reshape(lengths)


def copy_for_each(value, axis):
    peers = lax.axis_size(axis)
    return lax.all_to_all(
        jnp.broadcast_to(value[None], (peers, *value.shape)), axis, 0, 0, tiled=True
    )


def gathered_copies(value, axis, dim):
    return joined_along(copy_for_each(value, axis), dim)


def sent_together(arrays, axis, dim, along):
    both = jnp.concatenate(arrays, axis=along)
    filled, at, gathered = (gathered_copies(both, axis, dim), 0, [])
    for a in arrays:
        gathered.append(lax.slice_in_dim(filled, at, at + a.shape[along], axis=along))
        at += a.shape[along]
    return tuple(gathered)


def split_up(value, dim, peers):
    before, after = (value.shape[:dim], value.shape[dim + 1 :])
    return jnp.moveaxis(value.reshape(*before, peers, -1, *after), dim, 0)


def summed_on_arrival(value, axis, dim):
    blocks = split_up(value, dim, lax.axis_size(axis))
    arrived = lax.all_to_all(blocks, axis, split_axis=0, concat_axis=0, tiled=True)
    return arrived.sum(axis=0)


def gathered_total(value, axis):
    blocks = lax.all_gather(value, axis)
    return blocks.sum(axis=0)


def normalize(matrix, gain_vector):
    widened = matrix.astype(jnp.float32)
    factor = lax.rsqrt(jnp.mean(widened * widened, axis=-1, keepdims=True) + EPSILON)
    return (widened * factor * gain_vector).astype(jnp.bfloat16)


def norm_back(matrix, gain_vector, upstream):
    widened = matrix.astype(jnp.float32)
    factor = lax.rsqrt(jnp.mean(widened * widened, axis=-1, keepdims=True) + EPSILON)
    weighted = upstream * gain_vector
    inner_sum = jnp.mean(weighted * widened, axis=-1, keepdims=True)
    return factor * weighted - widened * factor**3 * inner_sum


def block_rows_for():
    return 512


def body(
    target_rows,
    source_rows,
    target_gain,
    source_gain,
    query_weight,
    key_weight,
    value_weight,
    out_weight,
    out_cotangent,
):
    tp_count = lax.axis_size("tp")
    local_heads = query_weight.shape[1] // HEAD_DIM
    slot_heads = max(1, KV_HEADS // tp_count)
    copies = max(1, tp_count // KV_HEADS)
    per_slot = local_heads // slot_heads
    score_scale = HEAD_DIM ** (-0.5)
    normed_t = normalize(target_rows, target_gain)
    normed_s = normalize(source_rows, source_gain)
    source_local = normed_s.shape[0]
    key_full, value_full = in_one_piece((key_weight, value_weight), "tp", 0, 1)
    key_own = jnp.dot(normed_s, key_full, preferred_element_type=jnp.float32).astype(jnp.bfloat16)
    value_own = jnp.dot(normed_s, value_full, preferred_element_type=jnp.float32).astype(
        jnp.bfloat16
    )

    def to_slots(matrix):
        split_heads = matrix.reshape(source_local, KV_HEADS, 1, HEAD_DIM)
        spread = jnp.broadcast_to(split_heads, (source_local, KV_HEADS, copies, HEAD_DIM))
        return spread.reshape(source_local, tp_count, slot_heads * HEAD_DIM)

    key_slots, value_slots = side_by_side((to_slots(key_own), to_slots(value_own)), "tp", 1, 0, 2)
    source_block = key_slots.shape[0]
    key_flat = key_slots.reshape(source_block, slot_heads * HEAD_DIM)
    value_flat = value_slots.reshape(source_block, slot_heads * HEAD_DIM)
    pieces = sent_together((normed_t, out_cotangent), "tp", 0, 1)
    queries = jnp.dot(pieces[0], query_weight, preferred_element_type=jnp.float32).astype(
        jnp.bfloat16
    )
    d_attended = jnp.dot(pieces[1], out_weight.T, preferred_element_type=jnp.float32).astype(
        jnp.bfloat16
    )
    queries, d_attended, cotangent_block = (queries, d_attended, pieces[1])
    target_block = queries.shape[0]
    query_view = queries.reshape(target_block, slot_heads, per_slot, HEAD_DIM)
    start_state = (
        jnp.full((slot_heads, per_slot, target_block), NEGATIVE, jnp.float32),
        jnp.zeros((slot_heads, per_slot, target_block), jnp.float32),
        jnp.zeros((slot_heads, per_slot, target_block, HEAD_DIM), jnp.float32),
    )
    running = start_state
    pieces = in_one_piece((key_flat, value_flat), "sp", 0, 1)
    length = pieces[0].shape[0]
    step_rows = 2048

    def one_block(carried, block_index):
        prior_max, prior_total, prior_sum = carried
        key_part = lax.dynamic_slice_in_dim(pieces[0], block_index * step_rows, step_rows, 0)
        value_part = lax.dynamic_slice_in_dim(pieces[1], block_index * step_rows, step_rows, 0)
        key_part = key_part.reshape(step_rows, slot_heads, HEAD_DIM)
        value_part = value_part.reshape(step_rows, slot_heads, HEAD_DIM)
        scores = (
            jnp.einsum("tgqd,sgd->gqts", query_view, key_part, preferred_element_type=jnp.float32)
            * score_scale
        )
        new_max = jnp.maximum(prior_max, jnp.max(scores, axis=-1))
        rescale = jnp.exp(prior_max - new_max)
        weights = jnp.exp(scores - new_max[..., None])
        new_total = prior_total * rescale + jnp.sum(weights, axis=-1)
        new_sum = prior_sum * rescale[..., None] + jnp.einsum(
            "gqts,sgd->gqtd",
            weights.astype(jnp.bfloat16),
            value_part,
            preferred_element_type=jnp.float32,
        )
        return ((new_max, new_total, new_sum), None)

    running, unused = lax.scan(one_block, running, jnp.arange(length // step_rows))
    row_max, total, summed = running
    attended = (
        (summed / total[..., None])
        .transpose(2, 0, 1, 3)
        .reshape(target_block, local_heads * HEAD_DIM)
        .astype(jnp.bfloat16)
    )
    log_total = (row_max + jnp.log(total)).transpose(2, 0, 1).reshape(target_block, local_heads)
    delta = jnp.sum(
        (d_attended.astype(jnp.float32) * attended.astype(jnp.float32)).reshape(
            target_block, local_heads, HEAD_DIM
        ),
        axis=-1,
    )
    all_queries, all_grads = in_one_piece((queries, d_attended), "sp", 0, 1)
    all_logs, all_deltas = in_one_piece((log_total, delta), "sp", 0, 1)
    whole_rows = all_queries.shape[0]
    step_rows = block_rows_for()
    block_shape = (whole_rows // step_rows, step_rows, slot_heads, per_slot)
    query_blocks = all_queries.reshape(block_shape + (HEAD_DIM,))
    grad_blocks = all_grads.reshape(block_shape + (HEAD_DIM,))
    log_blocks = all_logs.reshape(block_shape)
    delta_blocks = all_deltas.reshape(block_shape)

    def backward_block(sums_so_far, inputs):
        key_sum, value_sum = sums_so_far
        query_part, grad_part, log_part, delta_part = inputs
        scores = (
            jnp.einsum("tgqd,sgd->gqts", query_part, key_slots, preferred_element_type=jnp.float32)
            * score_scale
        )
        probs = jnp.exp(scores - log_part.transpose(1, 2, 0)[..., None])
        value_sum = value_sum + jnp.einsum(
            "gqts,tgqd->sgd",
            probs.astype(jnp.bfloat16),
            grad_part,
            preferred_element_type=jnp.float32,
        )
        d_probs = jnp.einsum(
            "tgqd,sgd->gqts", grad_part, value_slots, preferred_element_type=jnp.float32
        )
        d_scores = (probs * (d_probs - delta_part.transpose(1, 2, 0)[..., None])).astype(
            jnp.bfloat16
        )
        d_query = (
            jnp.einsum("gqts,sgd->tgqd", d_scores, key_slots, preferred_element_type=jnp.float32)
            * score_scale
        )
        key_sum = (
            key_sum
            + jnp.einsum("gqts,tgqd->sgd", d_scores, query_part, preferred_element_type=jnp.float32)
            * score_scale
        )
        return ((key_sum, value_sum), d_query)

    zero_sums = jnp.zeros((source_block, slot_heads, HEAD_DIM), jnp.float32)
    (key_sum, value_sum), d_query = lax.scan(
        backward_block,
        (zero_sums, zero_sums),
        (query_blocks, grad_blocks, log_blocks, delta_blocks),
    )
    query_terms = d_query.reshape(whole_rows, local_heads * HEAD_DIM)
    query_grad = summed_on_arrival(query_terms, "sp", 0).astype(jnp.bfloat16)
    key_back, value_back = side_by_side((key_sum, value_sum), "tp", 0, 1, 2)

    def from_slots(matrix):
        folded = jnp.sum(matrix.reshape(source_local, KV_HEADS, copies, HEAD_DIM), axis=2)
        return folded.reshape(source_local, KV_HEADS * HEAD_DIM).astype(jnp.bfloat16)

    key_grad = from_slots(key_back)
    value_grad = from_slots(value_back)
    d_normed_s = jnp.dot(key_grad, key_full.T, preferred_element_type=jnp.float32) + jnp.dot(
        value_grad, value_full.T, preferred_element_type=jnp.float32
    )
    source_grad = norm_back(source_rows, source_gain, d_normed_s)
    d_normed_t = summed_on_arrival(
        jnp.dot(query_grad, query_weight.T, preferred_element_type=jnp.float32), "tp", 0
    )
    target_grad = out_cotangent.astype(jnp.float32) + norm_back(
        target_rows, target_gain, d_normed_t
    )
    weight_part = jnp.dot(attended.T, cotangent_block, preferred_element_type=jnp.float32)
    out_weight_grad = gathered_total(weight_part, "sp")
    return (target_grad, source_grad, out_weight_grad)


def solution(mesh):
    return jax.shard_map(
        body,
        mesh=mesh,
        in_specs=(
            P(("sp", "tp"), None),
            P(("sp", "tp"), None),
            P(),
            P(),
            P(None, "tp"),
            P("tp", None),
            P("tp", None),
            P("tp", None),
            P(("sp", "tp"), None),
        ),
        out_specs=(P(("sp", "tp"), None), P(("sp", "tp"), None), P("tp", None)),
        check_vma=False,
    )
```

profile of v0, /device:TPU:1, one launch (start us, length us, event | category | flops | bytes accessed | tf_op | source)
XLA Modules:
  0.0 483.3 jit_solution(8040531760311093068)
XLA Ops:
  10.6 68.2 %all-gather.6.cloned.1.call-done = bf16[2048,1024]{1,0:T(8,128)(2,1)} async-done(((bf16[64,1024]{1,0:T(8,128)(2,1)}), bf16[2048,1024]{1,0:T(8,128)(2,1)}) %all-gather.6.cloned.1.call-update) | async-done | bytes 4194320 | tf_op jit(solution)/shard_map/all_gather | solution.py:20
  83.6 14.0 %all_to_all.51 = bf16[32,32,128]{2,0,1:T(8,128)(2,1)S(1)} all-to-all(bf16[32,32,128]{2,0,1:T(8,128)(2,1)S(1)} %pad_maximum_fusion.1), channel_id=1, replica_groups=mesh['sp'=16,'tp'=32] {'tp'}, dimensions={1} | all-to-all | bytes 524288 | tf_op jit(solution)/shard_map/all_to_all | solution.py:31
  101.2 3.8 all-to-all-start
  105.1 28.2 %all-to-all-done = bf16[32,6,4096]{2,1,0:T(8,128)(2,1)S(1)} async-done(((bf16[32,6,4096]{2,1,0:T(8,128)(2,1)}), bf16[32,6,4096]{2,1,0:T(8,128)(2,1)S(1)}, u32[]{:S(2)}, u32[]{:S(2)}) %all-to-all-start) | async-done | bytes 1572896 | tf_op jit(solution)/shard_map/all_to_all | solution.py:46
  136.8 29.1 %all-gather.8.cloned.1.call-done = bf16[16384,128]{0,1:T(8,128)(2,1)} async-done(((bf16[1024,128]{0,1:T(8,128)(2,1)}), bf16[16384,128]{0,1:T(8,128)(2,1)}) %all-gather.8.cloned.1.call-update) | async-done | bytes 4194320 | tf_op jit(solution)/shard_map/all_gather | solution.py:20
  166.0 4.6 fusion.82
  171.1 55.7 %while.30 = (s32[]{:T(128)}, f32[1,1,192]{2,1,0:T(1,128)S(1)}, f32[1,1,192]{2,1,0:T(1,128)}, f32[1,1,192,64]{2,3,1,0:T(8,128)}, s32[8]{0:T(128)}, /*index=5*/bf1...) while((s32[]{:T(128)}, f32[1,1,192]{2,1,0:T(1,128)S(1)}, ...), condition=%wide.region_5.6_spmd.clone, body=%wide.region_2.5_spmd.clone.sunk | while | flops 103060416 | bytes 5402819 | solution.py:175
  230.2 20.5 %all-gather.1 = f32[16,192,2]{1,2,0:T(2,128)S(1)} all-gather(f32[1,192,2]{1,2,0:T(2,128)S(1)} %maximum_bitcast_fusion), channel_id=1, replica_groups=mesh['sp'=16,'tp'=32] {'sp'}, dimensions={0}, use_global_device_ids=true | all-gather | bytes 26112 | tf_op jit(solution)/shard_map/all_gather | solution.py:20
  251.0 35.0 %all_gather.18 = bf16[3072,128]{1,0:T(8,128)(2,1)S(1)} all-gather(bf16[192,128]{1,0:T(8,128)(2,1)S(1)} %copy.71), channel_id=1, replica_groups=mesh['sp'=16,'tp'=32] {'sp'}, dimensions={0}, use_global_device_ids=true | all-gather | bytes 835584 | tf_op jit(solution)/shard_map/all_gather | solution.py:20
  287.6 70.7 %while.31 = (s32[]{:T(128)}, f32[1024,1,64]{0,2,1:T(8,128)}, f32[1024,1,64]{0,2,1:T(8,128)}, f32[6,512,1,1,64]{1,0,4,3,2:T(8,128)}, bf16[6,512,1,1,64]{1,4,3,2,0...) while((s32[]{:T(128)}, f32[1024,1,64]{0,2,1:T(8,128)}, ...), condition=%wide.region_8.9_spmd.clone, body=%wide.region_7.8_spmd.clone.sunk | while | flops 340099072 | bytes 15679312 | solution.py:232
  291.4 3.7 dynamic_update_slice.6
  302.9 3.7 dynamic_update_slice.6
  314.8 3.7 dynamic_update_slice.6
  326.6 3.7 dynamic_update_slice.6
  338.4 3.7 dynamic_update_slice.6
  350.3 3.7 dynamic_update_slice.6
  361.7 4.9 %all-to-all-start.2 = ((f32[16,192,64]{1,2,0:T(8,128)}), f32[16,192,64]{1,2,0:T(8,128)S(1)}, u32[]{:S(2)}, u32[]{:S(2)}) async-start(f32[16,192,64]{1,2,0:T(8,128)} %copy.88), calls=%async_computation.2 | async-start | bytes 2097152 | tf_op jit(solution)/shard_map/all_to_all | solution.py:71
  369.3 24.6 %all-to-all-done.2 = f32[16,192,64]{1,2,0:T(8,128)S(1)} async-done(((f32[16,192,64]{1,2,0:T(8,128)}), f32[16,192,64]{1,2,0:T(8,128)S(1)}, u32[]{:S(2)}, u32[]{:S(2)}) %all-to-all-start.2) | async-done | bytes 786464 | tf_op jit(solution)/shard_map/all_to_all | solution.py:71
  393.9 33.3 %all-to-all-start.4 = ((f32[1024,1,128]{2,1,0:T(1,128)}), f32[1024,1,128]{2,1,0:T(1,128)S(1)}, u32[]{:S(2)}, u32[]{:S(2)}) async-start(f32[1024,1,128]{2,1,0:T(1,128)} %pad_maximum_fusion), calls=%async_computation.4 | async-start | bytes 1048576 | tf_op jit(solution)/shard_map/all_to_all | solution.py:31
  429.2 9.4 %all-to-all-done.4 = f32[1024,1,128]{2,1,0:T(1,128)S(1)} async-done(((f32[1024,1,128]{2,1,0:T(1,128)}), f32[1024,1,128]{2,1,0:T(1,128)S(1)}, u32[]{:S(2)}, u32[]{:S(2)}) %all-to-all-start.4) | async-done | bytes 524320 | tf_op jit(solution)/shard_map/all_to_all | solution.py:31
  438.6 4.1 all-to-all-start.3
  445.6 2.4 fusion.68
  448.9 22.1 %all-to-all-done.3 = f32[32,6,2048]{2,1,0:T(8,128)S(1)} async-done(((f32[32,6,2048]{2,1,0:T(8,128)}), f32[32,6,2048]{2,1,0:T(8,128)S(1)}, u32[]{:S(2)}, u32[]{:S(2)}) %all-to-all-start.3) | async-done | bytes 1572896 | tf_op jit(solution)/shard_map/all_to_all | solution.py:71
  472.0 4.7 reduce_sum.121
  (295 shorter events, 131.9 us)
Async XLA Ops:
  7.2 127.6 %copy-start = (bf16[2048,64]{0,1:T(8,128)(2,1)S(1)}, bf16[2048,64]{0,1:T(8,128)(2,1)}, u32[]{:S(2)}) copy-start(bf16[2048,64]{0,1:T(8,128)(2,1)} %param.17) | copy-start | bytes 786436
  7.2 73.9 %copy-start.9 = (bf16[32,2048]{1,0:T(8,128)(2,1)S(1)}, bf16[32,2048]{1,0:T(8,128)(2,1)}, u32[]{:S(2)}) copy-start(bf16[32,2048]{1,0:T(8,128)(2,1)} %param.14) | copy-start | bytes 393220
  7.2 73.9 %copy-start.21 = (f32[2048]{0:T(1024)S(1)}, f32[2048]{0:T(1024)}, u32[]{:S(2)}) copy-start(f32[2048]{0:T(1024)} %param.16) | copy-start | bytes 24580
  7.2 71.6 %all-gather.6.cloned.1.call-start = ((), (), s32[]{:S(2)}) async-start(), calls=%async_computation.5 | async-start | bytes 4325376 | tf_op jit(solution)/shard_map/all_gather | solution.py:20
  8.9 157.1 %all-gather.8.cloned.1.call-start = ((), (), s32[]{:S(2)}) async-start(), calls=%async_computation.6 | async-start | bytes 4456448 | tf_op jit(solution)/shard_map/all_gather | solution.py:20
  10.5 72.7 %copy-start.27 = (f32[32]{0:T(128)}, f32[32]{0:T(128)S(1)}, u32[]{:S(2)}) copy-start(f32[32]{0:T(128)S(1)} %get-tuple-element.310) | copy-start | bytes 388
  83.4 15.4 %copy-start.11 = (bf16[6,2048]{1,0:T(8,128)(2,1)S(1)}, bf16[6,2048]{1,0:T(8,128)(2,1)}, u32[]{:S(2)}) copy-start(bf16[6,2048]{1,0:T(8,128)(2,1)} %param.13) | copy-start | bytes 73732
  83.4 16.1 %copy-start.15 = (f32[2048]{0:T(1024)S(1)}, f32[2048]{0:T(1024)}, u32[]{:S(2)}) copy-start(f32[2048]{0:T(1024)} %param.15) | copy-start | bytes 24580
  83.5 16.1 %copy-start.13 = (bf16[6,2048]{1,0:T(8,128)(2,1)S(1)}, bf16[6,2048]{1,0:T(8,128)(2,1)}, u32[]{:S(2)}) copy-start(bf16[6,2048]{1,0:T(8,128)(2,1)} %param.21) | copy-start | bytes 73732
  101.2 32.1 %all-to-all-start = ((bf16[32,6,4096]{2,1,0:T(8,128)(2,1)}), bf16[32,6,4096]{2,1,0:T(8,128)(2,1)S(1)}, u32[]{:S(2)}, u32[]{:S(2)}) async-start(bf16[32,6,4096]{2,1,0:T(8,128)(2,1)} %broadcast_in_dim.28), calls=%async_computation | async-start | bytes 4194304 | tf_op jit(solution)/shard_map/all_to_all | solution.py:46
  105.0 367.0 %all-gather.10.cloned.1.call-start = ((), (), s32[]{:S(2)}) async-start(), calls=%async_computation.7 | async-start | bytes 8912896 | tf_op jit(solution)/shard_map/all_gather | solution.py:76
  171.1 55.7 %copy-start.5 = (bf16[192,4096]{1,0:T(8,128)(2,1)S(1)}, bf16[192,4096]{1,0:T(8,128)(2,1)}, u32[]{:S(2)}) copy-start(bf16[192,4096]{1,0:T(8,128)(2,1)} %reshape.169) | copy-start | bytes 4718596
  226.8 3.3 copy-start.8
  360.0 6.6 %copy-start.1 = (f32[1024,1,64]{0,2,1:T(8,128)S(1)}, f32[1024,1,64]{0,2,1:T(8,128)}, u32[]{:S(2)}) copy-start(f32[1024,1,64]{0,2,1:T(8,128)} %get-tuple-element.105) | copy-start | bytes 786436
  360.1 6.9 %copy-start.2 = (f32[1024,1,64]{0,2,1:T(8,128)S(1)}, f32[1024,1,64]{0,2,1:T(8,128)}, u32[]{:S(2)}) copy-start(f32[1024,1,64]{0,2,1:T(8,128)} %get-tuple-element.106) | copy-start | bytes 786436
  361.7 32.1 %all-to-all-start.2 = ((f32[16,192,64]{1,2,0:T(8,128)}), f32[16,192,64]{1,2,0:T(8,128)S(1)}, u32[]{:S(2)}, u32[]{:S(2)}) async-start(f32[16,192,64]{1,2,0:T(8,128)} %copy.88), calls=%async_computation.2 | async-start | bytes 2097152 | tf_op jit(solution)/shard_map/all_to_all | solution.py:71
  393.9 44.8 %all-to-all-start.4 = ((f32[1024,1,128]{2,1,0:T(1,128)}), f32[1024,1,128]{2,1,0:T(1,128)S(1)}, u32[]{:S(2)}, u32[]{:S(2)}) async-start(f32[1024,1,128]{2,1,0:T(1,128)} %pad_maximum_fusion), calls=%async_computation.4 | async-start | bytes 1048576 | tf_op jit(solution)/shard_map/all_to_all | solution.py:31
  438.6 32.4 %all-to-all-start.3 = ((f32[32,6,2048]{2,1,0:T(8,128)}), f32[32,6,2048]{2,1,0:T(8,128)S(1)}, u32[]{:S(2)}, u32[]{:S(2)}) async-start(f32[32,6,2048]{2,1,0:T(8,128)} %reshape.179), calls=%async_computation.3 | async-start | bytes 4194304 | tf_op jit(solution)/shard_map/all_to_all | solution.py:71
  443.2 4.8 copy-start.26
  443.2 4.8 copy-start.28
  448.0 23.2 %copy-start.12 = (bf16[6,2048]{1,0:T(8,128)(2,1)S(1)}, bf16[6,2048]{1,0:T(8,128)(2,1)}, u32[]{:S(2)}) copy-start(bf16[6,2048]{1,0:T(8,128)(2,1)} %param.13) | copy-start | bytes 73732
  448.0 23.3 %copy-start.14 = (bf16[6,2048]{1,0:T(8,128)(2,1)S(1)}, bf16[6,2048]{1,0:T(8,128)(2,1)}, u32[]{:S(2)}) copy-start(bf16[6,2048]{1,0:T(8,128)(2,1)} %param.21) | copy-start | bytes 73732
  448.0 23.3 %copy-start.24 = (f32[6]{0:T(128)S(1)}, f32[6]{0:T(128)}, u32[]{:S(2)}) copy-start(f32[6]{0:T(128)} %copy-done.23) | copy-start | bytes 76
  448.0 23.3 %copy-start.25 = (f32[6]{0:T(128)S(1)}, f32[6]{0:T(128)}, u32[]{:S(2)}) copy-start(f32[6]{0:T(128)} %get-tuple-element.311) | copy-start | bytes 76
  (47 other events, 75.2 us)
Sparse Core Ops, SparseCore 0:
  11.7 67.0 all-gather.5
  98.9 67.0 all-gather.7
  230.3 118.6 all-gather.9
where the time goes:
time: 486 us; the launch traced here: 483 us
  waiting for transfers between devices  182 us (37%)
  matrix products  82.3 us (17%)
  blocking collectives  69.5 us (14%)
  local copies, waits for them, and re-layouts  57.4 us (12%)
  starting transfers between devices  46.3 us (10%)
  other arithmetic  26.3 us (5%)
  between operations  14.3 us (3%)
  loops' own time  5.57 us (1%)
    all_gather x2, waiting for transfers between devices, in_one_piece(): lax.all_gather(both, axis, axis=dim, tiled=True)  97.3 us
    all_gather x2, blocking collectives, in_one_piece(): lax.all_gather(both, axis, axis=dim, tiled=True)  55.6 us
    all_to_all x2, waiting for transfers between devices, summed_on_arrival(): lax.all_to_all(blocks, axis, split_axis=0, concat_axis=0, tiled=True)  46.7 us
    all_to_all x1, starting transfers between devices, side_by_side(): lax.all_to_all(both, axis, split_axis=split_dim, concat_axis=concat_dim,...  33.3 us
    all_to_all x1, waiting for transfers between devices, copy_for_each(): lax.all_to_all(jnp.broadcast_to(value[None], (peers, *value.shape)), axis...  28.2 us
    dynamic_update_slice x12, local copies, waits for them, and re-layouts, body(): lax.scan(backward_block, (zero_sums, zero_sums), (query_blocks, grad_bloc...  27.3 us
    dot_general x8, matrix products, one_block(): jnp.einsum('gqts,sgd->gqtd', weights.astype(jnp.bfloat16), value_part, pr...  16.3 us
    all_to_all x1, blocking collectives, side_by_side(): lax.all_to_all(both, axis, split_axis=split_dim, concat_axis=concat_dim,...  14 us
  transfers between devices with their start and end apart: 7, of which 6 were waited for; matrix products, arithmetic and copies ran while one was open for 19% of the time, Pallas kernels for 0%

commit v1 on v0

v1 whole, which is shorter than its diff:
```python
import functools

import jax
import jax.numpy as jnp
from jax import lax
from jax.experimental import pallas as pl
from jax.experimental.pallas import tpu as pltpu
from jax.sharding import Mesh
from jax.sharding import PartitionSpec as P

MESH = pl.DeviceIdType.MESH
HD = 64
EPSILON = 1e-06
F32, BF16 = jnp.float32, jnp.bfloat16
VMEM = pl.BlockSpec(memory_space=pltpu.VMEM)
SIZES = {"y": 4, "x": 4, "c": 2}
PIECES = 2


def dma(n):
    return pltpu.SemaphoreType.DMA((n,))


def params(cid):
    return pltpu.CompilerParams(
        collective_id=cid, has_side_effects=True, vmem_limit_bytes=62 * 1024 * 1024
    )


def group_size(axes):
    n = 1
    for a in axes:
        n *= SIZES[a]
    return n


def group_index(axes):
    i = 0
    for a in axes:
        i = i * SIZES[a] + lax.axis_index(a)
    return i


def coords_of(index, axes):
    out = {}
    for a in reversed(axes):
        out[a] = lax.rem(index, SIZES[a])
        index = index // SIZES[a]
    return out


def greet(axes):
    n, me = group_size(axes), group_index(axes)
    sem = pltpu.get_barrier_semaphore()

    def one(k, carry):
        pl.semaphore_signal(
            sem, inc=1, device_id=coords_of(lax.rem(me + k, n), axes), device_id_type=MESH
        )
        return carry

    lax.fori_loop(1, n, one, 0)
    return n - 1


def greeted(count):
    pl.semaphore_wait(pltpu.get_barrier_semaphore(), count)


class Exchange:
    def __init__(self, axes, src, dst, send, recv, pick=None):
        self.axes, self.src, self.dst, self.send, self.recv = axes, src, dst, send, recv
        self.n, self.me = group_size(axes), group_index(axes)
        self.pick = pick

    def block(self, index):
        if self.pick is None:
            return self.src
        return self.src.at[self.pick(coords_of(index, self.axes), index)]

    def copy(self, k, slot):
        to = lax.rem(self.me + k, self.n)
        return pltpu.make_async_remote_copy(
            src_ref=self.block(to),
            dst_ref=self.dst.at[slot],
            send_sem=self.send.at[k],
            recv_sem=self.recv.at[k],
            device_id=coords_of(to, self.axes),
            device_id_type=MESH,
        )

    def start(self):
        def one(k, carry):
            self.copy(k, self.me).start()
            return carry

        lax.fori_loop(1, self.n, one, 0)
        self.dst[self.me] = self.block(self.me)[...]

    def arrive(self):
        def one(k, carry):
            self.copy(k, lax.rem(self.me + self.n - k, self.n)).wait_recv()
            return carry

        lax.fori_loop(1, self.n, one, 0)

    def drain(self):
        def one(k, carry):
            self.copy(k, self.me).wait_send()
            return carry

        lax.fori_loop(1, self.n, one, 0)


def gather_kernel(rows, weights, pair, targets, kv, w_all, pair_all, t_all, *scratch):
    rows_all, part, part_all, rs, rr, ws, wr, ps, pr, ts, tr, ds, dr = scratch
    seen = greet(("y", "x", "c"))
    greeted(seen)
    by_rows = Exchange(("y", "c"), rows, rows_all, rs, rr, lambda at, i: at["c"])
    by_w = Exchange(("y", "x"), weights, w_all, ws, wr, lambda at, i: at["y"])
    by_t = Exchange(("y", "x"), targets, t_all, ts, tr)
    by_pair = Exchange(("c",), pair, pair_all, ps, pr)
    for e in (by_rows, by_w, by_t, by_pair):
        e.start()
    by_w.arrive()
    by_rows.arrive()
    left = rows_all[...].reshape(256, 1024)
    right = w_all[...].reshape(1024, 256)
    both = jnp.dot(left, right, preferred_element_type=F32)
    part[0] = both[:, :128]
    part[1] = both[:, 128:]
    by_part = Exchange(("c",), part, part_all, ds, dr, lambda at, i: i)
    by_part.start()
    by_part.arrive()
    kv[...] = (part_all[0] + part_all[1]).astype(BF16)
    by_t.arrive()
    by_pair.arrive()
    for e in (by_rows, by_w, by_t, by_pair, by_part):
        e.drain()


def gather(rows, weights, pair, targets):
    return pl.pallas_call(
        gather_kernel,
        out_shape=(
            jax.ShapeDtypeStruct((256, 128), BF16),
            jax.ShapeDtypeStruct((16, 64, 256), BF16),
            jax.ShapeDtypeStruct((2, 2, 64, 2048), BF16),
            jax.ShapeDtypeStruct((16, 16, 2048), BF16),
        ),
        in_specs=[VMEM] * 4,
        out_specs=(VMEM,) * 4,
        scratch_shapes=[
            pltpu.VMEM((8, 32, 1024), BF16),
            pltpu.VMEM((2, 256, 128), F32),
            pltpu.VMEM((2, 256, 128), F32),
            dma(8), dma(8), dma(16), dma(16), dma(2), dma(2), dma(16), dma(16), dma(2), dma(2),
        ],
        compiler_params=params(0),
    )(rows, weights, pair, targets)


class ToReaders:
    def __init__(self, src, dst, send, recv):
        self.src, self.dst, self.send, self.recv = src, dst, send, recv
        self.y, self.x, self.c = (lax.axis_index(a) for a in "yxc")
        self.mine = self.x // 2 == self.c

    def copy(self, k, slot):
        return pltpu.make_async_remote_copy(
            src_ref=self.src,
            dst_ref=self.dst.at[slot],
            send_sem=self.send.at[k],
            recv_sem=self.recv.at[slot],
            device_id={"x": lax.rem(self.x + k, 4), "c": self.x // 2},
            device_id_type=MESH,
        )

    def slot(self):
        return lax.rem(self.x, 2) * 2 + self.c

    def start(self):
        for k in range(1, 4):
            self.copy(k, self.slot()).start()

        @pl.when(jnp.logical_not(self.mine))
        def _():
            self.copy(0, self.slot()).start()

        @pl.when(self.mine)
        def _():
            self.dst[self.slot()] = self.src[...]

    def arrive(self):
        for s in range(4):
            own = jnp.logical_and(2 * self.c + s // 2 == self.x, self.c == s % 2)

            @pl.when(jnp.logical_not(own))
            def _():
                self.copy(1, s).wait_recv()

    def drain(self):
        for k in range(1, 4):
            self.copy(k, self.slot()).wait_send()

        @pl.when(jnp.logical_not(self.mine))
        def _():
            self.copy(0, self.slot()).wait_send()


class ToOwners:
    def __init__(self, src, dst, send, recv):
        self.src, self.dst, self.send, self.recv = src, dst, send, recv
        self.y, self.x, self.c = (lax.axis_index(a) for a in "yxc")

    def copy(self, s, slot):
        return pltpu.make_async_remote_copy(
            src_ref=self.src.at[s],
            dst_ref=self.dst.at[slot],
            send_sem=self.send.at[s],
            recv_sem=self.recv.at[slot],
            device_id={"x": 2 * self.c + s // 2, "c": jnp.int32(s % 2)},
            device_id_type=MESH,
        )

    def own(self, s):
        return jnp.logical_and(2 * self.c + s // 2 == self.x, self.c == s % 2)

    def start(self):
        for s in range(4):
            @pl.when(jnp.logical_not(self.own(s)))
            def _():
                self.copy(s, self.x).start()

            @pl.when(self.own(s))
            def _():
                self.dst[self.x] = self.src[s]

    def arrive(self):
        for j in range(4):
            own = jnp.logical_and(self.x == j, self.x // 2 == self.c)

            @pl.when(jnp.logical_not(own))
            def _():
                self.copy(0, j).wait_recv()

    def drain(self):
        for s in range(4):
            @pl.when(jnp.logical_not(self.own(s)))
            def _():
                self.copy(s, self.x).wait_send()


def readers_kernel(block, out, send, recv):
    greeted(greet(("x", "c")))
    e = ToReaders(block, out, send, recv)
    e.start()
    e.arrive()
    e.drain()


def to_readers(block):
    return pl.pallas_call(
        readers_kernel,
        out_shape=jax.ShapeDtypeStruct((4, *block.shape), block.dtype),
        in_specs=[VMEM],
        out_specs=VMEM,
        scratch_shapes=[dma(4), dma(4)],
        compiler_params=params(1),
    )(block)


def owners_kernel(a, b, a_out, b_out, a_send, a_recv, b_send, b_recv):
    greeted(greet(("x", "c")))
    both = (ToOwners(a, a_out, a_send, a_recv), ToOwners(b, b_out, b_send, b_recv))
    for e in both:
        e.start()
    for e in both:
        e.arrive()
    for e in both:
        e.drain()


def to_owners(a, b):
    return pl.pallas_call(
        owners_kernel,
        out_shape=(jax.ShapeDtypeStruct(a.shape, a.dtype), jax.ShapeDtypeStruct(b.shape, b.dtype)),
        in_specs=[VMEM, VMEM],
        out_specs=(VMEM, VMEM),
        scratch_shapes=[dma(4)] * 4,
        compiler_params=params(3),
    )(a, b)


def lanes_below(shape, bound):
    return lax.broadcasted_iota(jnp.int32, shape, 1) < bound


def contract(a, b, da, db):
    return lax.dot_general(a, b, (((da,), (db,)), ((), ())), preferred_element_type=F32)


def ring_greet(nz):
    z = lax.axis_index("z")
    sem = pltpu.get_barrier_semaphore()
    right, left = lax.rem(z + 1, nz), lax.rem(z + nz - 1, nz)
    for to in (left, right):
        pl.semaphore_signal(sem, inc=1, device_id={"z": to}, device_id_type=MESH)
    return 2


def forward_kernel(nz, qa, kv, kv_all, stats, out, m, l, o, said, heard, rs, rr, ls, lr, ss, sr):
    z = lax.axis_index("z")
    right, left = lax.rem(z + 1, nz), lax.rem(z + nz - 1, nz)
    greeted(ring_greet(nz) + greet(("x",)))
    steps_r = nz // 2
    steps_l = nz - 1 - steps_r
    piece = 256 // PIECES
    kv_all[z] = kv[...]

    def hop(step, p, sign):
        at = lax.rem(z + nz - sign * step, nz)
        ssem, rsem = (rs, rr) if sign > 0 else (ls, lr)
        src = kv_all.at[at, pl.ds(p * piece, piece)]
        return pltpu.make_async_remote_copy(
            src_ref=src,
            dst_ref=src,
            send_sem=ssem.at[step, p],
            recv_sem=rsem.at[step, p],
            device_id={"z": right if sign > 0 else left},
            device_id_type=MESH,
        )

    def landed(step, p, sign):
        at = lax.rem(z + nz - sign * (step + 1), nz)
        ssem, rsem = (rs, rr) if sign > 0 else (ls, lr)
        dst = kv_all.at[at, pl.ds(p * piece, piece)]
        return pltpu.make_async_remote_copy(
            src_ref=dst,
            dst_ref=dst,
            send_sem=ssem.at[step, p],
            recv_sem=rsem.at[step, p],
            device_id={"z": right if sign > 0 else left},
            device_id_type=MESH,
        )

    for p in range(PIECES):
        hop(0, p, 1).start()
        hop(0, p, -1).start()
    m[...] = jnp.full(m.shape, -1e30, F32)
    l[...] = jnp.zeros(l.shape, F32)
    o[...] = jnp.zeros(o.shape, F32)

    def attend(at):
        block = kv_all[at]
        keys = jnp.where(lanes_below(block.shape, HD), block, jnp.zeros_like(block))
        scores = contract(keys, qa[...], 1, 1)
        top = jnp.maximum(m[...], jnp.max(scores, axis=0, keepdims=True))
        weights = jnp.exp(scores - top)
        old = jnp.exp(m[...] - top)
        m[...] = top
        l[...] = l[...] * old + jnp.sum(weights, axis=0, keepdims=True)
        o[...] = o[...] * old + contract(block, weights.astype(BF16), 0, 0)[HD:]

    attend(z)

    def step(s, carry):
        for p in range(PIECES):
            landed(s - 1, p, 1).wait_recv()
            hop(s, p, 1).start()
            landed(s - 1, p, -1).wait_recv()

            @pl.when(s < steps_l)
            def _():
                hop(s, p, -1).start()

        attend(lax.rem(z + nz - s, nz))
        attend(lax.rem(z + s, nz))
        return carry

    lax.fori_loop(1, steps_r, step, 0)
    for p in range(PIECES):
        landed(steps_r - 1, p, 1).wait_recv()
    attend(lax.rem(z + nz - steps_r, nz))
    upright = jnp.transpose(qa[...].astype(F32))
    delta = jnp.sum(upright[HD:] * o[...], axis=0, keepdims=True)
    row = lax.broadcasted_iota(jnp.int32, (8, qa.shape[0]), 0)
    said[...] = jnp.where(row == 0, m[...], jnp.where(row == 1, l[...], delta))
    e = Exchange(("x",), said, heard, ss, sr)
    e.start()
    e.arrive()
    top = jnp.max(heard[:, 0:1], axis=0)
    total = jnp.zeros_like(top)
    both = jnp.zeros_like(top)
    for j in range(4):
        w = jnp.exp(heard[j, 0:1] - top)
        total = total + w * heard[j, 1:2]
        both = both + w * heard[j, 2:3]
    stats[...] = jnp.where(row == 0, top + jnp.log(total), both / total)
    scaled = o[...] * (jnp.exp(m[...] - top) / total)
    out[...] = jnp.transpose(jnp.concatenate([scaled, jnp.zeros_like(scaled)], axis=0)).astype(BF16)
    e.drain()

    def drain(s, carry):
        for p in range(PIECES):
            hop(s, p, 1).wait_send()

            @pl.when(s < steps_l)
            def _():
                hop(s, p, -1).wait_send()

        return carry

    lax.fori_loop(0, steps_r, drain, 0)


def forward(qa, kv, nz):
    t = qa.shape[0]
    sems = pltpu.SemaphoreType.DMA((nz // 2, PIECES))
    return pl.pallas_call(
        functools.partial(forward_kernel, nz),
        out_shape=(
            jax.ShapeDtypeStruct((nz, 256, 128), BF16),
            jax.ShapeDtypeStruct((8, t), F32),
            jax.ShapeDtypeStruct((t, 128), BF16),
        ),
        in_specs=[VMEM, VMEM],
        out_specs=(VMEM,) * 3,
        scratch_shapes=[
            pltpu.VMEM((1, t), F32),
            pltpu.VMEM((1, t), F32),
            pltpu.VMEM((HD, t), F32),
            pltpu.VMEM((8, t), F32),
            pltpu.VMEM((4, 8, t), F32),
            sems, sems, sems, sems, dma(4), dma(4),
        ],
        compiler_params=params(2),
    )(qa, kv)


def backward_kernel(nz, qa, kv_all, stats, kv_grad, q_grad, dq, own, tor, tol, inr, inl, rs, rr, ls, lr):
    z = lax.axis_index("z")
    right, left = lax.rem(z + 1, nz), lax.rem(z + nz - 1, nz)
    greeted(ring_greet(nz))
    steps_l = nz // 2
    steps_r = nz - 1 - steps_l
    piece = 256 // PIECES
    dq[...] = jnp.zeros(dq.shape, F32)

    def grads(at):
        block = kv_all[at]
        low = lanes_below(block.shape, HD)
        none = jnp.zeros_like(block)
        scores = contract(jnp.where(low, block, none), qa[...], 1, 1)
        probs = jnp.exp(scores - stats[0:1])
        d_probs = contract(jnp.where(low, none, block), qa[...], 1, 1)
        d_scores = (probs * (d_probs - stats[1:2])).astype(BF16)
        for_v = contract(probs.astype(BF16), qa[...], 1, 0)
        for_k = contract(d_scores, qa[...], 1, 0)
        dq[...] += contract(block, d_scores, 0, 0)[:HD]
        return jnp.where(lanes_below(for_k.shape, HD), for_k, for_v)

    def hop(s, p, sign):
        ssem, rsem = (rs, rr) if sign > 0 else (ls, lr)
        src, dst = (tor, inr) if sign > 0 else (tol, inl)
        return pltpu.make_async_remote_copy(
            src_ref=src.at[s, pl.ds(p * piece, piece)],
            dst_ref=dst.at[s, pl.ds(p * piece, piece)],
            send_sem=ssem.at[s, p],
            recv_sem=rsem.at[s, p],
            device_id={"z": right if sign > 0 else left},
            device_id_type=MESH,
        )

    def send_first(sign, value):
        ref = tor if sign > 0 else tol
        ref[0] = value.astype(BF16)
        for p in range(PIECES):
            hop(0, p, sign).start()

    def send_on(s, sign):
        ref, arrived = (tor, inr) if sign > 0 else (tol, inl)
        for p in range(PIECES):
            hop(s - 1, p, sign).wait_recv()
            at = pl.ds(p * piece, piece)
            ref[s, at] = (arrived[s - 1, at].astype(F32) + own[at]).astype(BF16)
            hop(s, p, sign).start()

    send_first(-1, grads(lax.rem(z + nz - steps_l, nz)))
    send_first(1, grads(lax.rem(z + steps_r, nz)))

    def step(s, carry):
        own[...] = grads(lax.rem(z + nz - steps_l + s, nz))
        send_on(s, -1)

        @pl.when(s < steps_r)
        def _():
            own[...] = grads(lax.rem(z + steps_r - s, nz))
            send_on(s, 1)

        return carry

    lax.fori_loop(1, steps_l, step, 0)
    own[...] = grads(z)
    q_grad[...] = jnp.transpose(
        jnp.concatenate([dq[...], jnp.zeros_like(dq[...])], axis=0)
    ).astype(BF16)
    for p in range(PIECES):
        at = pl.ds(p * piece, piece)
        hop(steps_l - 1, p, -1).wait_recv()
        hop(steps_r - 1, p, 1).wait_recv()
        kv_grad[at] = (
            inl[steps_l - 1, at].astype(F32) + inr[steps_r - 1, at].astype(F32) + own[at]
        ).astype(BF16)

    def drain(s, carry):
        for p in range(PIECES):
            hop(s, p, -1).wait_send()

            @pl.when(s < steps_r)
            def _():
                hop(s, p, 1).wait_send()

        return carry

    lax.fori_loop(0, steps_l, drain, 0)


def backward(qa, kv_all, stats, nz):
    t = qa.shape[0]
    half = nz // 2
    sems = pltpu.SemaphoreType.DMA((half, PIECES))
    return pl.pallas_call(
        functools.partial(backward_kernel, nz),
        out_shape=(
            jax.ShapeDtypeStruct((256, 128), BF16),
            jax.ShapeDtypeStruct((t, 128), BF16),
        ),
        in_specs=[VMEM] * 3,
        out_specs=(VMEM,) * 2,
        scratch_shapes=[
            pltpu.VMEM((HD, t), F32),
            pltpu.VMEM((256, 128), F32),
            pltpu.VMEM((half, 256, 128), BF16),
            pltpu.VMEM((half, 256, 128), BF16),
            pltpu.VMEM((half, 256, 128), BF16),
            pltpu.VMEM((half, 256, 128), BF16),
            sems, sems, sems, sems,
        ],
        compiler_params=params(4),
    )(qa, kv_all, stats)


def last_kernel(kv_grad, w_all, d_target, s_out, t_out, *scratch):
    grads, parts, ps, pr, ss, sr, ts, tr = scratch
    greeted(greet(("y", "x", "c")))
    by_pair = Exchange(("c",), kv_grad, grads, ps, pr)
    by_pair.start()
    by_t = Exchange(("y", "x"), d_target, t_out, ts, tr, lambda at, i: i)
    by_t.start()
    by_pair.arrive()
    right = w_all[...].reshape(1024, 256)
    d_rows = contract(grads[0], right[:, :128], 1, 1) + contract(grads[1], right[:, 128:], 1, 1)
    parts[...] = d_rows.astype(BF16).reshape(8, 32, 1024)
    by_s = Exchange(("y", "c"), parts, s_out, ss, sr, lambda at, i: i)
    by_s.start()
    by_t.arrive()
    by_s.arrive()
    for e in (by_pair, by_t, by_s):
        e.drain()


def last(kv_grad, w_all, d_target):
    return pl.pallas_call(
        last_kernel,
        out_shape=(
            jax.ShapeDtypeStruct((8, 32, 1024), BF16),
            jax.ShapeDtypeStruct(d_target.shape, BF16),
        ),
        in_specs=[VMEM] * 3,
        out_specs=(VMEM,) * 2,
        scratch_shapes=[
            pltpu.VMEM((2, 256, 128), BF16),
            pltpu.VMEM((8, 32, 1024), BF16),
            dma(2), dma(2), dma(8), dma(8), dma(16), dma(16),
        ],
        compiler_params=params(5),
    )(kv_grad, w_all, d_target)


def total_kernel(nz, part, out, halves, terms, sums, all_sums, mine_sum, cs, cr, ss, sr, gs, gr):
    greeted(greet(("c",)) + greet(("z",)))
    swap = Exchange(("c",), part, halves, cs, cr, lambda at, i: i)
    swap.start()
    swap.arrive()
    terms[...] = (halves[0].astype(F32) + halves[1].astype(F32)).astype(BF16)
    by_z = Exchange(("z",), terms, sums, ss, sr, lambda at, i: i)
    by_z.start()
    by_z.arrive()
    mine = jnp.zeros(sums.shape[1:], F32)
    for i in range(nz):
        mine = mine + sums[i].astype(F32)
    mine_sum[...] = mine.astype(BF16)
    back = Exchange(("z",), mine_sum, all_sums, gs, gr)
    back.start()
    back.arrive()
    out[...] = all_sums[...].astype(F32)
    for e in (swap, by_z, back):
        e.drain()


def total(part, nz):
    shape = part.shape[1:]
    return pl.pallas_call(
        functools.partial(total_kernel, nz),
        out_shape=jax.ShapeDtypeStruct(shape, F32),
        in_specs=[VMEM],
        out_specs=VMEM,
        scratch_shapes=[
            pltpu.VMEM((2, *shape), BF16),
            pltpu.VMEM(shape, BF16),
            pltpu.VMEM(shape, BF16),
            pltpu.VMEM(shape, BF16),
            pltpu.VMEM(shape[1:], BF16),
            dma(2), dma(2), dma(nz), dma(nz), dma(nz), dma(nz),
        ],
        compiler_params=params(6),
    )(part)


def normalize(matrix, gain):
    wide = matrix.astype(F32)
    factor = lax.rsqrt(jnp.mean(wide * wide, axis=-1, keepdims=True) + EPSILON)
    return (wide * factor * gain).astype(BF16)


def norm_back(matrix, gain, upstream):
    wide = matrix.astype(F32)
    factor = lax.rsqrt(jnp.mean(wide * wide, axis=-1, keepdims=True) + EPSILON)
    weighted = upstream * gain
    inner = jnp.mean(weighted * wide, axis=-1, keepdims=True)
    return factor * weighted - wide * factor**3 * inner


def pad_rows(a, rows):
    return jnp.pad(a, ((0, rows - a.shape[0]), (0, 0)))


def body(nz, target_rows, source_rows, t_gain, s_gain, wq, wk, wv, wo, cot):
    normed_s = normalize(source_rows, s_gain)
    normed_t = normalize(target_rows, t_gain)
    rows = normed_s.reshape(32, 16, 2, 64).transpose(2, 0, 1, 3).reshape(2, 32, 1024)
    weights = jnp.stack([wk.reshape(64, 4, 2, 64), wv.reshape(64, 4, 2, 64)], axis=3)
    weights = weights.transpose(1, 0, 2, 3, 4).reshape(4, 64, 256)
    pair = jnp.stack([wq.T, wo])
    targets = jnp.concatenate([pad_rows(normed_t, 8), pad_rows(cot, 8)])
    kv, w_all, pair_all, t_all = gather(rows, weights, pair, targets)
    wq2 = pair_all[:, 0].reshape(128, 2048)
    wo2 = pair_all[:, 1].reshape(128, 2048)
    t_all = t_all.reshape(16, 2, 8, 2048)
    normed2 = t_all[:, 0].reshape(128, 2048)
    cot2 = t_all[:, 1].reshape(128, 2048)

    def six(a):
        return a.reshape(16, 8, 2, HD)[:, :6].reshape(96, 2, HD).transpose(1, 0, 2)

    q2 = six((contract(normed2, wq2, 1, 1)).astype(BF16) * jnp.asarray(HD**-0.5, BF16))
    da2 = six(contract(cot2, wo2, 1, 1).astype(BF16))
    qa = to_readers(jnp.concatenate([q2, da2], axis=-1).reshape(192, 128)).reshape(768, 128)
    kv_all, stats, out = forward(qa, kv, nz)
    kv_grad, q_grad = backward(qa, kv_all, stats, nz)
    outs, q_grads = to_owners(out.reshape(4, 192, 128), q_grad.reshape(4, 192, 128))

    def pair_of(a):
        s = jnp.sum(a.astype(F32), axis=0)[:, :HD].reshape(2, 96, HD)
        return s.transpose(1, 0, 2).reshape(96, 128)

    attended = pair_of(outs).astype(BF16)
    query_grad = (pair_of(q_grads) * HD**-0.5).astype(BF16)
    padded = jnp.pad(attended.reshape(16, 6, 128), ((0, 0), (0, 2), (0, 0))).reshape(128, 128)
    o_part = contract(padded, cot2, 0, 0)
    d_target = jnp.dot(query_grad, wq2, preferred_element_type=F32).astype(BF16)
    d_target = jnp.pad(d_target.reshape(16, 6, 2048), ((0, 0), (0, 2), (0, 0)))
    s_back, t_back = last(kv_grad, w_all, d_target)
    d_normed_s = jnp.sum(s_back.reshape(4, 2, 32, 1024).astype(F32), axis=0)
    d_normed_s = d_normed_s.reshape(2, 32, 16, 64).transpose(1, 2, 0, 3).reshape(32, 2048)
    source_grad = norm_back(source_rows, s_gain, d_normed_s)
    d_normed_t = jnp.sum(t_back.astype(F32), axis=0)[:6]
    target_grad = cot.astype(F32) + norm_back(target_rows, t_gain, d_normed_t)
    o_grad = total(o_part.astype(BF16).reshape(2, nz, 64 * 2048 // nz // 128, 128), nz)
    return target_grad, source_grad, o_grad.reshape(64, 2048)


def solution(mesh):
    nz = mesh.shape["sp"]
    SIZES["z"] = nz
    fine = Mesh(mesh.devices.reshape(nz, 4, 4, 2), ("z", "y", "x", "c"))
    every, plane = ("z", "y", "x", "c"), ("y", "x", "c")
    return jax.shard_map(
        functools.partial(body, nz),
        mesh=fine,
        in_specs=(
            P(every, None), P(every, None), P(), P(),
            P(None, plane), P(plane, None), P(plane, None), P(plane, None), P(every, None),
        ),
        out_specs=(P(every, None), P(every, None), P(plane, None)),
        check_vma=False,
    )
```

time: 486 us -> 217 us (0.45)
  Pallas kernels: 0 us -> 191 us
  waiting for transfers between devices: 182 us -> 0 us
  matrix products: 82.3 us -> 2.25 us
  blocking collectives: 69.5 us -> 0 us
  starting transfers between devices: 46.3 us -> 0 us
  local copies, waits for them, and re-layouts: 57.4 us -> 13.3 us
  other arithmetic: 26.3 us -> 8.55 us
  between operations: 14.3 us -> 1 us
  loops' own time: 5.57 us -> 0 us
    pallas_call x0 -> x7, Pallas kernels: none -> 191 us  [the longest x1 38.4 us: total(): pl.pallas_call(functools.partial(total_kernel, nz), out_shape=jax.ShapeDt...]
    all_gather x3 -> x0, waiting for transfers between devices: 97.3 us -> none  [the longest x2 97.3 us: in_one_piece(): lax.all_gather(both, axis, axis=dim, tiled=True)]
    all_to_all x4 -> x0, waiting for transfers between devices: 84.3 us -> none  [the longest x2 46.7 us: summed_on_arrival(): lax.all_to_all(blocks, axis, split_axis=0, concat_axis=0, tiled=True)]
    dot_general x54 -> x4, matrix products: 82.3 us -> 2.25 us  [the longest x3 1.95 us: contract(): lax.dot_general(a, b, (((da,), (db,)), ((), ())), preferred_element_type=...]
    all_gather x2 -> x0, blocking collectives: 55.6 us -> none  [in_one_piece(): lax.all_gather(both, axis, axis=dim, tiled=True)]
    all_to_all x4 -> x0, starting transfers between devices: 46.1 us -> none  [the longest x1 33.3 us: side_by_side(): lax.all_to_all(both, axis, split_axis=split_dim, concat_axis=concat_dim,...]
    dynamic_update_slice x12 -> x0, local copies, waits for them, and re-layouts: 27.3 us -> none  [body(): lax.scan(backward_block, (zero_sums, zero_sums), (query_blocks, grad_bloc...]
    all_to_all x1 -> x0, blocking collectives: 14 us -> none  [side_by_side(): lax.all_to_all(both, axis, split_axis=split_dim, concat_axis=concat_dim,...]
  transfers between devices with their start and end apart: 7 -> 0, of which waited for: 6 -> 0; matrix products, arithmetic and copies ran while one was open for 19% -> 0% of each run, Pallas kernels for 0% -> 0%
where the time goes in v1:
time: 217 us; the launch traced here: 216 us
  Pallas kernels  191 us (88%)
  local copies, waits for them, and re-layouts  13.3 us (6%)
  other arithmetic  8.55 us (4%)
  matrix products  2.25 us (1%)
    pallas_call x1, Pallas kernels, total(): pl.pallas_call(functools.partial(total_kernel, nz), out_shape=jax.ShapeDt...  38.4 us
    pallas_call x1, Pallas kernels, gather(): pl.pallas_call(gather_kernel, out_shape=(jax.ShapeDtypeStruct((256, 128),...  37.4 us
    pallas_call x1, Pallas kernels, forward(): pl.pallas_call(functools.partial(forward_kernel, nz), out_shape=(jax.Shap...  35.6 us
    pallas_call x1, Pallas kernels, backward(): pl.pallas_call(functools.partial(backward_kernel, nz), out_shape=(jax.Sha...  24.9 us
    pallas_call x1, Pallas kernels, to_owners(): pl.pallas_call(owners_kernel, out_shape=(jax.ShapeDtypeStruct(a.shape, a....  22.8 us
    pallas_call x1, Pallas kernels, last(): pl.pallas_call(last_kernel, out_shape=(jax.ShapeDtypeStruct((8, 32, 1024)...  22.3 us
    pallas_call x1, Pallas kernels, to_readers(): pl.pallas_call(readers_kernel, out_shape=jax.ShapeDtypeStruct((4, *block....  9.93 us

profile of v1, /device:TPU:1, one launch (start us, length us, event | category | flops | bytes accessed | tf_op | source)
XLA Modules:
  0.0 216.4 jit_solution(3351843078350889314)
XLA Ops:
  0.6 0.9 fusion.9
  1.5 1.1 fusion.1
  2.8 0.6 fusion.16.targets
  3.9 0.9 reshape.114.rows
  6.2 0.7 maximum_bitcast_fusion
  6.9 0.9 reshape.115.weights
  7.9 0.8 pad_maximum_fusion.pair
  8.7 37.4 %shard_map.112 = (bf16[256,128]{1,0:T(8,128)(2,1)}, bf16[16,64,256]{2,1,0:T(8,128)(2,1)}, bf16[2,2,64,2048]{3,2,1,0:T(8,128)(2,1)}, bf16[16,16,2048]{2,1,0:T(8,128)(2,1)}) custom-call(bf16[2,32,1024]{2,1,0:T(8,128)(2,1)} %reshape.114.rows, bf16[4,64,256]{2,1,0:T(8,128)(2,1)} %reshape.115.weights, bf16[2,64,2048]{2,1,0:T(8,128)(2,1)} %pad_maximum_fusion.pair, ...), custom_call_target="tpu_custom_call" | custom-call | tf_op jit(solution)/shard_map/pallas_call | solution.py:143
  46.1 1.4 fusion.20
  49.1 0.7 slice-done
  50.6 9.9 %shard_map.113 = bf16[4,192,128]{2,1,0:T(8,128)(2,1)} custom-call(bf16[192,128]{1,0:T(8,128)(2,1)} %bitcast.71), custom_call_target="tpu_custom_call" | custom-call | tf_op jit(solution)/shard_map/pallas_call | solution.py:263
  60.5 35.6 %shard_map.114 = (bf16[16,256,128]{2,1,0:T(8,128)(2,1)}, f32[8,768]{1,0:T(8,128)}, bf16[768,128]{1,0:T(8,128)(2,1)}) custom-call(bf16[768,128]{1,0:T(8,128)(2,1)} %bitcast.55, bf16[256,128]{1,0:T(8,128)(2,1)} %get-tuple-element.18.kv), custom_call_target="tpu_custom_call" | custom-call | tf_op jit(solution)/shard_map/pallas_call | solution.py:420
  96.1 24.9 %shard_map.115 = (bf16[256,128]{1,0:T(8,128)(2,1)}, bf16[768,128]{1,0:T(8,128)(2,1)}) custom-call(bf16[768,128]{1,0:T(8,128)(2,1)} %bitcast.56, bf16[16,256,128]{2,1,0:T(8,128)(2,1)} %get-tuple-element.19.kv_all, f32[8,768]{1,0:T(8,128)} %get-tuple-element.20.stats), custom_call_target="tpu_custom_call" | custom-call | tf_op jit(solution)/shard_map/pallas_call | solution.py:533
  121.1 22.8 %shard_map.116 = (bf16[4,192,128]{2,1,0:T(8,128)(2,1)}, bf16[4,192,128]{2,1,0:T(8,128)(2,1)}) custom-call(bf16[4,192,128]{2,1,0:T(8,128)(2,1)} %bitcast.67, bf16[4,192,128]{2,1,0:T(8,128)(2,1)} %bitcast.68), custom_call_target="tpu_custom_call" | custom-call | tf_op jit(solution)/shard_map/pallas_call | solution.py:285
  143.9 1.0 convert_reduce_fusion.2
  146.2 1.4 convolution_convert_fusion
  147.6 1.0 reshape.129.part
  148.6 38.4 %shard_map.118 = f32[16,64,128]{2,1,0:T(8,128)} custom-call(bf16[2,16,64,128]{3,2,1,0:T(8,128)(2,1)} %reshape.129.part), custom_call_target="tpu_custom_call" | custom-call | tf_op jit(solution)/shard_map/pallas_call | solution.py:614
  187.0 1.9 reshape.130
  189.1 0.9 pad.17.d_target
  190.0 22.3 %shard_map.117 = (bf16[8,32,1024]{2,1,0:T(8,128)(2,1)}, bf16[16,8,2048]{2,1,0:T(8,128)(2,1)}) custom-call(bf16[256,128]{1,0:T(8,128)(2,1)} %get-tuple-element.21.kv_grad, bf16[16,64,256]{2,1,0:T(8,128)(2,1)} %get-tuple-element.22.w_all, bf16[16,8,2048]{2,1,0:T(8,128)(2,1)} %pad.17.d_target), custom_call_target="tpu_custom_call" | custom-call | tf_op jit(solution)/shard_map/pallas_call | solution.py:574
  212.2 1.2 convert_reduce_fusion.1
  213.7 0.7 fusion.14
  215.6 0.8 fusion.5
  (61 shorter events, 7.2 us)
Async XLA Ops:
  1.5 1.1 copy-start.1
  1.5 1.1 copy-start.10
  1.5 1.2 copy-start.8
  2.6 0.9 copy-start
  2.7 0.8 copy-start.9
  3.9 0.9 copy-start.11
  4.9 0.8 copy-start.12
  6.2 1.6 copy-start.5
  6.9 1.0 copy-start.4
  46.1 1.5 copy-start.3
  48.0 0.6 copy-start.6
  49.0 0.8 slice-start
  145.1 0.9 copy-start.7
  212.2 1.2 copy-start.2

commit v2 on v1

v2 whole, which is shorter than its diff:
```python
import functools

import jax
import jax.numpy as jnp
from jax import lax
from jax.experimental import pallas as pl
from jax.experimental.pallas import tpu as pltpu
from jax.sharding import Mesh
from jax.sharding import PartitionSpec as P

MESH = pl.DeviceIdType.MESH
HD = 64
EPSILON = 1e-06
F32, BF16 = jnp.float32, jnp.bfloat16
VMEM = pl.BlockSpec(memory_space=pltpu.VMEM)
SIZES = {"y": 4, "x": 4, "c": 2}
PIECES = 2


def dma(n):
    return pltpu.SemaphoreType.DMA((n,))


def params(cid):
    return pltpu.CompilerParams(
        collective_id=cid, has_side_effects=True, vmem_limit_bytes=62 * 1024 * 1024
    )


def group_size(axes):
    n = 1
    for a in axes:
        n *= SIZES[a]
    return n


def group_index(axes):
    i = 0
    for a in axes:
        i = i * SIZES[a] + lax.axis_index(a)
    return i


def coords_of(index, axes):
    out = {}
    for a in reversed(axes):
        out[a] = lax.rem(index, SIZES[a])
        index = index // SIZES[a]
    return out


def greet(axes):
    n, me = group_size(axes), group_index(axes)
    sem = pltpu.get_barrier_semaphore()

    def one(k, carry):
        pl.semaphore_signal(
            sem, inc=1, device_id=coords_of(lax.rem(me + k, n), axes), device_id_type=MESH
        )
        return carry

    lax.fori_loop(1, n, one, 0)
    return n - 1


def greeted(count):
    pl.semaphore_wait(pltpu.get_barrier_semaphore(), count)


class Exchange:
    def __init__(self, axes, src, dst, send, recv, pick=None):
        self.axes, self.src, self.dst, self.send, self.recv = axes, src, dst, send, recv
        self.n, self.me = group_size(axes), group_index(axes)
        self.pick = pick

    def block(self, index):
        if self.pick is None:
            return self.src
        return self.src.at[self.pick(coords_of(index, self.axes), index)]

    def copy(self, k, slot):
        to = lax.rem(self.me + k, self.n)
        return pltpu.make_async_remote_copy(
            src_ref=self.block(to),
            dst_ref=self.dst.at[slot],
            send_sem=self.send.at[k],
            recv_sem=self.recv.at[k],
            device_id=coords_of(to, self.axes),
            device_id_type=MESH,
        )

    def start(self):
        def one(k, carry):
            self.copy(k, self.me).start()
            return carry

        lax.fori_loop(1, self.n, one, 0)
        self.dst[self.me] = self.block(self.me)[...]

    def arrive(self):
        def one(k, carry):
            self.copy(k, lax.rem(self.me + self.n - k, self.n)).wait_recv()
            return carry

        lax.fori_loop(1, self.n, one, 0)

    def drain(self):
        def one(k, carry):
            self.copy(k, self.me).wait_send()
            return carry

        lax.fori_loop(1, self.n, one, 0)


class ToReaders:
    def __init__(self, src, dst, send, recv):
        self.src, self.dst, self.send, self.recv = src, dst, send, recv
        self.y, self.x, self.c = (lax.axis_index(a) for a in "yxc")
        self.mine = self.x // 2 == self.c

    def copy(self, k, slot):
        return pltpu.make_async_remote_copy(
            src_ref=self.src,
            dst_ref=self.dst.at[slot],
            send_sem=self.send.at[k],
            recv_sem=self.recv.at[slot],
            device_id={"x": lax.rem(self.x + k, 4), "c": self.x // 2},
            device_id_type=MESH,
        )

    def slot(self):
        return lax.rem(self.x, 2) * 2 + self.c

    def start(self):
        for k in range(1, 4):
            self.copy(k, self.slot()).start()

        @pl.when(jnp.logical_not(self.mine))
        def _():
            self.copy(0, self.slot()).start()

        @pl.when(self.mine)
        def _():
            self.dst[self.slot()] = self.src[...]

    def arrive(self):
        for s in range(4):
            own = jnp.logical_and(2 * self.c + s // 2 == self.x, self.c == s % 2)

            @pl.when(jnp.logical_not(own))
            def _():
                self.copy(1, s).wait_recv()

    def drain(self):
        for k in range(1, 4):
            self.copy(k, self.slot()).wait_send()

        @pl.when(jnp.logical_not(self.mine))
        def _():
            self.copy(0, self.slot()).wait_send()


class ToOwners:
    def __init__(self, src, dst, send, recv):
        self.src, self.dst, self.send, self.recv = src, dst, send, recv
        self.y, self.x, self.c = (lax.axis_index(a) for a in "yxc")

    def copy(self, s, slot):
        return pltpu.make_async_remote_copy(
            src_ref=self.src.at[s],
            dst_ref=self.dst.at[slot],
            send_sem=self.send.at[s],
            recv_sem=self.recv.at[slot],
            device_id={"x": 2 * self.c + s // 2, "c": jnp.int32(s % 2)},
            device_id_type=MESH,
        )

    def own(self, s):
        return jnp.logical_and(2 * self.c + s // 2 == self.x, self.c == s % 2)

    def start(self):
        for s in range(4):
            @pl.when(jnp.logical_not(self.own(s)))
            def _():
                self.copy(s, self.x).start()

            @pl.when(self.own(s))
            def _():
                self.dst[self.x] = self.src[s]

    def arrive(self):
        for j in range(4):
            own = jnp.logical_and(self.x == j, self.x // 2 == self.c)

            @pl.when(jnp.logical_not(own))
            def _():
                self.copy(0, j).wait_recv()

    def drain(self):
        for s in range(4):
            @pl.when(jnp.logical_not(self.own(s)))
            def _():
                self.copy(s, self.x).wait_send()


def lanes_below(shape, bound):
    return lax.broadcasted_iota(jnp.int32, shape, 1) < bound


def contract(a, b, da, db):
    return lax.dot_general(a, b, (((da,), (db,)), ((), ())), preferred_element_type=F32)


def ring_greet(nz):
    z = lax.axis_index("z")
    sem = pltpu.get_barrier_semaphore()
    right, left = lax.rem(z + 1, nz), lax.rem(z + nz - 1, nz)
    for to in (left, right):
        pl.semaphore_signal(sem, inc=1, device_id={"z": to}, device_id_type=MESH)
    return 2


class RingGather:
    def __init__(self, axis, piece, count, send, recv):
        self.axis, self.piece, self.count, self.send, self.recv = axis, piece, count, send, recv
        self.me = lax.axis_index(axis)

    def at(self, offset):
        return lax.rem(self.me + offset + 4, 4)

    def copy(self, slot, p, sign, kind):
        ref = self.piece(slot, p)
        return pltpu.make_async_remote_copy(
            src_ref=ref,
            dst_ref=ref,
            send_sem=self.send.at[kind, p],
            recv_sem=self.recv.at[kind, p],
            device_id={self.axis: self.at(sign)},
            device_id_type=MESH,
        )

    def start(self, p):
        self.copy(self.me, p, 1, 0).start()
        self.copy(self.me, p, -1, 1).start()

    def relay(self, p):
        self.copy(self.at(-1), p, 1, 0).wait_recv()
        self.copy(self.at(1), p, -1, 1).wait_recv()
        if p < self.count // 2:
            self.copy(self.at(-1), p, 1, 2).start()
        else:
            self.copy(self.at(1), p, -1, 2).start()

    def arrive(self, p):
        self.copy(self.at(2), p, 1, 2).wait_recv()

    def drain(self):
        for p in range(self.count):
            for kind in range(3):
                self.copy(self.me, p, 1, kind).wait_send()


class RowGather:
    def __init__(self, halves, out, send, recv):
        self.halves, self.out, self.send, self.recv = halves, out, send, recv
        self.y, self.c = lax.axis_index("y"), lax.axis_index("c")

    def at(self, offset):
        return lax.rem(self.y + offset + 4, 4)

    def first(self, sign, core, slot_y, slot_c):
        kind = 0 if sign > 0 else 1
        return pltpu.make_async_remote_copy(
            src_ref=self.halves.at[core],
            dst_ref=self.out.at[slot_y, slot_c],
            send_sem=self.send.at[kind, core],
            recv_sem=self.recv.at[kind, slot_c],
            device_id={"y": self.at(sign), "c": jnp.int32(core)},
            device_id_type=MESH,
        )

    def partner(self, slot_c):
        return pltpu.make_async_remote_copy(
            src_ref=self.halves.at[1 - self.c],
            dst_ref=self.out.at[self.y, slot_c],
            send_sem=self.send.at[4, 0],
            recv_sem=self.recv.at[4, 0],
            device_id={"c": 1 - self.c},
            device_id_type=MESH,
        )

    def second(self, sign, slot_y, slot_c):
        kind = 2 if sign > 0 else 3
        ref = self.out.at[slot_y, slot_c, pl.ds(0 if sign > 0 else 16, 16)]
        return pltpu.make_async_remote_copy(
            src_ref=ref,
            dst_ref=ref,
            send_sem=self.send.at[kind, slot_c],
            recv_sem=self.recv.at[kind, slot_c],
            device_id={"y": self.at(sign)},
            device_id_type=MESH,
        )

    def start(self):
        for core in range(2):
            self.first(1, core, self.y, self.c).start()
            self.first(-1, core, self.y, self.c).start()
        self.partner(self.c).start()
        self.out[self.y, self.c] = self.halves[self.c]

    def relay(self):
        for core in range(2):
            self.first(1, 0, self.at(-1), core).wait_recv()
            self.second(1, self.at(-1), core).start()
            self.first(-1, 0, self.at(1), core).wait_recv()
            self.second(-1, self.at(1), core).start()

    def arrive(self):
        self.partner(1 - self.c).wait_recv()
        for core in range(2):
            self.second(1, self.at(2), core).wait_recv()
            self.second(-1, self.at(2), core).wait_recv()

    def drain(self):
        self.partner(self.c).wait_send()
        for core in range(2):
            self.first(1, core, self.y, self.c).wait_send()
            self.first(-1, core, self.y, self.c).wait_send()
            self.second(1, self.y, core).wait_send()
            self.second(-1, self.y, core).wait_send()


class WeightColumn:
    def __init__(self, wk, wv, out, send, recv):
        self.parts, self.out, self.send, self.recv = (wk, wv), out, send, recv
        self.y, self.x = lax.axis_index("y"), lax.axis_index("x")

    def lanes(self, y):
        return pl.ds(pl.multiple_of(y * 128, 128), 128)

    def copy(self, k, i, slot_y):
        to = lax.rem(self.y + k, 4)
        return pltpu.make_async_remote_copy(
            src_ref=self.parts[i].at[:, self.lanes(to)],
            dst_ref=self.out.at[self.x, slot_y, i],
            send_sem=self.send.at[k, i],
            recv_sem=self.recv.at[k, i],
            device_id={"y": to},
            device_id_type=MESH,
        )

    def start(self):
        for k in (2, 1, 3):
            for i in range(2):
                self.copy(k, i, self.y).start()
        for i in range(2):
            self.out[self.x, self.y, i] = self.parts[i][:, self.lanes(self.y)]

    def arrive(self):
        for k in range(1, 4):
            for i in range(2):
                self.copy(k, i, lax.rem(self.y + 4 - k, 4)).wait_recv()

    def drain(self):
        for k in range(1, 4):
            for i in range(2):
                self.copy(k, i, self.y).wait_send()


def unit_rows(matrix, gain):
    wide = matrix.astype(F32)
    factor = lax.rsqrt(jnp.mean(wide * wide, axis=-1, keepdims=True) + EPSILON)
    return wide * factor * gain


def swap_halves(a):
    return pltpu.roll(a, HD, 1)


def forward_kernel(
    nz, target_rows, source_rows, t_gain, s_gain, pair, wk, wv, cot, pick,
    kv_all, stats, out, qa, t_all, pair_all, w_all,
    halves, rows_all, part, part_all, block, blocks, m, l, o, said, heard,
    row_s, row_r, wy_s, wy_r, wx_s, wx_r, ty_s, ty_r, tx_s, tx_r, pair_s, pair_r,
    part_s, part_r, q_s, q_r, rs, rr, ls, lr, ss, sr,
):
    z, y, x, c = (lax.axis_index(a) for a in "zyxc")
    right, left = lax.rem(z + 1, nz), lax.rem(z + nz - 1, nz)
    met = greet(("y", "x", "c")) + ring_greet(nz)

    normed = unit_rows(source_rows[...], s_gain[...])
    low = lanes_below((32, 128), HD)
    for j in range(8):
        chip = (2 * j % 4) * 4 + j // 2
        first, second = (normed[:, 128 * i : 128 * i + 128] for i in (chip, chip + 4))
        halves[0, :, 128 * j : 128 * j + 128] = jnp.where(low, first, swap_halves(second)).astype(BF16)
        halves[1, :, 128 * j : 128 * j + 128] = jnp.where(low, swap_halves(first), second).astype(BF16)
    greeted(met)

    by_rows = RowGather(halves, rows_all, row_s, row_r)
    by_wy = WeightColumn(wk, wv, w_all, wy_s, wy_r)
    by_wx = RingGather("x", lambda slot, p: w_all.at[slot, p], 4, wx_s, wx_r)
    by_ty = RingGather("y", lambda slot, p: t_all.at[x, slot, :, pl.ds(1024 * p, 1024)], 2, ty_s, ty_r)
    by_tx = RingGather("x", lambda slot, p: t_all.at[slot, p], 4, tx_s, tx_r)
    by_pair = Exchange(("c",), pair, pair_all, pair_s, pair_r)
    by_wy.start()
    by_rows.start()
    zero = jnp.zeros((2, target_rows.shape[1]), F32)
    t_all[x, y] = jnp.concatenate(
        [unit_rows(target_rows[...], t_gain[...]), zero, cot[...].astype(F32), zero], axis=0
    ).astype(BF16)
    for p in range(2):
        by_ty.start(p)
    by_pair.start()

    by_wy.arrive()
    for p in range(4):
        by_wx.start(p)
    by_rows.relay()
    for p in range(2):
        by_ty.relay(p)
    for p in range(4):
        by_wx.relay(p)
    for p in range(2):
        by_ty.arrive(p)
    for p in range(4):
        by_tx.start(p)
    by_rows.arrive()
    for p in range(4):
        by_wx.arrive(p)

    rows = rows_all[...].reshape(256, 1024)
    k2 = jnp.dot(rows, w_all[:, :, 0].reshape(1024, 128), preferred_element_type=F32)
    v2 = jnp.dot(rows, w_all[:, :, 1].reshape(1024, 128), preferred_element_type=F32)
    wide_low = lanes_below((256, 128), HD)
    part[0] = jnp.where(wide_low, k2, swap_halves(v2))
    part[1] = jnp.where(wide_low, swap_halves(k2), v2)
    by_part = Exchange(("c",), part, part_all, part_s, part_r, lambda at, i: i)
    by_part.start()
    for p in range(4):
        by_tx.relay(p)
    by_part.arrive()
    kv_all[z] = (part_all[0] + part_all[1]).astype(BF16)

    steps_r = nz // 2
    steps_l = nz - 1 - steps_r
    piece = 256 // PIECES

    def hop(step, p, sign, ahead=0):
        at = lax.rem(z + 2 * nz - sign * (step + ahead), nz)
        ssem, rsem = (rs, rr) if sign > 0 else (ls, lr)
        ref = kv_all.at[at, pl.ds(p * piece, piece)]
        return pltpu.make_async_remote_copy(
            src_ref=ref,
            dst_ref=ref,
            send_sem=ssem.at[step, p],
            recv_sem=rsem.at[step, p],
            device_id={"z": right if sign > 0 else left},
            device_id_type=MESH,
        )

    for p in range(PIECES):
        hop(0, p, 1).start()
        hop(0, p, -1).start()

    def pass_on(s):
        for p in range(PIECES):
            hop(s - 1, p, 1, 1).wait_recv()
            hop(s, p, 1).start()
            hop(s - 1, p, -1, 1).wait_recv()

            @pl.when(s < steps_l)
            def _():
                hop(s, p, -1).start()

    by_pair.arrive()
    for p in range(4):
        by_tx.arrive(p)
    everything = t_all[...].reshape(256, 2048)
    scale = jnp.where(lanes_below((256, 128), HD), HD**-0.5, 1.0)
    for a in range(2):
        both = (contract(everything, pair_all[a], 1, 1) * scale).astype(BF16)
        chosen = jnp.dot(pick[...], both, preferred_element_type=F32)
        block[96 * a : 96 * a + 96] = jnp.where(
            lanes_below((96, 128), HD), chosen[:96], chosen[96:]
        ).astype(BF16)
    by_q = ToReaders(block, blocks, q_s, q_r)
    by_q.start()
    pass_on(jnp.int32(1))
    m[...] = jnp.full(m.shape, -1e30, F32)
    l[...] = jnp.zeros(l.shape, F32)
    o[...] = jnp.zeros(o.shape, F32)
    by_q.arrive()
    qa[...] = blocks[...].reshape(qa.shape)

    def attend(at):
        block = kv_all[at]
        keys = jnp.where(lanes_below(block.shape, HD), block, jnp.zeros_like(block))
        scores = contract(keys, qa[...], 1, 1)
        top = jnp.maximum(m[...], jnp.max(scores, axis=0, keepdims=True))
        weights = jnp.exp(scores - top)
        old = jnp.exp(m[...] - top)
        m[...] = top
        l[...] = l[...] * old + jnp.sum(weights, axis=0, keepdims=True)
        o[...] = o[...] * old + contract(block, weights.astype(BF16), 0, 0)[HD:]

    attend(z)

    def step(s, carry):
        pass_on(s)
        attend(lax.rem(z + nz - s + 1, nz))
        attend(lax.rem(z + s - 1, nz))
        return carry

    lax.fori_loop(2, steps_r, step, 0)
    for p in range(PIECES):
        hop(steps_r - 1, p, 1, 1).wait_recv()

    attend(lax.rem(z + nz - steps_r + 1, nz))
    attend(lax.rem(z + steps_r - 1, nz))
    attend(lax.rem(z + nz - steps_r, nz))
    upright = jnp.transpose(qa[...].astype(F32))
    delta = jnp.sum(upright[HD:] * o[...], axis=0, keepdims=True)
    row = lax.broadcasted_iota(jnp.int32, (8, qa.shape[0]), 0)
    said[...] = jnp.where(row == 0, m[...], jnp.where(row == 1, l[...], delta))
    e = Exchange(("x",), said, heard, ss, sr)
    e.start()
    for by in (by_rows, by_wy, by_wx, by_ty, by_tx, by_pair, by_part, by_q):
        by.drain()

    def drain(s, carry):
        for p in range(PIECES):
            hop(s, p, 1).wait_send()

            @pl.when(s < steps_l)
            def _():
                hop(s, p, -1).wait_send()

        return carry

    lax.fori_loop(0, steps_r, drain, 0)
    e.arrive()
    top = jnp.max(heard[:, 0:1], axis=0)
    total = jnp.zeros_like(top)
    both = jnp.zeros_like(top)
    for j in range(4):
        w = jnp.exp(heard[j, 0:1] - top)
        total = total + w * heard[j, 1:2]
        both = both + w * heard[j, 2:3]
    stats[...] = jnp.where(row == 0, top + jnp.log(total), both / total)
    scaled = o[...] * (jnp.exp(m[...] - top) / total)
    out[...] = jnp.transpose(jnp.concatenate([scaled, jnp.zeros_like(scaled)], axis=0)).astype(BF16)
    e.drain()


def sems(*shape):
    return pltpu.SemaphoreType.DMA(shape)


def forward(args, nz):
    t = 768
    ring = sems(nz // 2, PIECES)
    return pl.pallas_call(
        functools.partial(forward_kernel, nz),
        out_shape=(
            jax.ShapeDtypeStruct((nz, 256, 128), BF16),
            jax.ShapeDtypeStruct((8, t), F32),
            jax.ShapeDtypeStruct((t, 128), BF16),
            jax.ShapeDtypeStruct((t, 128), BF16),
            jax.ShapeDtypeStruct((4, 4, 16, 2048), BF16),
            jax.ShapeDtypeStruct((2, 128, 2048), BF16),
            jax.ShapeDtypeStruct((4, 4, 2, 64, 128), BF16),
        ),
        in_specs=[VMEM] * len(args),
        out_specs=(VMEM,) * 7,
        scratch_shapes=[
            pltpu.VMEM((2, 32, 1024), BF16),
            pltpu.VMEM((4, 2, 32, 1024), BF16),
            pltpu.VMEM((2, 256, 128), F32),
            pltpu.VMEM((2, 256, 128), F32),
            pltpu.VMEM((192, 128), BF16),
            pltpu.VMEM((4, 192, 128), BF16),
            pltpu.VMEM((1, t), F32),
            pltpu.VMEM((1, t), F32),
            pltpu.VMEM((HD, t), F32),
            pltpu.VMEM((8, t), F32),
            pltpu.VMEM((4, 8, t), F32),
            sems(5, 2), sems(5, 2), sems(4, 2), sems(4, 2), sems(3, 4), sems(3, 4),
            sems(3, 2), sems(3, 2), sems(3, 4), sems(3, 4), dma(2), dma(2),
            dma(2), dma(2), dma(4), dma(4), ring, ring, ring, ring, dma(4), dma(4),
        ],
        compiler_params=params(0),
    )(*args)


def backward_kernel(
    nz, qa, kv_all, stats, out, t_all, pair_all, w_all, pick, pick8,
    s_out, t_out, w_out,
    dq, own, tor, tol, inr, inl, outs, dq_block, dqs, o_part, swapped, terms, sums, mine_sum, all_sums,
    kv_grad, grads2, parts, d_parts, s_in, t_in,
    rs, rr, ls, lr, o_s, o_r, dq_s, dq_r, sw_s, sw_r, z_s, z_r, back_s, back_r,
    pair_s, pair_r, s_s, s_r, t_s, t_r,
):
    z, c = lax.axis_index("z"), lax.axis_index("c")
    right, left = lax.rem(z + 1, nz), lax.rem(z + nz - 1, nz)
    greeted(greet(("y", "x", "c")) + greet(("z",)))
    by_o = ToOwners(out, outs, o_s, o_r)
    by_o.start()
    steps_l = nz // 2
    steps_r = nz - 1 - steps_l
    piece = 256 // PIECES
    dq[...] = jnp.zeros(dq.shape, F32)

    def grads(at):
        block = kv_all[at]
        low = lanes_below(block.shape, HD)
        none = jnp.zeros_like(block)
        scores = contract(jnp.where(low, block, none), qa[...], 1, 1)
        probs = jnp.exp(scores - stats[0:1])
        d_probs = contract(jnp.where(low, none, block), qa[...], 1, 1)
        d_scores = (probs * (d_probs - stats[1:2])).astype(BF16)
        for_v = contract(probs.astype(BF16), qa[...], 1, 0)
        for_k = contract(d_scores, qa[...], 1, 0)
        dq[...] += contract(block, d_scores, 0, 0)[:HD]
        return jnp.where(lanes_below(for_k.shape, HD), for_k, for_v)

    def hop(s, p, sign):
        ssem, rsem = (rs, rr) if sign > 0 else (ls, lr)
        src, dst = (tor, inr) if sign > 0 else (tol, inl)
        return pltpu.make_async_remote_copy(
            src_ref=src.at[s, pl.ds(p * piece, piece)],
            dst_ref=dst.at[s, pl.ds(p * piece, piece)],
            send_sem=ssem.at[s, p],
            recv_sem=rsem.at[s, p],
            device_id={"z": right if sign > 0 else left},
            device_id_type=MESH,
        )

    def send_first(sign, value):
        ref = tor if sign > 0 else tol
        ref[0] = value.astype(BF16)
        for p in range(PIECES):
            hop(0, p, sign).start()

    def send_on(s, sign):
        ref, arrived = (tor, inr) if sign > 0 else (tol, inl)
        for p in range(PIECES):
            hop(s - 1, p, sign).wait_recv()
            at = pl.ds(p * piece, piece)
            ref[s, at] = (arrived[s - 1, at].astype(F32) + own[at]).astype(BF16)
            hop(s, p, sign).start()

    send_first(-1, grads(lax.rem(z + nz - steps_l, nz)))
    send_first(1, grads(lax.rem(z + steps_r, nz)))

    by_o.arrive()
    attended = jnp.sum(outs[...].astype(F32), axis=0).astype(BF16)
    everything = t_all[...].reshape(256, 2048)
    for a in range(2):
        spread = contract(pick[96:], attended[96 * a : 96 * a + 96], 0, 0).astype(BF16)
        product = contract(spread, everything, 0, 0)[:HD].astype(BF16)
        for i in range(nz):
            o_part[a, i] = product[:, 128 * i : 128 * i + 128]
    swap = Exchange(("c",), o_part, swapped, sw_s, sw_r, lambda at, i: i)
    swap.start()
    by_z = Exchange(("z",), terms, sums, z_s, z_r, lambda at, i: i)
    back = Exchange(("z",), mine_sum, all_sums, back_s, back_r)

    def step(s, carry):
        own[...] = grads(lax.rem(z + nz - steps_l + s, nz))
        send_on(s, -1)

        @pl.when(s < steps_r)
        def _():
            own[...] = grads(lax.rem(z + steps_r - s, nz))
            send_on(s, 1)

        @pl.when(s == 1)
        def _():
            swap.arrive()
            terms[...] = (swapped[0].astype(F32) + swapped[1].astype(F32)).astype(BF16)
            by_z.start()

        @pl.when(s == steps_l - 1)
        def _():
            by_z.arrive()
            mine_sum[...] = jnp.sum(sums[...].astype(F32), axis=0).astype(BF16)
            back.start()

        return carry

    lax.fori_loop(1, steps_l, step, 0)
    own[...] = grads(z)
    dq_block[...] = (
        jnp.transpose(jnp.concatenate([dq[...], jnp.zeros_like(dq[...])], axis=0)) * HD**-0.5
    ).astype(BF16).reshape(4, 192, 128)
    by_dq = ToOwners(dq_block, dqs, dq_s, dq_r)
    by_dq.start()
    for p in range(PIECES):
        at = pl.ds(p * piece, piece)
        hop(steps_l - 1, p, -1).wait_recv()
        hop(steps_r - 1, p, 1).wait_recv()
        kv_grad[at] = (
            inl[steps_l - 1, at].astype(F32) + inr[steps_r - 1, at].astype(F32) + own[at]
        ).astype(BF16)
    by_pair = Exchange(("c",), kv_grad, grads2, pair_s, pair_r)
    by_pair.start()
    by_dq.arrive()
    query_grad = jnp.sum(dqs[...].astype(F32), axis=0).astype(BF16)
    d_target = jnp.zeros((128, 2048), F32)
    for a in range(2):
        spread = contract(pick8[...], query_grad[96 * a : 96 * a + 96], 0, 0).astype(BF16)
        d_target = d_target + jnp.dot(spread, pair_all[a], preferred_element_type=F32)
    d_parts[...] = d_target.astype(BF16).reshape(16, 8, 2048)
    by_pair.arrive()
    low = lanes_below((256, 128), HD)
    g0, g1 = grads2[0].astype(F32), grads2[1].astype(F32)
    k2 = jnp.where(low, g0, swap_halves(g1)).astype(BF16)
    v2 = jnp.where(low, swap_halves(g0), g1).astype(BF16)
    d_rows = contract(k2, w_all[:, :, 0].reshape(1024, 128), 1, 1)
    d_rows = d_rows + contract(v2, w_all[:, :, 1].reshape(1024, 128), 1, 1)
    parts[...] = d_rows.astype(BF16).reshape(8, 32, 1024)
    by_s = Exchange(("y", "c"), parts, s_in, s_s, s_r, lambda at, i: i)
    by_s.start()
    by_t = Exchange(("x", "y"), d_parts, t_in, t_s, t_r, lambda at, i: i)
    by_t.start()
    back.arrive()
    for i in range(nz):
        w_out[:, 128 * i : 128 * i + 128] = all_sums[i].astype(F32)
    by_t.arrive()
    t_out[...] = jnp.sum(t_in[...].astype(F32), axis=0)
    by_s.arrive()
    low = lanes_below((32, 128), HD)
    for core in range(2):
        got = s_in[core].astype(F32)
        for i in range(1, 4):
            got = got + s_in[2 * i + core].astype(F32)
        parts_f = got
        if core == 0:
            got0 = parts_f
        else:
            got1 = parts_f
    for j in range(8):
        chip = (2 * j % 4) * 4 + j // 2
        a, b = got0[:, 128 * j : 128 * j + 128], got1[:, 128 * j : 128 * j + 128]
        s_out[:, 128 * chip : 128 * chip + 128] = jnp.where(low, a, swap_halves(b))
        s_out[:, 128 * chip + 512 : 128 * chip + 640] = jnp.where(low, swap_halves(a), b)
    for e in (by_o, by_dq, swap, by_z, back, by_pair, by_s, by_t):
        e.drain()

    def drain(s, carry):
        for p in range(PIECES):
            hop(s, p, -1).wait_send()

            @pl.when(s < steps_r)
            def _():
                hop(s, p, 1).wait_send()

        return carry

    lax.fori_loop(0, steps_l, drain, 0)


def backward(args, nz):
    t = 768
    half = nz // 2
    ring = sems(half, PIECES)
    slots = pltpu.VMEM((half, 256, 128), BF16)
    owned = pltpu.VMEM((4, 192, 128), BF16)
    return pl.pallas_call(
        functools.partial(backward_kernel, nz),
        out_shape=(
            jax.ShapeDtypeStruct((32, 2048), F32),
            jax.ShapeDtypeStruct((8, 2048), F32),
            jax.ShapeDtypeStruct((64, 2048), F32),
        ),
        in_specs=[VMEM] * len(args),
        out_specs=(VMEM,) * 3,
        scratch_shapes=[
            pltpu.VMEM((HD, t), F32),
            pltpu.VMEM((256, 128), F32),
            slots, slots, slots, slots,
            owned, owned, owned,
            pltpu.VMEM((2, nz, HD, 128), BF16),
            pltpu.VMEM((2, nz, HD, 128), BF16),
            pltpu.VMEM((nz, HD, 128), BF16),
            pltpu.VMEM((nz, HD, 128), BF16),
            pltpu.VMEM((HD, 128), BF16),
            pltpu.VMEM((nz, HD, 128), BF16),
            pltpu.VMEM((256, 128), BF16),
            pltpu.VMEM((2, 256, 128), BF16),
            pltpu.VMEM((8, 32, 1024), BF16),
            pltpu.VMEM((16, 8, 2048), BF16),
            pltpu.VMEM((8, 32, 1024), BF16),
            pltpu.VMEM((16, 8, 2048), BF16),
            ring, ring, ring, ring, dma(4), dma(4), dma(4), dma(4), dma(2), dma(2),
            dma(nz), dma(nz), dma(nz), dma(nz), dma(2), dma(2), dma(8), dma(8), dma(16), dma(16),
        ],
        compiler_params=params(1),
    )(*args)


def norm_back(matrix, gain, upstream):
    wide = matrix.astype(F32)
    factor = lax.rsqrt(jnp.mean(wide * wide, axis=-1, keepdims=True) + EPSILON)
    weighted = upstream * gain
    inner = jnp.mean(weighted * wide, axis=-1, keepdims=True)
    return factor * weighted - wide * factor**3 * inner


def picks():
    r = jnp.arange(96)
    at = 16 * (r // 6) + r % 6
    pick = jnp.concatenate([at, at + 8])[:, None] == jnp.arange(256)[None]
    pick8 = (8 * (r // 6) + r % 6)[:, None] == jnp.arange(128)[None]
    return pick.astype(BF16), pick8.astype(BF16)


def body(nz, target_rows, source_rows, t_gain, s_gain, wq, wk, wv, wo, cot):
    pick, pick8 = picks()
    pair = jnp.concatenate([wq.T, wo])
    kv_all, stats, out, qa, t_all, pair_all, w_all = forward(
        (target_rows, source_rows, t_gain[None], s_gain[None], pair, wk, wv, cot, pick), nz
    )
    d_source, d_target, o_grad = backward(
        (qa, kv_all, stats, out.reshape(4, 192, 128), t_all, pair_all, w_all, pick, pick8), nz
    )
    source_grad = norm_back(source_rows, s_gain, d_source)
    target_grad = cot.astype(F32) + norm_back(target_rows, t_gain, d_target[:6])
    return target_grad, source_grad, o_grad


def solution(mesh):
    nz = mesh.shape["sp"]
    SIZES["z"] = nz
    fine = Mesh(mesh.devices.reshape(nz, 4, 4, 2), ("z", "y", "x", "c"))
    every, plane = ("z", "y", "x", "c"), ("y", "x", "c")
    return jax.shard_map(
        functools.partial(body, nz),
        mesh=fine,
        in_specs=(
            P(every, None), P(every, None), P(), P(),
            P(None, plane), P(plane, None), P(plane, None), P(plane, None), P(every, None),
        ),
        out_specs=(P(every, None), P(every, None), P(plane, None)),
        check_vma=False,
    )
```

time: 217 us -> 153 us (0.71)
  Pallas kernels: 191 us -> 144 us
  local copies, waits for them, and re-layouts: 13.3 us -> 0.97 us
  matrix products: 2.25 us -> 0 us
    pallas_call x5 -> x0, Pallas kernels: 131 us -> none  [the longest x1 38.4 us: total(): pl.pallas_call(functools.partial(total_kernel, nz), out_shape=jax.ShapeDt...]
    pallas_call x1, Pallas kernels: 24.9 us -> 72.5 us  [backward(): pl.pallas_call(functools.partial(backward_kernel, nz), out_shape=(jax.Sha...]
    pallas_call x1, Pallas kernels: 35.6 us -> 71.2 us  [forward(): pl.pallas_call(functools.partial(forward_kernel, nz), out_shape=(jax.Shap...]
    reshape x11 -> x0, local copies, waits for them, and re-layouts: 5.86 us -> none  [the longest x1 1.92 us: body(): return (target_grad, source_grad, o_grad.reshape(64, 2048))]
    reduce_sum x7 -> x0, other arithmetic: 3.6 us -> none  [the longest x1 1.18 us: body(): d_normed_t = jnp.sum(t_back.astype(F32), axis=0)[:6]]
    dot_general x4 -> x0, matrix products: 2.25 us -> none  [the longest x3 1.95 us: contract(): lax.dot_general(a, b, (((da,), (db,)), ((), ())), preferred_element_type=...]
where the time goes in v2:
time: 153 us
  Pallas kernels  144 us (94%)
  other arithmetic  7.13 us (5%)
    pallas_call x1, Pallas kernels, backward(): pl.pallas_call(functools.partial(backward_kernel, nz), out_shape=(jax.Sha...  72.5 us
    pallas_call x1, Pallas kernels, forward(): pl.pallas_call(functools.partial(forward_kernel, nz), out_shape=(jax.Shap...  71.2 us

profile of v2, /device:TPU:1, one launch (start us, length us, event | category | flops | bytes accessed | tf_op | source)
XLA Modules:
  0.0 152.6 jit_solution(13878356843960646610)
XLA Ops:
  0.7 0.1 pad_add_fusion
  0.7 0.7 fusion.10.pick8
  1.4 0.7 fusion.4.pick
  2.2 1.9 %pad_maximum_fusion.pair = bf16[128,2048]{1,0:T(8,128)(2,1)} fusion(bf16[64,2048]{1,0:T(8,128)(2,1)} %param.16, bf16[64,2048]{1,0:T(8,128)(2,1)} %bitcast.4), kind=kLoop, calls=%fused_computation | loop fusion | flops 1048576 | bytes 1048576 | tf_op jit(solution)/shard_map/concatenate | solution.py:821
  4.0 71.2 %shard_map.112 = (bf16[16,256,128]{2,1,0:T(8,128)(2,1)}, f32[8,768]{1,0:T(8,128)}, bf16[768,128]{1,0:T(8,128)(2,1)}, bf16[768,128]{1,0:T(8,128)(2,1)}, bf16[4,4,...) custom-call(bf16[6,2048]{1,0:T(8,128)(2,1)} %target_rows.1, ...), custom_call_target="tpu_custom_call" | custom-call | tf_op jit(solution)/shard_map/pallas_call | solution.py:563
  75.3 0.0 copy-start.3
  75.3 0.0 copy-start.7
  75.3 72.5 %shard_map.113 = (f32[32,2048]{1,0:T(8,128)}, f32[8,2048]{1,0:T(8,128)}, f32[64,2048]{1,0:T(8,128)}) custom-call(bf16[768,128]{1,0:T(8,128)(2,1)} %get-tuple-element.13.qa, bf16[16,256,128]{2,1,0:T(8,128)(2,1)} %get-tuple-element.14.kv_all, f32[8,768]{1,0:T(8,128)} %get-tuple-element.15.stats, bf16[4,192,128]{2,1,0:T(8,128)(2,1)} %bitcast.5, ...), custom_call_target="tpu_custom_call" | custom-call | tf_op jit(solution)/shard_map/pallas_call | solution.py:770
  147.8 0.0 copy-start.4
  147.8 0.0 copy-done.3
  147.8 0.0 copy-done.7
  147.8 0.0 copy-start.5
  147.8 0.0 copy-start.6
  147.8 1.0 fusion.5
  148.8 0.0 copy-start
  148.9 0.0 copy-done.4
  148.9 0.0 copy-done.5
  148.9 0.0 copy-start.1
  148.9 0.7 fusion.8
  149.6 0.0 copy-done.6
  149.6 0.1 copy-done
  149.7 1.2 fusion
  150.9 0.8 fusion.2
  151.8 0.8 copy.13
  (9 shorter events, 0.1 us)
Async XLA Ops:
  75.3 72.5 %copy-start.3 = (bf16[6,2048]{1,0:T(8,128)(2,1)S(1)}, bf16[6,2048]{1,0:T(8,128)(2,1)}, u32[]{:S(2)}) copy-start(bf16[6,2048]{1,0:T(8,128)(2,1)} %target_rows.1) | copy-start | bytes 73732
  75.3 72.5 %copy-start.7 = (f32[2048]{0:T(1024)S(1)}, f32[2048]{0:T(1024)}, u32[]{:S(2)}) copy-start(f32[2048]{0:T(1024)} %param.11) | copy-start | bytes 24580
  147.8 1.1 copy-start.4
  147.8 1.1 copy-start.5
  147.8 1.8 %copy-start.6 = (f32[2048]{0:T(1024)S(1)}, f32[2048]{0:T(1024)}, u32[]{:S(2)}) copy-start(f32[2048]{0:T(1024)} %param.12) | copy-start | bytes 24580
  148.8 0.9 copy-start
  148.9 2.1 %copy-start.1 = (f32[32,2048]{1,0:T(8,128)S(1)}, f32[32,2048]{1,0:T(8,128)}, u32[]{:S(2)}) copy-start(f32[32,2048]{1,0:T(8,128)} %get-tuple-element.21) | copy-start | bytes 786436
  149.7 2.0 %copy-start.2 = (f32[64,2048]{1,0:T(8,128)S(1)}, f32[64,2048]{1,0:T(8,128)}, u32[]{:S(2)}) copy-start(f32[64,2048]{1,0:T(8,128)} %get-tuple-element.38) | copy-start | bytes 1572868

commit v3 on v2

--- a/solution.py
+++ b/solution.py
@@ -15,6 +15,7 @@
 VMEM = pl.BlockSpec(memory_space=pltpu.VMEM)
 SIZES = {"y": 4, "x": 4, "c": 2}
 PIECES = 2
+REACH = 4
 
 
 def dma(n):
@@ -377,16 +378,139 @@
     return pltpu.roll(a, HD, 1)
 
 
-def forward_kernel(
-    nz, target_rows, source_rows, t_gain, s_gain, pair, wk, wv, cot, pick,
+class RingSum:
+    def __init__(self, nz, term, out, arrived, send, recv, pieces):
+        self.nz, self.term, self.out, self.arrived = nz, term, out, arrived
+        self.send, self.recv, self.pieces = send, recv, pieces
+        self.rows = out.shape[2] // pieces
+        self.last = (nz // 2 - 1, nz // 2 - 2)
+        z = lax.axis_index("z")
+        self.to = (lax.rem(z + nz - 1, nz), lax.rem(z + 1, nz))
+
+    def hop(self, side, s, p):
+        at = pl.ds(p * self.rows, self.rows)
+        return pltpu.make_async_remote_copy(
+            src_ref=self.out.at[side, s, at],
+            dst_ref=self.arrived.at[side, s, at],
+            send_sem=self.send.at[side, s, p],
+            recv_sem=self.recv.at[side, s, p],
+            device_id={"z": self.to[side]},
+            device_id_type=MESH,
+        )
+
+    def first(self, side):
+        self.out[side, 0] = self.term(side, 0, pl.ds(0, self.rows * self.pieces)).astype(BF16)
+        for p in range(self.pieces):
+            self.hop(side, 0, p).start()
+
+    def step(self, s, side):
+        for p in range(self.pieces):
+            at = pl.ds(p * self.rows, self.rows)
+            self.hop(side, s - 1, p).wait_recv()
+            value = self.arrived[side, s - 1, at].astype(F32) + self.term(side, s, at)
+            self.out[side, s, at] = value.astype(BF16)
+            self.hop(side, s, p).start()
+
+    def total(self, p):
+        at = pl.ds(p * self.rows, self.rows)
+        value = self.term(1, self.nz // 2 - 1, at)
+        for side in (1, 0):
+            self.hop(side, self.last[side], p).wait_recv()
+            value = value + self.arrived[side, self.last[side], at].astype(F32)
+        return value
+
+    def drain(self):
+        def one(s, carry):
+            for p in range(self.pieces):
+                self.hop(0, s, p).wait_send()
+                self.hop(1, s, p).wait_send()
+            return carry
+
+        lax.fori_loop(0, self.last[1] + 1, one, 0)
+        for p in range(self.pieces):
+            self.hop(0, self.last[0], p).wait_send()
+
+
+class FarGather:
+    def __init__(self, nz, src, dst, send, recv):
+        self.nz, self.src, self.dst, self.send, self.recv = nz, src, dst, send, recv
+        self.z = lax.axis_index("z")
+        self.far = {1: nz // 2 - REACH, -1: nz - 1 - nz // 2 - REACH}
+
+    def at(self, offset):
+        return lax.rem(self.z + offset + self.nz, self.nz)
+
+    def copy(self, slot, sign, d, relay):
+        i, j = (2 if relay else 0) + (0 if sign > 0 else 1), d - 1
+        return pltpu.make_async_remote_copy(
+            src_ref=self.dst.at[slot] if relay else self.src,
+            dst_ref=self.dst.at[slot],
+            send_sem=self.send.at[i, j],
+            recv_sem=self.recv.at[i, j],
+            device_id={"z": self.at(sign * d)},
+            device_id_type=MESH,
+        )
+
+    def start(self):
+        for d in range(REACH, 0, -1):
+            for sign in (1, -1):
+                self.copy(self.z, sign, d, False).start()
+        self.dst[self.z] = self.src[...]
+
+    def relay(self):
+        for sign in (1, -1):
+            slot = self.at(-sign * REACH)
+            self.copy(slot, sign, REACH, False).wait_recv()
+            for d in range(self.far[sign], 0, -1):
+                self.copy(slot, sign, d, True).start()
+
+    def arrive(self):
+        for sign in (1, -1):
+            for d in range(1, REACH):
+                self.copy(self.at(-sign * d), sign, d, False).wait_recv()
+            for d in range(1, self.far[sign] + 1):
+                self.copy(self.at(-sign * (REACH + d)), sign, d, True).wait_recv()
+
+    def drain(self):
+        for sign in (1, -1):
+            for d in range(1, REACH + 1):
+                self.copy(self.z, sign, d, False).wait_send()
+            for d in range(1, self.far[sign] + 1):
+                self.copy(self.z, sign, d, True).wait_send()
+
+
+def reach_greet(nz):
+    z = lax.axis_index("z")
+    for d in range(1, REACH + 1):
+        for sign in (1, -1):
+            pl.semaphore_signal(
+                pltpu.get_barrier_semaphore(),
+                inc=1,
+                device_id={"z": lax.rem(z + sign * d + nz, nz)},
+                device_id_type=MESH,
+            )
+    return 2 * REACH
+
+
+def sems(*shape):
+    return pltpu.SemaphoreType.DMA(shape)
+
+
+def kernel(
+    nz, target_rows, source_rows, t_gain, s_gain, pair, wk, wv, cot, pick, pick8,
+    s_out, t_out, w_out,
     kv_all, stats, out, qa, t_all, pair_all, w_all,
     halves, rows_all, part, part_all, block, blocks, m, l, o, said, heard,
+    dq, mine, ring_out, ring_in, w_ring_out, w_ring_in, outs, dq_block, dqs, o_part, swapped,
+    mine_sum, all_sums, kv_grad, grads2, parts, d_parts, s_in, t_in,
     row_s, row_r, wy_s, wy_r, wx_s, wx_r, ty_s, ty_r, tx_s, tx_r, pair_s, pair_r,
     part_s, part_r, q_s, q_r, rs, rr, ls, lr, ss, sr,
+    o_s, o_r, dq_s, dq_r, sw_s, sw_r, g_s, g_r, h_s, h_r, back_s, back_r,
+    kv_s, kv_r, s_s, s_r, t_s, t_r,
 ):
     z, y, x, c = (lax.axis_index(a) for a in "zyxc")
     right, left = lax.rem(z + 1, nz), lax.rem(z + nz - 1, nz)
-    met = greet(("y", "x", "c")) + ring_greet(nz)
+    met = greet(("y", "x", "c")) + reach_greet(nz)
 
     normed = unit_rows(source_rows[...], s_gain[...])
     low = lanes_below((32, 128), HD)
@@ -437,8 +561,6 @@
     part[1] = jnp.where(wide_low, swap_halves(k2), v2)
     by_part = Exchange(("c",), part, part_all, part_s, part_r, lambda at, i: i)
     by_part.start()
-    for p in range(4):
-        by_tx.relay(p)
     by_part.arrive()
     kv_all[z] = (part_all[0] + part_all[1]).astype(BF16)
 
@@ -473,6 +595,9 @@
             def _():
                 hop(s, p, -1).start()
 
+    for p in range(4):
+        by_tx.relay(p)
+    pass_on(jnp.int32(1))
     by_pair.arrive()
     for p in range(4):
         by_tx.arrive(p)
@@ -486,7 +611,7 @@
         ).astype(BF16)
     by_q = ToReaders(block, blocks, q_s, q_r)
     by_q.start()
-    pass_on(jnp.int32(1))
+    pass_on(jnp.int32(2))
     m[...] = jnp.full(m.shape, -1e30, F32)
     l[...] = jnp.zeros(l.shape, F32)
     o[...] = jnp.zeros(o.shape, F32)
@@ -504,42 +629,30 @@
         l[...] = l[...] * old + jnp.sum(weights, axis=0, keepdims=True)
         o[...] = o[...] * old + contract(block, weights.astype(BF16), 0, 0)[HD:]
 
+    def attend_both(d):
+        attend(lax.rem(z + nz - d, nz))
+        attend(lax.rem(z + d, nz))
+
     attend(z)
+    attend_both(1)
 
     def step(s, carry):
         pass_on(s)
-        attend(lax.rem(z + nz - s + 1, nz))
-        attend(lax.rem(z + s - 1, nz))
+        attend_both(s - 1)
         return carry
 
-    lax.fori_loop(2, steps_r, step, 0)
+    lax.fori_loop(3, steps_r, step, 0)
+    attend_both(steps_r - 1)
     for p in range(PIECES):
         hop(steps_r - 1, p, 1, 1).wait_recv()
-
-    attend(lax.rem(z + nz - steps_r + 1, nz))
-    attend(lax.rem(z + steps_r - 1, nz))
     attend(lax.rem(z + nz - steps_r, nz))
     upright = jnp.transpose(qa[...].astype(F32))
     delta = jnp.sum(upright[HD:] * o[...], axis=0, keepdims=True)
     row = lax.broadcasted_iota(jnp.int32, (8, qa.shape[0]), 0)
     said[...] = jnp.where(row == 0, m[...], jnp.where(row == 1, l[...], delta))
-    e = Exchange(("x",), said, heard, ss, sr)
-    e.start()
-    for by in (by_rows, by_wy, by_wx, by_ty, by_tx, by_pair, by_part, by_q):
-        by.drain()
-
-    def drain(s, carry):
-        for p in range(PIECES):
-            hop(s, p, 1).wait_send()
-
-            @pl.when(s < steps_l)
-            def _():
-                hop(s, p, -1).wait_send()
-
-        return carry
-
-    lax.fori_loop(0, steps_r, drain, 0)
-    e.arrive()
+    by_stats = Exchange(("x",), said, heard, ss, sr)
+    by_stats.start()
+    by_stats.arrive()
     top = jnp.max(heard[:, 0:1], axis=0)
     total = jnp.zeros_like(top)
     both = jnp.zeros_like(top)
@@ -549,69 +662,15 @@
         both = both + w * heard[j, 2:3]
     stats[...] = jnp.where(row == 0, top + jnp.log(total), both / total)
     scaled = o[...] * (jnp.exp(m[...] - top) / total)
-    out[...] = jnp.transpose(jnp.concatenate([scaled, jnp.zeros_like(scaled)], axis=0)).astype(BF16)
-    e.drain()
-
-
-def sems(*shape):
-    return pltpu.SemaphoreType.DMA(shape)
-
-
-def forward(args, nz):
-    t = 768
-    ring = sems(nz // 2, PIECES)
-    return pl.pallas_call(
-        functools.partial(forward_kernel, nz),
-        out_shape=(
-            jax.ShapeDtypeStruct((nz, 256, 128), BF16),
-            jax.ShapeDtypeStruct((8, t), F32),
-            jax.ShapeDtypeStruct((t, 128), BF16),
-            jax.ShapeDtypeStruct((t, 128), BF16),
-            jax.ShapeDtypeStruct((4, 4, 16, 2048), BF16),
-            jax.ShapeDtypeStruct((2, 128, 2048), BF16),
-            jax.ShapeDtypeStruct((4, 4, 2, 64, 128), BF16),
-        ),
-        in_specs=[VMEM] * len(args),
-        out_specs=(VMEM,) * 7,
-        scratch_shapes=[
-            pltpu.VMEM((2, 32, 1024), BF16),
-            pltpu.VMEM((4, 2, 32, 1024), BF16),
-            pltpu.VMEM((2, 256, 128), F32),
-            pltpu.VMEM((2, 256, 128), F32),
-            pltpu.VMEM((192, 128), BF16),
-            pltpu.VMEM((4, 192, 128), BF16),
-            pltpu.VMEM((1, t), F32),
-            pltpu.VMEM((1, t), F32),
-            pltpu.VMEM((HD, t), F32),
-            pltpu.VMEM((8, t), F32),
-            pltpu.VMEM((4, 8, t), F32),
-            sems(5, 2), sems(5, 2), sems(4, 2), sems(4, 2), sems(3, 4), sems(3, 4),
-            sems(3, 2), sems(3, 2), sems(3, 4), sems(3, 4), dma(2), dma(2),
-            dma(2), dma(2), dma(4), dma(4), ring, ring, ring, ring, dma(4), dma(4),
-        ],
-        compiler_params=params(0),
-    )(*args)
-
-
-def backward_kernel(
-    nz, qa, kv_all, stats, out, t_all, pair_all, w_all, pick, pick8,
-    s_out, t_out, w_out,
-    dq, own, tor, tol, inr, inl, outs, dq_block, dqs, o_part, swapped, terms, sums, mine_sum, all_sums,
-    kv_grad, grads2, parts, d_parts, s_in, t_in,
-    rs, rr, ls, lr, o_s, o_r, dq_s, dq_r, sw_s, sw_r, z_s, z_r, back_s, back_r,
-    pair_s, pair_r, s_s, s_r, t_s, t_r,
-):
-    z, c = lax.axis_index("z"), lax.axis_index("c")
-    right, left = lax.rem(z + 1, nz), lax.rem(z + nz - 1, nz)
-    greeted(greet(("y", "x", "c")) + greet(("z",)))
+    upright = jnp.concatenate([scaled, jnp.zeros_like(scaled)], axis=0)
+    out[...] = jnp.transpose(upright).astype(BF16).reshape(out.shape)
+
     by_o = ToOwners(out, outs, o_s, o_r)
     by_o.start()
-    steps_l = nz // 2
-    steps_r = nz - 1 - steps_l
-    piece = 256 // PIECES
     dq[...] = jnp.zeros(dq.shape, F32)
 
-    def grads(at):
+    def grads(side, j):
+        at = lax.rem(z + nz - nz // 2 + j, nz) if side == 0 else lax.rem(z + nz // 2 - 1 - j, nz)
         block = kv_all[at]
         low = lanes_below(block.shape, HD)
         none = jnp.zeros_like(block)
@@ -622,153 +681,146 @@
         for_v = contract(probs.astype(BF16), qa[...], 1, 0)
         for_k = contract(d_scores, qa[...], 1, 0)
         dq[...] += contract(block, d_scores, 0, 0)[:HD]
-        return jnp.where(lanes_below(for_k.shape, HD), for_k, for_v)
-
-    def hop(s, p, sign):
-        ssem, rsem = (rs, rr) if sign > 0 else (ls, lr)
-        src, dst = (tor, inr) if sign > 0 else (tol, inl)
-        return pltpu.make_async_remote_copy(
-            src_ref=src.at[s, pl.ds(p * piece, piece)],
-            dst_ref=dst.at[s, pl.ds(p * piece, piece)],
-            send_sem=ssem.at[s, p],
-            recv_sem=rsem.at[s, p],
-            device_id={"z": right if sign > 0 else left},
-            device_id_type=MESH,
-        )
-
-    def send_first(sign, value):
-        ref = tor if sign > 0 else tol
-        ref[0] = value.astype(BF16)
-        for p in range(PIECES):
-            hop(0, p, sign).start()
-
-    def send_on(s, sign):
-        ref, arrived = (tor, inr) if sign > 0 else (tol, inl)
-        for p in range(PIECES):
-            hop(s - 1, p, sign).wait_recv()
-            at = pl.ds(p * piece, piece)
-            ref[s, at] = (arrived[s - 1, at].astype(F32) + own[at]).astype(BF16)
-            hop(s, p, sign).start()
-
-    send_first(-1, grads(lax.rem(z + nz - steps_l, nz)))
-    send_first(1, grads(lax.rem(z + steps_r, nz)))
+        mine[side, j] = jnp.where(lanes_below(for_k.shape, HD), for_k, for_v)
+
+    main = RingSum(nz, lambda side, j, at: mine[side, j, at], ring_out, ring_in, g_s, g_r, PIECES)
+
+    def own_weight(side, j, at):
+        to = lax.rem(z + nz - nz // 2 + j, nz) if side == 0 else lax.rem(z + nz // 2 - 1 - j, nz)
+        return swapped[0, to, at].astype(F32) + swapped[1, to, at].astype(F32)
+
+    weight = RingSum(nz, own_weight, w_ring_out, w_ring_in, h_s, h_r, 1)
+    for side in range(2):
+        grads(side, 0)
+        main.first(side)
+    for side in range(2):
+        grads(side, 1)
 
     by_o.arrive()
     attended = jnp.sum(outs[...].astype(F32), axis=0).astype(BF16)
-    everything = t_all[...].reshape(256, 2048)
     for a in range(2):
         spread = contract(pick[96:], attended[96 * a : 96 * a + 96], 0, 0).astype(BF16)
-        product = contract(spread, everything, 0, 0)[:HD].astype(BF16)
+        product = contract(spread, t_all[...].reshape(256, 2048), 0, 0)[:HD].astype(BF16)
         for i in range(nz):
             o_part[a, i] = product[:, 128 * i : 128 * i + 128]
     swap = Exchange(("c",), o_part, swapped, sw_s, sw_r, lambda at, i: i)
     swap.start()
-    by_z = Exchange(("z",), terms, sums, z_s, z_r, lambda at, i: i)
-    back = Exchange(("z",), mine_sum, all_sums, back_s, back_r)
-
-    def step(s, carry):
-        own[...] = grads(lax.rem(z + nz - steps_l + s, nz))
-        send_on(s, -1)
-
-        @pl.when(s < steps_r)
-        def _():
-            own[...] = grads(lax.rem(z + steps_r - s, nz))
-            send_on(s, 1)
-
-        @pl.when(s == 1)
-        def _():
-            swap.arrive()
-            terms[...] = (swapped[0].astype(F32) + swapped[1].astype(F32)).astype(BF16)
-            by_z.start()
-
-        @pl.when(s == steps_l - 1)
-        def _():
-            by_z.arrive()
-            mine_sum[...] = jnp.sum(sums[...].astype(F32), axis=0).astype(BF16)
-            back.start()
-
+    for side in range(2):
+        main.step(1, side)
+    for side in range(2):
+        grads(side, 2)
+        grads(side, 3)
+    swap.arrive()
+    for side in range(2):
+        weight.first(side)
+
+    def ahead(s, carry):
+        for side in range(2):
+            main.step(s, side)
+        for side in range(2):
+            weight.step(s - 1, side)
+        for side in range(2):
+            grads(side, 2 * s)
+            grads(side, 2 * s + 1)
         return carry
 
-    lax.fori_loop(1, steps_l, step, 0)
-    own[...] = grads(z)
-    dq_block[...] = (
-        jnp.transpose(jnp.concatenate([dq[...], jnp.zeros_like(dq[...])], axis=0)) * HD**-0.5
-    ).astype(BF16).reshape(4, 192, 128)
+    lax.fori_loop(2, nz // 4, ahead, 0)
+    upright = jnp.concatenate([dq[...], jnp.zeros_like(dq[...])], axis=0) * HD**-0.5
+    dq_block[...] = jnp.transpose(upright).astype(BF16).reshape(4, 192, 128)
     by_dq = ToOwners(dq_block, dqs, dq_s, dq_r)
     by_dq.start()
+    by_t = Exchange(("x", "y"), d_parts, t_in, t_s, t_r, lambda at, i: i)
+
+    def behind(s, carry):
+        main.step(s, 0)
+
+        @pl.when(s < nz // 2 - 1)
+        def _():
+            main.step(s, 1)
+
+        for side in range(2):
+            weight.step(s - 1, side)
+
+        @pl.when(s == nz // 4)
+        def _():
+            by_dq.arrive()
+            query_grad = jnp.sum(dqs[...].astype(F32), axis=0).astype(BF16)
+            d_target = jnp.zeros((128, 2048), F32)
+            for a in range(2):
+                spread = contract(pick8[...], query_grad[96 * a : 96 * a + 96], 0, 0).astype(BF16)
+                d_target = d_target + jnp.dot(spread, pair_all[a], preferred_element_type=F32)
+            d_parts[...] = d_target.astype(BF16).reshape(16, 8, 2048)
+            by_t.start()
+
+        return carry
+
+    lax.fori_loop(nz // 4, nz // 2, behind, 0)
+    weight.step(nz // 2 - 1, 0)
     for p in range(PIECES):
-        at = pl.ds(p * piece, piece)
-        hop(steps_l - 1, p, -1).wait_recv()
-        hop(steps_r - 1, p, 1).wait_recv()
-        kv_grad[at] = (
-            inl[steps_l - 1, at].astype(F32) + inr[steps_r - 1, at].astype(F32) + own[at]
-        ).astype(BF16)
-    by_pair = Exchange(("c",), kv_grad, grads2, pair_s, pair_r)
-    by_pair.start()
-    by_dq.arrive()
-    query_grad = jnp.sum(dqs[...].astype(F32), axis=0).astype(BF16)
-    d_target = jnp.zeros((128, 2048), F32)
-    for a in range(2):
-        spread = contract(pick8[...], query_grad[96 * a : 96 * a + 96], 0, 0).astype(BF16)
-        d_target = d_target + jnp.dot(spread, pair_all[a], preferred_element_type=F32)
-    d_parts[...] = d_target.astype(BF16).reshape(16, 8, 2048)
-    by_pair.arrive()
-    low = lanes_below((256, 128), HD)
+        kv_grad[pl.ds(p * piece, piece)] = main.total(p).astype(BF16)
+    by_kv = Exchange(("c",), kv_grad, grads2, kv_s, kv_r)
+    by_kv.start()
+    by_kv.arrive()
     g0, g1 = grads2[0].astype(F32), grads2[1].astype(F32)
-    k2 = jnp.where(low, g0, swap_halves(g1)).astype(BF16)
-    v2 = jnp.where(low, swap_halves(g0), g1).astype(BF16)
+    k2 = jnp.where(wide_low, g0, swap_halves(g1)).astype(BF16)
+    v2 = jnp.where(wide_low, swap_halves(g0), g1).astype(BF16)
     d_rows = contract(k2, w_all[:, :, 0].reshape(1024, 128), 1, 1)
     d_rows = d_rows + contract(v2, w_all[:, :, 1].reshape(1024, 128), 1, 1)
     parts[...] = d_rows.astype(BF16).reshape(8, 32, 1024)
     by_s = Exchange(("y", "c"), parts, s_in, s_s, s_r, lambda at, i: i)
     by_s.start()
-    by_t = Exchange(("x", "y"), d_parts, t_in, t_s, t_r, lambda at, i: i)
-    by_t.start()
+    mine_sum[...] = weight.total(0).astype(BF16)
+    back = FarGather(nz, mine_sum, all_sums, back_s, back_r)
+    back.start()
+    by_t.arrive()
+    t_out[...] = jnp.sum(t_in[...].astype(F32), axis=0)
+    back.relay()
+    by_s.arrive()
+    got = []
+    for core in range(2):
+        total = s_in[core].astype(F32)
+        for i in range(1, 4):
+            total = total + s_in[2 * i + core].astype(F32)
+        got.append(total)
+    for j in range(8):
+        chip = (2 * j % 4) * 4 + j // 2
+        a, b = (g[:, 128 * j : 128 * j + 128] for g in got)
+        s_out[:, 128 * chip : 128 * chip + 128] = jnp.where(low, a, swap_halves(b))
+        s_out[:, 128 * chip + 512 : 128 * chip + 640] = jnp.where(low, swap_halves(a), b)
     back.arrive()
     for i in range(nz):
         w_out[:, 128 * i : 128 * i + 128] = all_sums[i].astype(F32)
-    by_t.arrive()
-    t_out[...] = jnp.sum(t_in[...].astype(F32), axis=0)
-    by_s.arrive()
-    low = lanes_below((32, 128), HD)
-    for core in range(2):
-        got = s_in[core].astype(F32)
-        for i in range(1, 4):
-            got = got + s_in[2 * i + core].astype(F32)
-        parts_f = got
-        if core == 0:
-            got0 = parts_f
-        else:
-            got1 = parts_f
-    for j in range(8):
-        chip = (2 * j % 4) * 4 + j // 2
-        a, b = got0[:, 128 * j : 128 * j + 128], got1[:, 128 * j : 128 * j + 128]
-        s_out[:, 128 * chip : 128 * chip + 128] = jnp.where(low, a, swap_halves(b))
-        s_out[:, 128 * chip + 512 : 128 * chip + 640] = jnp.where(low, swap_halves(a), b)
-    for e in (by_o, by_dq, swap, by_z, back, by_pair, by_s, by_t):
-        e.drain()
-
-    def drain(s, carry):
+    for by in (by_stats, by_o, by_dq, swap, back, by_kv, by_s, by_t, main, weight):
+        by.drain()
+    for by in (by_rows, by_wy, by_wx, by_ty, by_tx, by_pair, by_part, by_q):
+        by.drain()
+
+    def drain_gather(s, carry):
         for p in range(PIECES):
-            hop(s, p, -1).wait_send()
-
-            @pl.when(s < steps_r)
+            hop(s, p, 1).wait_send()
+
+            @pl.when(s < steps_l)
             def _():
-                hop(s, p, 1).wait_send()
+                hop(s, p, -1).wait_send()
 
         return carry
 
-    lax.fori_loop(0, steps_l, drain, 0)
-
-
-def backward(args, nz):
+    lax.fori_loop(0, steps_r, drain_gather, 0)
+
+
+def whole(args, nz):
     t = 768
     half = nz // 2
     ring = sems(half, PIECES)
-    slots = pltpu.VMEM((half, 256, 128), BF16)
-    owned = pltpu.VMEM((4, 192, 128), BF16)
+
+    def bf16(*shape):
+        return pltpu.VMEM(shape, BF16)
+
+    def f32(*shape):
+        return pltpu.VMEM(shape, F32)
+
     return pl.pallas_call(
-        functools.partial(backward_kernel, nz),
+        functools.partial(kernel, nz),
         out_shape=(
             jax.ShapeDtypeStruct((32, 2048), F32),
             jax.ShapeDtypeStruct((8, 2048), F32),
@@ -777,26 +829,25 @@
         in_specs=[VMEM] * len(args),
         out_specs=(VMEM,) * 3,
         scratch_shapes=[
-            pltpu.VMEM((HD, t), F32),
-            pltpu.VMEM((256, 128), F32),
-            slots, slots, slots, slots,
-            owned, owned, owned,
-            pltpu.VMEM((2, nz, HD, 128), BF16),
-            pltpu.VMEM((2, nz, HD, 128), BF16),
-            pltpu.VMEM((nz, HD, 128), BF16),
-            pltpu.VMEM((nz, HD, 128), BF16),
-            pltpu.VMEM((HD, 128), BF16),
-            pltpu.VMEM((nz, HD, 128), BF16),
-            pltpu.VMEM((256, 128), BF16),
-            pltpu.VMEM((2, 256, 128), BF16),
-            pltpu.VMEM((8, 32, 1024), BF16),
-            pltpu.VMEM((16, 8, 2048), BF16),
-            pltpu.VMEM((8, 32, 1024), BF16),
-            pltpu.VMEM((16, 8, 2048), BF16),
-            ring, ring, ring, ring, dma(4), dma(4), dma(4), dma(4), dma(2), dma(2),
-            dma(nz), dma(nz), dma(nz), dma(nz), dma(2), dma(2), dma(8), dma(8), dma(16), dma(16),
+            bf16(nz, 256, 128), f32(8, t), bf16(4, 192, 128), bf16(t, 128),
+            bf16(4, 4, 16, 2048), bf16(2, 128, 2048), bf16(4, 4, 2, 64, 128),
+            bf16(2, 32, 1024), bf16(4, 2, 32, 1024), f32(2, 256, 128), f32(2, 256, 128),
+            bf16(192, 128), bf16(4, 192, 128), f32(1, t), f32(1, t), f32(HD, t), f32(8, t), f32(4, 8, t),
+            f32(HD, t), f32(2, half, 256, 128), bf16(2, half, 256, 128), bf16(2, half, 256, 128),
+            bf16(2, half, HD, 128), bf16(2, half, HD, 128),
+            bf16(4, 192, 128), bf16(4, 192, 128), bf16(4, 192, 128),
+            bf16(2, nz, HD, 128), bf16(2, nz, HD, 128), bf16(HD, 128), bf16(nz, HD, 128),
+            bf16(256, 128), bf16(2, 256, 128), bf16(8, 32, 1024), bf16(16, 8, 2048),
+            bf16(8, 32, 1024), bf16(16, 8, 2048),
+            sems(5, 2), sems(5, 2), sems(4, 2), sems(4, 2), sems(3, 4), sems(3, 4),
+            sems(3, 2), sems(3, 2), sems(3, 4), sems(3, 4), dma(2), dma(2),
+            dma(2), dma(2), dma(4), dma(4), ring, ring, ring, ring, dma(4), dma(4),
+            dma(4), dma(4), dma(4), dma(4), dma(2), dma(2),
+            sems(2, half, PIECES), sems(2, half, PIECES), sems(2, half, 1), sems(2, half, 1),
+            sems(4, REACH), sems(4, REACH),
+            dma(2), dma(2), dma(8), dma(8), dma(16), dma(16),
         ],
-        compiler_params=params(1),
+        compiler_params=params(0),
     )(*args)
 
 
@@ -819,11 +870,8 @@
 def body(nz, target_rows, source_rows, t_gain, s_gain, wq, wk, wv, wo, cot):
     pick, pick8 = picks()
     pair = jnp.concatenate([wq.T, wo])
-    kv_all, stats, out, qa, t_all, pair_all, w_all = forward(
-        (target_rows, source_rows, t_gain[None], s_gain[None], pair, wk, wv, cot, pick), nz
-    )
-    d_source, d_target, o_grad = backward(
-        (qa, kv_all, stats, out.reshape(4, 192, 128), t_all, pair_all, w_all, pick, pick8), nz
+    d_source, d_target, o_grad = whole(
+        (target_rows, source_rows, t_gain[None], s_gain[None], pair, wk, wv, cot, pick, pick8), nz
     )
     source_grad = norm_back(source_rows, s_gain, d_source)
     target_grad = cot.astype(F32) + norm_back(target_rows, t_gain, d_target[:6])

time: 153 us -> 126 us (0.82); the launches traced: 153 us -> 124 us
  Pallas kernels: 144 us -> 115 us
    pallas_call x2 -> x1, Pallas kernels: 144 us -> 115 us  [whole(): pl.pallas_call(functools.partial(kernel, nz), out_shape=(jax.ShapeDtypeSt...]
where the time goes in v3:
time: 126 us; the launch traced here: 124 us
  Pallas kernels  115 us (91%)
  other arithmetic  7.13 us (6%)
    pallas_call x1, Pallas kernels, whole(): pl.pallas_call(functools.partial(kernel, nz), out_shape=(jax.ShapeDtypeSt...  115 us

profile of v3, /device:TPU:1, one launch (start us, length us, event | category | flops | bytes accessed | tf_op | source)
XLA Modules:
  0.0 123.9 jit_solution(10200636141708941576)
XLA Ops:
  0.7 0.1 pad_add_fusion
  0.7 0.7 fusion.10.pick8
  1.4 0.7 fusion.4.pick
  2.2 1.9 %pad_maximum_fusion.pair = bf16[128,2048]{1,0:T(8,128)(2,1)} fusion(bf16[64,2048]{1,0:T(8,128)(2,1)} %param.16, bf16[64,2048]{1,0:T(8,128)(2,1)} %bitcast.3), kind=kLoop, calls=%fused_computation | loop fusion | flops 1048576 | bytes 1048576 | tf_op jit(solution)/shard_map/concatenate | solution.py:872
  4.0 0.0 copy-start.3
  4.0 115.1 %shard_map.112 = (f32[32,2048]{1,0:T(8,128)}, f32[8,2048]{1,0:T(8,128)}, f32[64,2048]{1,0:T(8,128)}) custom-call(bf16[6,2048]{1,0:T(8,128)(2,1)} %target_rows.1, bf16[32,2048]{1,0:T(8,128)(2,1)} %source_rows.1, f32[1,2048]{1,0:T(1,128)} %bitcast.5, f32[1,2048]{1,0:T(1,128)} %bitcast.4, bf16[128,2048]{1,0:T(8,128)(2,1)} %pad_maximum_fusion.pair, ...), custom_call_target="tpu_custom_call" | custom-call | tf_op jit(solution)/shard_map/pallas_call | solution.py:822
  119.1 0.0 copy-start.4
  119.1 0.0 copy-done.3
  119.1 0.0 copy-done.7
  119.1 0.0 copy-start.5
  119.1 0.0 copy-start.6
  119.1 1.0 fusion.5
  120.2 0.0 copy-start
  120.2 0.0 copy-done.4
  120.2 0.0 copy-done.5
  120.2 0.0 copy-start.1
  120.2 0.7 fusion.8
  120.9 0.0 copy-done.6
  120.9 0.1 copy-done
  121.1 1.2 fusion
  122.3 0.0 copy-done.1
  122.3 0.8 fusion.2
  123.1 0.0 copy-done.2
  123.1 0.8 copy.13
  (8 shorter events, 0.1 us)
Async XLA Ops:
  4.0 115.1 %copy-start.3 = (bf16[6,2048]{1,0:T(8,128)(2,1)S(1)}, bf16[6,2048]{1,0:T(8,128)(2,1)}, u32[]{:S(2)}) copy-start(bf16[6,2048]{1,0:T(8,128)(2,1)} %target_rows.1) | copy-start | bytes 73732
  4.0 115.1 %copy-start.7 = (f32[2048]{0:T(1024)S(1)}, f32[2048]{0:T(1024)}, u32[]{:S(2)}) copy-start(f32[2048]{0:T(1024)} %param.11) | copy-start | bytes 24580
  119.1 1.1 copy-start.4
  119.1 1.1 copy-start.5
  119.1 1.8 %copy-start.6 = (f32[2048]{0:T(1024)S(1)}, f32[2048]{0:T(1024)}, u32[]{:S(2)}) copy-start(f32[2048]{0:T(1024)} %param.12) | copy-start | bytes 24580
  120.2 0.9 copy-start
  120.2 2.1 %copy-start.1 = (f32[32,2048]{1,0:T(8,128)S(1)}, f32[32,2048]{1,0:T(8,128)}, u32[]{:S(2)}) copy-start(f32[32,2048]{1,0:T(8,128)} %get-tuple-element.7) | copy-start | bytes 786436
  121.1 2.0 %copy-start.2 = (f32[64,2048]{1,0:T(8,128)S(1)}, f32[64,2048]{1,0:T(8,128)}, u32[]{:S(2)}) copy-start(f32[64,2048]{1,0:T(8,128)} %get-tuple-element.24) | copy-start | bytes 1572868

commit v4 on v3

--- a/solution.py
+++ b/solution.py
@@ -2,6 +2,7 @@
 
 import jax
 import jax.numpy as jnp
+import numpy as np
 from jax import lax
 from jax.experimental import pallas as pl
 from jax.experimental.pallas import tpu as pltpu
@@ -84,8 +85,8 @@
         return pltpu.make_async_remote_copy(
             src_ref=self.block(to),
             dst_ref=self.dst.at[slot],
-            send_sem=self.send.at[k],
-            recv_sem=self.recv.at[k],
+            send_sem=self.send.at[0],
+            recv_sem=self.recv.at[0],
             device_id=coords_of(to, self.axes),
             device_id_type=MESH,
         )
@@ -98,19 +99,25 @@
         lax.fori_loop(1, self.n, one, 0)
         self.dst[self.me] = self.block(self.me)[...]
 
+    def others(self):
+        return bulk(self.dst.at[pl.ds(0, self.n - 1)], self.send, self.recv)
+
     def arrive(self):
-        def one(k, carry):
-            self.copy(k, lax.rem(self.me + self.n - k, self.n)).wait_recv()
-            return carry
-
-        lax.fori_loop(1, self.n, one, 0)
+        self.others().wait_recv()
 
     def drain(self):
-        def one(k, carry):
-            self.copy(k, self.me).wait_send()
-            return carry
-
-        lax.fori_loop(1, self.n, one, 0)
+        self.others().wait_send()
+
+
+def bulk(ref, send, recv):
+    return pltpu.make_async_remote_copy(
+        src_ref=ref,
+        dst_ref=ref,
+        send_sem=send.at[0],
+        recv_sem=recv.at[0],
+        device_id={"c": 1 - lax.axis_index("c")},
+        device_id_type=MESH,
+    )
 
 
 class ToReaders:
@@ -222,8 +229,9 @@
 
 
 class RingGather:
-    def __init__(self, axis, piece, count, send, recv):
+    def __init__(self, axis, piece, count, three, send, recv):
         self.axis, self.piece, self.count, self.send, self.recv = axis, piece, count, send, recv
+        self.three = three
         self.me = lax.axis_index(axis)
 
     def at(self, offset):
@@ -234,7 +242,7 @@
         return pltpu.make_async_remote_copy(
             src_ref=ref,
             dst_ref=ref,
-            send_sem=self.send.at[kind, p],
+            send_sem=self.send.at[0],
             recv_sem=self.recv.at[kind, p],
             device_id={self.axis: self.at(sign)},
             device_id_type=MESH,
@@ -256,9 +264,7 @@
         self.copy(self.at(2), p, 1, 2).wait_recv()
 
     def drain(self):
-        for p in range(self.count):
-            for kind in range(3):
-                self.copy(self.me, p, 1, kind).wait_send()
+        bulk(self.three, self.send, self.send).wait_send()
 
 
 class RowGather:
@@ -344,8 +350,8 @@
         return pltpu.make_async_remote_copy(
             src_ref=self.parts[i].at[:, self.lanes(to)],
             dst_ref=self.out.at[self.x, slot_y, i],
-            send_sem=self.send.at[k, i],
-            recv_sem=self.recv.at[k, i],
+            send_sem=self.send.at[0],
+            recv_sem=self.recv.at[0],
             device_id={"y": to},
             device_id_type=MESH,
         )
@@ -357,15 +363,14 @@
         for i in range(2):
             self.out[self.x, self.y, i] = self.parts[i][:, self.lanes(self.y)]
 
+    def others(self):
+        return bulk(self.out.at[self.x, pl.ds(0, 3)], self.send, self.recv)
+
     def arrive(self):
-        for k in range(1, 4):
-            for i in range(2):
-                self.copy(k, i, lax.rem(self.y + 4 - k, 4)).wait_recv()
+        self.others().wait_recv()
 
     def drain(self):
-        for k in range(1, 4):
-            for i in range(2):
-                self.copy(k, i, self.y).wait_send()
+        self.others().wait_send()
 
 
 def unit_rows(matrix, gain):
@@ -378,57 +383,116 @@
     return pltpu.roll(a, HD, 1)
 
 
-class RingSum:
+class StrideGather:
+    def __init__(self, nz, blocks, send, recv):
+        self.nz, self.blocks, self.send, self.recv = nz, blocks, send, recv
+        self.z = lax.axis_index("z")
+        self.rows = blocks.shape[1] // PIECES
+        self.far = {1: nz // 2, -1: nz - 1 - nz // 2}
+
+    def at(self, offset):
+        return lax.rem(self.z + offset + self.nz, self.nz)
+
+    def copy(self, sign, distance, d, p):
+        ref = self.blocks.at[self.at(-sign * distance), pl.ds(p * self.rows, self.rows)]
+        return pltpu.make_async_remote_copy(
+            src_ref=ref,
+            dst_ref=ref,
+            send_sem=self.send.at[0],
+            recv_sem=self.recv.at[0 if sign > 0 else 1, distance + d - 1, p],
+            device_id={"z": self.at(sign * d)},
+            device_id_type=MESH,
+        )
+
+    def arrived(self, sign, distance, p):
+        ref = self.blocks.at[self.at(-sign * distance), pl.ds(p * self.rows, self.rows)]
+        return pltpu.make_async_remote_copy(
+            src_ref=ref,
+            dst_ref=ref,
+            send_sem=self.send.at[0],
+            recv_sem=self.recv.at[0 if sign > 0 else 1, distance - 1, p],
+            device_id={"z": self.at(sign)},
+            device_id_type=MESH,
+        )
+
+    def start(self):
+        for d in (2, 1):
+            for p in range(PIECES):
+                for sign in (1, -1):
+                    self.copy(sign, 0, d, p).start()
+
+    def relay(self, distance):
+        for p in range(PIECES):
+            for sign in (1, -1):
+                if distance <= self.far[sign]:
+                    self.arrived(sign, distance, p).wait_recv()
+                if distance + 2 <= self.far[sign]:
+                    self.copy(sign, distance, 2, p).start()
+        for p in range(PIECES):
+            for sign in (1, -1):
+                if distance + 1 <= self.far[sign]:
+                    self.copy(sign, distance, 1, p).start()
+
+    def arrive(self, distance):
+        for sign in (1, -1):
+            if distance <= self.far[sign]:
+                for p in range(PIECES):
+                    self.arrived(sign, distance, p).wait_recv()
+
+    def drain(self):
+        bulk(self.blocks.at[pl.ds(0, self.nz - 1)], self.send, self.send).wait_send()
+
+
+class StrideSum:
     def __init__(self, nz, term, out, arrived, send, recv, pieces):
         self.nz, self.term, self.out, self.arrived = nz, term, out, arrived
         self.send, self.recv, self.pieces = send, recv, pieces
         self.rows = out.shape[2] // pieces
-        self.last = (nz // 2 - 1, nz // 2 - 2)
-        z = lax.axis_index("z")
-        self.to = (lax.rem(z + nz - 1, nz), lax.rem(z + 1, nz))
-
-    def hop(self, side, s, p):
+        self.z = lax.axis_index("z")
+
+    def chained(self, side, j):
+        return (j + side) % 2 == 0
+
+    def hop(self, side, j, p):
         at = pl.ds(p * self.rows, self.rows)
-        return pltpu.make_async_remote_copy(
-            src_ref=self.out.at[side, s, at],
-            dst_ref=self.arrived.at[side, s, at],
-            send_sem=self.send.at[side, s, p],
-            recv_sem=self.recv.at[side, s, p],
-            device_id={"z": self.to[side]},
-            device_id_type=MESH,
-        )
-
-    def first(self, side):
-        self.out[side, 0] = self.term(side, 0, pl.ds(0, self.rows * self.pieces)).astype(BF16)
-        for p in range(self.pieces):
-            self.hop(side, 0, p).start()
-
-    def step(self, s, side):
+        d = (2 if self.chained(side, j) else 1) * (1 if side else -1)
+        return pltpu.make_async_remote_copy(
+            src_ref=self.out.at[side, j, at],
+            dst_ref=self.arrived.at[side, j, at],
+            send_sem=self.send.at[side],
+            recv_sem=self.recv.at[side, j, p],
+            device_id={"z": lax.rem(self.z + d + self.nz, self.nz)},
+            device_id_type=MESH,
+        )
+
+    def joined(self, side, j, p, value):
+        at = pl.ds(p * self.rows, self.rows)
+        for i in (j - 1, j - 2):
+            if i >= 0:
+                self.hop(side, i, p).wait_recv()
+                value = value + self.arrived[side, i, at].astype(F32)
+        return value
+
+    def step(self, side, j):
         for p in range(self.pieces):
             at = pl.ds(p * self.rows, self.rows)
-            self.hop(side, s - 1, p).wait_recv()
-            value = self.arrived[side, s - 1, at].astype(F32) + self.term(side, s, at)
-            self.out[side, s, at] = value.astype(BF16)
-            self.hop(side, s, p).start()
+            value = self.term(side, j, at)
+            if self.chained(side, j):
+                value = self.joined(side, j, p, value)
+            self.out[side, j, at] = value.astype(BF16)
+            self.hop(side, j, p).start()
 
     def total(self, p):
+        half = self.nz // 2
         at = pl.ds(p * self.rows, self.rows)
-        value = self.term(1, self.nz // 2 - 1, at)
-        for side in (1, 0):
-            self.hop(side, self.last[side], p).wait_recv()
-            value = value + self.arrived[side, self.last[side], at].astype(F32)
-        return value
+        value = self.joined(1, half - 1, p, self.term(1, half - 1, at))
+        return self.joined(0, half, p, value)
 
     def drain(self):
-        def one(s, carry):
-            for p in range(self.pieces):
-                self.hop(0, s, p).wait_send()
-                self.hop(1, s, p).wait_send()
-            return carry
-
-        lax.fori_loop(0, self.last[1] + 1, one, 0)
-        for p in range(self.pieces):
-            self.hop(0, self.last[0], p).wait_send()
+        half = self.nz // 2
+        for side in range(2):
+            sem = self.send.at[pl.ds(side, 1)]
+            bulk(self.out.at[side, pl.ds(0, half - side)], sem, sem).wait_send()
 
 
 class FarGather:
@@ -441,15 +505,18 @@
         return lax.rem(self.z + offset + self.nz, self.nz)
 
     def copy(self, slot, sign, d, relay):
-        i, j = (2 if relay else 0) + (0 if sign > 0 else 1), d - 1
+        kind = 3 if relay else 2 if d < REACH else 0 if sign > 0 else 1
         return pltpu.make_async_remote_copy(
             src_ref=self.dst.at[slot] if relay else self.src,
             dst_ref=self.dst.at[slot],
-            send_sem=self.send.at[i, j],
-            recv_sem=self.recv.at[i, j],
+            send_sem=self.send.at[0],
+            recv_sem=self.recv.at[kind],
             device_id={"z": self.at(sign * d)},
             device_id_type=MESH,
         )
+
+    def several(self, count, kind):
+        return bulk(self.dst.at[pl.ds(0, count)], self.send, self.recv.at[pl.ds(kind, 1)])
 
     def start(self):
         for d in range(REACH, 0, -1):
@@ -465,18 +532,11 @@
                 self.copy(slot, sign, d, True).start()
 
     def arrive(self):
-        for sign in (1, -1):
-            for d in range(1, REACH):
-                self.copy(self.at(-sign * d), sign, d, False).wait_recv()
-            for d in range(1, self.far[sign] + 1):
-                self.copy(self.at(-sign * (REACH + d)), sign, d, True).wait_recv()
+        self.several(2 * REACH - 2, 2).wait_recv()
+        self.several(self.nz - 1 - 2 * REACH, 3).wait_recv()
 
     def drain(self):
-        for sign in (1, -1):
-            for d in range(1, REACH + 1):
-                self.copy(self.z, sign, d, False).wait_send()
-            for d in range(1, self.far[sign] + 1):
-                self.copy(self.z, sign, d, True).wait_send()
+        self.several(self.nz - 1, 0).wait_send()
 
 
 def reach_greet(nz):
@@ -496,20 +556,27 @@
     return pltpu.SemaphoreType.DMA(shape)
 
 
+def norm_back(matrix, gain, upstream):
+    wide = matrix.astype(F32)
+    factor = lax.rsqrt(jnp.mean(wide * wide, axis=-1, keepdims=True) + EPSILON)
+    weighted = upstream * gain
+    inner = jnp.mean(weighted * wide, axis=-1, keepdims=True)
+    return factor * weighted - wide * factor**3 * inner
+
+
 def kernel(
-    nz, target_rows, source_rows, t_gain, s_gain, pair, wk, wv, cot, pick, pick8,
+    nz, target_rows, source_rows, t_gain, s_gain, wq, wk, wv, wo, cot, pick, pick8,
     s_out, t_out, w_out,
-    kv_all, stats, out, qa, t_all, pair_all, w_all,
+    pair, kv_all, stats, out, qa, t_all, pair_all, w_all,
     halves, rows_all, part, part_all, block, blocks, m, l, o, said, heard,
     dq, mine, ring_out, ring_in, w_ring_out, w_ring_in, outs, dq_block, dqs, o_part, swapped,
-    mine_sum, all_sums, kv_grad, grads2, parts, d_parts, s_in, t_in,
-    row_s, row_r, wy_s, wy_r, wx_s, wx_r, ty_s, ty_r, tx_s, tx_r, pair_s, pair_r,
-    part_s, part_r, q_s, q_r, rs, rr, ls, lr, ss, sr,
+    mine_sum, all_sums, upstream_s, kv_grad, grads2, parts, d_parts, s_in, t_in,
+    row_s, row_r, wy_s, wy_r, wx_s, wx_r, ya_s, ya_r, xb_s, xb_r, xa_s, xa_r, yb_s, yb_r, pair_s, pair_r,
+    part_s, part_r, q_s, q_r, z_s, z_r, ss, sr,
     o_s, o_r, dq_s, dq_r, sw_s, sw_r, g_s, g_r, h_s, h_r, back_s, back_r,
     kv_s, kv_r, s_s, s_r, t_s, t_r,
 ):
     z, y, x, c = (lax.axis_index(a) for a in "zyxc")
-    right, left = lax.rem(z + 1, nz), lax.rem(z + nz - 1, nz)
     met = greet(("y", "x", "c")) + reach_greet(nz)
 
     normed = unit_rows(source_rows[...], s_gain[...])
@@ -519,13 +586,28 @@
         first, second = (normed[:, 128 * i : 128 * i + 128] for i in (chip, chip + 4))
         halves[0, :, 128 * j : 128 * j + 128] = jnp.where(low, first, swap_halves(second)).astype(BF16)
         halves[1, :, 128 * j : 128 * j + 128] = jnp.where(low, swap_halves(first), second).astype(BF16)
+    pair[:HD] = jnp.transpose(wq[...].astype(F32)).astype(BF16)
+    pair[HD:] = wo[...]
     greeted(met)
 
     by_rows = RowGather(halves, rows_all, row_s, row_r)
     by_wy = WeightColumn(wk, wv, w_all, wy_s, wy_r)
-    by_wx = RingGather("x", lambda slot, p: w_all.at[slot, p], 4, wx_s, wx_r)
-    by_ty = RingGather("y", lambda slot, p: t_all.at[x, slot, :, pl.ds(1024 * p, 1024)], 2, ty_s, ty_r)
-    by_tx = RingGather("x", lambda slot, p: t_all.at[slot, p], 4, tx_s, tx_r)
+    by_wx = RingGather("x", lambda slot, p: w_all.at[slot, p], 4, w_all.at[pl.ds(0, 3)], wx_s, wx_r)
+    three, first, second = pl.ds(0, 3), pl.ds(0, 1024), pl.ds(1024, 1024)
+    by_ya = RingGather(
+        "y", lambda slot, p: t_all.at[x, slot, :, pl.ds(512 * p, 512)], 2,
+        t_all.at[x, three, :, first], ya_s, ya_r,
+    )
+    by_xb = RingGather(
+        "x", lambda slot, p: t_all.at[slot, y, :, pl.ds(1024 + 512 * p, 512)], 2,
+        t_all.at[three, y, :, second], xb_s, xb_r,
+    )
+    by_xa = RingGather(
+        "x", lambda slot, p: t_all.at[slot, p, :, first], 4, t_all.at[three, :, :, first], xa_s, xa_r
+    )
+    by_yb = RingGather(
+        "y", lambda slot, p: t_all.at[p, slot, :, second], 4, t_all.at[:, three, :, second], yb_s, yb_r
+    )
     by_pair = Exchange(("c",), pair, pair_all, pair_s, pair_r)
     by_wy.start()
     by_rows.start()
@@ -534,21 +616,19 @@
         [unit_rows(target_rows[...], t_gain[...]), zero, cot[...].astype(F32), zero], axis=0
     ).astype(BF16)
     for p in range(2):
-        by_ty.start(p)
+        by_xb.start(p)
+        by_ya.start(p)
     by_pair.start()
 
     by_wy.arrive()
     for p in range(4):
         by_wx.start(p)
     by_rows.relay()
-    for p in range(2):
-        by_ty.relay(p)
     for p in range(4):
         by_wx.relay(p)
     for p in range(2):
-        by_ty.arrive(p)
-    for p in range(4):
-        by_tx.start(p)
+        by_xb.relay(p)
+        by_ya.relay(p)
     by_rows.arrive()
     for p in range(4):
         by_wx.arrive(p)
@@ -561,46 +641,25 @@
     part[1] = jnp.where(wide_low, swap_halves(k2), v2)
     by_part = Exchange(("c",), part, part_all, part_s, part_r, lambda at, i: i)
     by_part.start()
+    for p in range(2):
+        by_xb.arrive(p)
+        by_ya.arrive(p)
+    for p in range(4):
+        by_xa.start(p)
+        by_yb.start(p)
     by_part.arrive()
     kv_all[z] = (part_all[0] + part_all[1]).astype(BF16)
 
-    steps_r = nz // 2
-    steps_l = nz - 1 - steps_r
-    piece = 256 // PIECES
-
-    def hop(step, p, sign, ahead=0):
-        at = lax.rem(z + 2 * nz - sign * (step + ahead), nz)
-        ssem, rsem = (rs, rr) if sign > 0 else (ls, lr)
-        ref = kv_all.at[at, pl.ds(p * piece, piece)]
-        return pltpu.make_async_remote_copy(
-            src_ref=ref,
-            dst_ref=ref,
-            send_sem=ssem.at[step, p],
-            recv_sem=rsem.at[step, p],
-            device_id={"z": right if sign > 0 else left},
-            device_id_type=MESH,
-        )
-
-    for p in range(PIECES):
-        hop(0, p, 1).start()
-        hop(0, p, -1).start()
-
-    def pass_on(s):
-        for p in range(PIECES):
-            hop(s - 1, p, 1, 1).wait_recv()
-            hop(s, p, 1).start()
-            hop(s - 1, p, -1, 1).wait_recv()
-
-            @pl.when(s < steps_l)
-            def _():
-                hop(s, p, -1).start()
-
+    by_z = StrideGather(nz, kv_all, z_s, z_r)
+    by_z.start()
     for p in range(4):
-        by_tx.relay(p)
-    pass_on(jnp.int32(1))
+        by_xa.relay(p)
+        by_yb.relay(p)
+    by_z.relay(2)
     by_pair.arrive()
     for p in range(4):
-        by_tx.arrive(p)
+        by_xa.arrive(p)
+        by_yb.arrive(p)
     everything = t_all[...].reshape(256, 2048)
     scale = jnp.where(lanes_below((256, 128), HD), HD**-0.5, 1.0)
     for a in range(2):
@@ -611,7 +670,7 @@
         ).astype(BF16)
     by_q = ToReaders(block, blocks, q_s, q_r)
     by_q.start()
-    pass_on(jnp.int32(2))
+    by_z.relay(4)
     m[...] = jnp.full(m.shape, -1e30, F32)
     l[...] = jnp.zeros(l.shape, F32)
     o[...] = jnp.zeros(o.shape, F32)
@@ -629,23 +688,25 @@
         l[...] = l[...] * old + jnp.sum(weights, axis=0, keepdims=True)
         o[...] = o[...] * old + contract(block, weights.astype(BF16), 0, 0)[HD:]
 
-    def attend_both(d):
-        attend(lax.rem(z + nz - d, nz))
-        attend(lax.rem(z + d, nz))
+    def attend_from(low, high):
+        def one(i, carry):
+            d = low + i // 2
+            attend(lax.rem(z + nz + jnp.where(lax.rem(i, 2) == 0, d, -d), nz))
+            return carry
+
+        lax.fori_loop(0, 2 * (high - low + 1), one, 0)
 
     attend(z)
-    attend_both(1)
-
-    def step(s, carry):
-        pass_on(s)
-        attend_both(s - 1)
-        return carry
-
-    lax.fori_loop(3, steps_r, step, 0)
-    attend_both(steps_r - 1)
-    for p in range(PIECES):
-        hop(steps_r - 1, p, 1, 1).wait_recv()
-    attend(lax.rem(z + nz - steps_r, nz))
+    by_z.arrive(1)
+    attend_from(1, 2)
+    by_z.relay(6)
+    by_z.arrive(3)
+    by_z.arrive(5)
+    attend_from(3, 6)
+    by_z.arrive(7)
+    attend_from(7, 7)
+    by_z.arrive(8)
+    attend(lax.rem(z + nz // 2, nz))
     upright = jnp.transpose(qa[...].astype(F32))
     delta = jnp.sum(upright[HD:] * o[...], axis=0, keepdims=True)
     row = lax.broadcasted_iota(jnp.int32, (8, qa.shape[0]), 0)
@@ -669,8 +730,12 @@
     by_o.start()
     dq[...] = jnp.zeros(dq.shape, F32)
 
+    def plane_of(side, j):
+        offset = jnp.where(side == 0, j - nz // 2, nz // 2 - 1 - j)
+        return lax.rem(z + nz + offset, nz)
+
     def grads(side, j):
-        at = lax.rem(z + nz - nz // 2 + j, nz) if side == 0 else lax.rem(z + nz // 2 - 1 - j, nz)
+        at = plane_of(side, j)
         block = kv_all[at]
         low = lanes_below(block.shape, HD)
         none = jnp.zeros_like(block)
@@ -683,19 +748,30 @@
         dq[...] += contract(block, d_scores, 0, 0)[:HD]
         mine[side, j] = jnp.where(lanes_below(for_k.shape, HD), for_k, for_v)
 
-    main = RingSum(nz, lambda side, j, at: mine[side, j, at], ring_out, ring_in, g_s, g_r, PIECES)
+    def both_grads(low, high):
+        def one(i, carry):
+            side = lax.rem(i, 2)
+            grads(side, low + i // 2 - side)
+            return carry
+
+        lax.fori_loop(0, 2 * (high - low + 1), one, 0)
+
+    main = StrideSum(nz, lambda side, j, at: mine[side, j, at], ring_out, ring_in, g_s, g_r, PIECES)
 
     def own_weight(side, j, at):
-        to = lax.rem(z + nz - nz // 2 + j, nz) if side == 0 else lax.rem(z + nz // 2 - 1 - j, nz)
+        to = plane_of(side, j)
         return swapped[0, to, at].astype(F32) + swapped[1, to, at].astype(F32)
 
-    weight = RingSum(nz, own_weight, w_ring_out, w_ring_in, h_s, h_r, 1)
-    for side in range(2):
-        grads(side, 0)
-        main.first(side)
-    for side in range(2):
-        grads(side, 1)
-
+    weight = StrideSum(nz, own_weight, w_ring_out, w_ring_in, h_s, h_r, 1)
+
+    def two(ring, j):
+        ring.step(0, j)
+        ring.step(1, j - 1)
+
+    grads(jnp.int32(0), jnp.int32(0))
+    main.step(0, 0)
+    both_grads(1, 1)
+    two(main, 1)
     by_o.arrive()
     attended = jnp.sum(outs[...].astype(F32), axis=0).astype(BF16)
     for a in range(2):
@@ -705,61 +781,41 @@
             o_part[a, i] = product[:, 128 * i : 128 * i + 128]
     swap = Exchange(("c",), o_part, swapped, sw_s, sw_r, lambda at, i: i)
     swap.start()
-    for side in range(2):
-        main.step(1, side)
-    for side in range(2):
-        grads(side, 2)
-        grads(side, 3)
+    both_grads(2, 3)
+    two(main, 3)
+    two(main, 2)
     swap.arrive()
-    for side in range(2):
-        weight.first(side)
-
-    def ahead(s, carry):
-        for side in range(2):
-            main.step(s, side)
-        for side in range(2):
-            weight.step(s - 1, side)
-        for side in range(2):
-            grads(side, 2 * s)
-            grads(side, 2 * s + 1)
-        return carry
-
-    lax.fori_loop(2, nz // 4, ahead, 0)
+    weight.step(0, 0)
+    for j in range(1, nz // 2, 2):
+        two(weight, j)
+    both_grads(4, 5)
+    two(main, 5)
+    two(main, 4)
+    both_grads(6, 7)
+    two(main, 7)
+    two(weight, 2)
+    grads(jnp.int32(1), jnp.int32(7))
     upright = jnp.concatenate([dq[...], jnp.zeros_like(dq[...])], axis=0) * HD**-0.5
     dq_block[...] = jnp.transpose(upright).astype(BF16).reshape(4, 192, 128)
     by_dq = ToOwners(dq_block, dqs, dq_s, dq_r)
     by_dq.start()
+    two(main, 6)
+    two(weight, 4)
+    by_dq.arrive()
+    query_grad = jnp.sum(dqs[...].astype(F32), axis=0).astype(BF16)
+    d_target = jnp.zeros((128, 2048), F32)
+    for a in range(2):
+        spread = contract(pick8[...], query_grad[96 * a : 96 * a + 96], 0, 0).astype(BF16)
+        d_target = d_target + jnp.dot(spread, pair_all[a], preferred_element_type=F32)
+    d_parts[...] = d_target.astype(BF16).reshape(16, 8, 2048)
     by_t = Exchange(("x", "y"), d_parts, t_in, t_s, t_r, lambda at, i: i)
-
-    def behind(s, carry):
-        main.step(s, 0)
-
-        @pl.when(s < nz // 2 - 1)
-        def _():
-            main.step(s, 1)
-
-        for side in range(2):
-            weight.step(s - 1, side)
-
-        @pl.when(s == nz // 4)
-        def _():
-            by_dq.arrive()
-            query_grad = jnp.sum(dqs[...].astype(F32), axis=0).astype(BF16)
-            d_target = jnp.zeros((128, 2048), F32)
-            for a in range(2):
-                spread = contract(pick8[...], query_grad[96 * a : 96 * a + 96], 0, 0).astype(BF16)
-                d_target = d_target + jnp.dot(spread, pair_all[a], preferred_element_type=F32)
-            d_parts[...] = d_target.astype(BF16).reshape(16, 8, 2048)
-            by_t.start()
-
-        return carry
-
-    lax.fori_loop(nz // 4, nz // 2, behind, 0)
-    weight.step(nz // 2 - 1, 0)
+    by_t.start()
+    piece = 256 // PIECES
     for p in range(PIECES):
         kv_grad[pl.ds(p * piece, piece)] = main.total(p).astype(BF16)
     by_kv = Exchange(("c",), kv_grad, grads2, kv_s, kv_r)
     by_kv.start()
+    two(weight, 6)
     by_kv.arrive()
     g0, g1 = grads2[0].astype(F32), grads2[1].astype(F32)
     k2 = jnp.where(wide_low, g0, swap_halves(g1)).astype(BF16)
@@ -773,7 +829,8 @@
     back = FarGather(nz, mine_sum, all_sums, back_s, back_r)
     back.start()
     by_t.arrive()
-    t_out[...] = jnp.sum(t_in[...].astype(F32), axis=0)
+    upstream = jnp.sum(t_in[...].astype(F32), axis=0)[:6]
+    t_out[...] = cot[...].astype(F32) + norm_back(target_rows[...], t_gain[...], upstream)
     back.relay()
     by_s.arrive()
     got = []
@@ -785,33 +842,21 @@
     for j in range(8):
         chip = (2 * j % 4) * 4 + j // 2
         a, b = (g[:, 128 * j : 128 * j + 128] for g in got)
-        s_out[:, 128 * chip : 128 * chip + 128] = jnp.where(low, a, swap_halves(b))
-        s_out[:, 128 * chip + 512 : 128 * chip + 640] = jnp.where(low, swap_halves(a), b)
+        upstream_s[:, 128 * chip : 128 * chip + 128] = jnp.where(low, a, swap_halves(b))
+        upstream_s[:, 128 * chip + 512 : 128 * chip + 640] = jnp.where(low, swap_halves(a), b)
+    s_out[...] = norm_back(source_rows[...], s_gain[...], upstream_s[...])
     back.arrive()
     for i in range(nz):
         w_out[:, 128 * i : 128 * i + 128] = all_sums[i].astype(F32)
-    for by in (by_stats, by_o, by_dq, swap, back, by_kv, by_s, by_t, main, weight):
+    for by in (by_rows, by_wy, by_wx, by_ya, by_xb, by_xa, by_yb, by_pair, by_part, by_q, by_z, by_stats):
         by.drain()
-    for by in (by_rows, by_wy, by_wx, by_ty, by_tx, by_pair, by_part, by_q):
+    for by in (by_o, by_dq, swap, back, by_kv, by_s, by_t, main, weight):
         by.drain()
-
-    def drain_gather(s, carry):
-        for p in range(PIECES):
-            hop(s, p, 1).wait_send()
-
-            @pl.when(s < steps_l)
-            def _():
-                hop(s, p, -1).wait_send()
-
-        return carry
-
-    lax.fori_loop(0, steps_r, drain_gather, 0)
 
 
 def whole(args, nz):
     t = 768
     half = nz // 2
-    ring = sems(half, PIECES)
 
     def bf16(*shape):
         return pltpu.VMEM(shape, BF16)
@@ -823,13 +868,13 @@
         functools.partial(kernel, nz),
         out_shape=(
             jax.ShapeDtypeStruct((32, 2048), F32),
-            jax.ShapeDtypeStruct((8, 2048), F32),
+            jax.ShapeDtypeStruct((6, 2048), F32),
             jax.ShapeDtypeStruct((64, 2048), F32),
         ),
         in_specs=[VMEM] * len(args),
         out_specs=(VMEM,) * 3,
         scratch_shapes=[
-            bf16(nz, 256, 128), f32(8, t), bf16(4, 192, 128), bf16(t, 128),
+            bf16(128, 2048), bf16(nz, 256, 128), f32(8, t), bf16(4, 192, 128), bf16(t, 128),
             bf16(4, 4, 16, 2048), bf16(2, 128, 2048), bf16(4, 4, 2, 64, 128),
             bf16(2, 32, 1024), bf16(4, 2, 32, 1024), f32(2, 256, 128), f32(2, 256, 128),
             bf16(192, 128), bf16(4, 192, 128), f32(1, t), f32(1, t), f32(HD, t), f32(8, t), f32(4, 8, t),
@@ -837,44 +882,30 @@
             bf16(2, half, HD, 128), bf16(2, half, HD, 128),
             bf16(4, 192, 128), bf16(4, 192, 128), bf16(4, 192, 128),
             bf16(2, nz, HD, 128), bf16(2, nz, HD, 128), bf16(HD, 128), bf16(nz, HD, 128),
-            bf16(256, 128), bf16(2, 256, 128), bf16(8, 32, 1024), bf16(16, 8, 2048),
+            f32(32, 2048), bf16(256, 128), bf16(2, 256, 128), bf16(8, 32, 1024), bf16(16, 8, 2048),
             bf16(8, 32, 1024), bf16(16, 8, 2048),
-            sems(5, 2), sems(5, 2), sems(4, 2), sems(4, 2), sems(3, 4), sems(3, 4),
-            sems(3, 2), sems(3, 2), sems(3, 4), sems(3, 4), dma(2), dma(2),
-            dma(2), dma(2), dma(4), dma(4), ring, ring, ring, ring, dma(4), dma(4),
-            dma(4), dma(4), dma(4), dma(4), dma(2), dma(2),
-            sems(2, half, PIECES), sems(2, half, PIECES), sems(2, half, 1), sems(2, half, 1),
-            sems(4, REACH), sems(4, REACH),
-            dma(2), dma(2), dma(8), dma(8), dma(16), dma(16),
+            sems(5, 2), sems(5, 2), dma(1), dma(1), dma(1), sems(3, 4),
+            dma(1), sems(3, 2), dma(1), sems(3, 2), dma(1), sems(3, 4), dma(1), sems(3, 4), dma(1), dma(1),
+            dma(1), dma(1), dma(4), dma(4), dma(1), sems(2, half, PIECES), dma(1), dma(1),
+            dma(4), dma(4), dma(4), dma(4), dma(1), dma(1),
+            dma(2), sems(2, half, PIECES), dma(2), sems(2, half, 1),
+            dma(1), dma(4), dma(1), dma(1), dma(1), dma(1), dma(1), dma(1),
         ],
         compiler_params=params(0),
     )(*args)
 
 
-def norm_back(matrix, gain, upstream):
-    wide = matrix.astype(F32)
-    factor = lax.rsqrt(jnp.mean(wide * wide, axis=-1, keepdims=True) + EPSILON)
-    weighted = upstream * gain
-    inner = jnp.mean(weighted * wide, axis=-1, keepdims=True)
-    return factor * weighted - wide * factor**3 * inner
-
-
 def picks():
-    r = jnp.arange(96)
+    r = np.arange(96)
     at = 16 * (r // 6) + r % 6
-    pick = jnp.concatenate([at, at + 8])[:, None] == jnp.arange(256)[None]
-    pick8 = (8 * (r // 6) + r % 6)[:, None] == jnp.arange(128)[None]
-    return pick.astype(BF16), pick8.astype(BF16)
+    pick = np.concatenate([at, at + 8])[:, None] == np.arange(256)[None]
+    pick8 = (8 * (r // 6) + r % 6)[:, None] == np.arange(128)[None]
+    return jnp.asarray(pick.astype(BF16)), jnp.asarray(pick8.astype(BF16))
 
 
 def body(nz, target_rows, source_rows, t_gain, s_gain, wq, wk, wv, wo, cot):
-    pick, pick8 = picks()
-    pair = jnp.concatenate([wq.T, wo])
-    d_source, d_target, o_grad = whole(
-        (target_rows, source_rows, t_gain[None], s_gain[None], pair, wk, wv, cot, pick, pick8), nz
-    )
-    source_grad = norm_back(source_rows, s_gain, d_source)
-    target_grad = cot.astype(F32) + norm_back(target_rows, t_gain, d_target[:6])
+    args = (target_rows, source_rows, t_gain[None], s_gain[None], wq, wk, wv, wo, cot, *picks())
+    source_grad, target_grad, o_grad = whole(args, nz)
     return target_grad, source_grad, o_grad
 
 

time: 126 us -> 110 us (0.87)
  the two profiles are of different devices: /device:TPU:1 before, /device:TPU:8 now
where the time goes in v4:
time: 110 us
  Pallas kernels  103 us (94%)
  local copies, waits for them, and re-layouts  5.95 us (5%)
    pallas_call x1, Pallas kernels, whole(): pl.pallas_call(functools.partial(kernel, nz), out_shape=(jax.ShapeDtypeSt...  103 us
    unnamed x6, local copies, waits for them, and re-layouts  5.95 us

profile of v4, /device:TPU:8, one launch (start us, length us, event | category | flops | bytes accessed | tf_op | source)
XLA Modules:
  0.0 109.6 jit_solution(2123034760545186755)
XLA Ops:
  0.6 2.0 %copy.14.wq = bf16[2048,64]{1,0:T(8,128)(2,1)} copy(bf16[2048,64]{0,1:T(8,128)(2,1)} %param.15) | data formatting | bytes 524288 | tf_op args[4]
  2.6 103.0 %shard_map.130 = (f32[32,2048]{1,0:T(8,128)}, f32[6,2048]{1,0:T(8,128)}, f32[64,2048]{1,0:T(8,128)}) custom-call(bf16[6,2048]{1,0:T(8,128)(2,1)} %target_rows.1, bf16[32,2048]{1,0:T(8,128)(2,1)} %source_rows.1, f32[1,2048]{1,0:T(1,128)} %bitcast.2, f32[1,2048]{1,0:T(1,128)} %bitcast.3, bf16[2048,64]{1,0:T(8,128)(2,1)} %copy.14.wq, bf16[64,512]{1,0:T(8,128)(2,1)} %wk.1, ...), custom_call_target="tpu_custom_call" | custom-call | tf_op jit(solution)/shard_map/pallas_call | solution.py:867
  105.6 0.0 copy-start
  105.6 1.5 %copy.18 = f32[6,2048]{1,0:T(8,128)} copy(f32[6,2048]{1,0:T(8,128)} %get-tuple-element.12) | data formatting | bytes 98304
  107.2 1.7 %copy.19 = f32[32,2048]{1,0:T(8,128)} copy(f32[32,2048]{1,0:T(8,128)} %get-tuple-element.13) | data formatting | bytes 524288
  108.8 0.0 copy-done
  108.8 0.8 copy.20
Async XLA Ops:
  105.6 3.2 %copy-start = (f32[64,2048]{1,0:T(8,128)S(1)}, f32[64,2048]{1,0:T(8,128)}, u32[]{:S(2)}) copy-start(f32[64,2048]{1,0:T(8,128)} %get-tuple-element.14) | copy-start | bytes 1572868

commit v5 on v4

--- a/solution.py
+++ b/solution.py
@@ -565,12 +565,13 @@
 
 
 def kernel(
-    nz, target_rows, source_rows, t_gain, s_gain, wq, wk, wv, wo, cot, pick, pick8,
-    s_out, t_out, w_out,
+    nz, target_rows_h, source_rows_h, t_gain_h, s_gain_h, wq_h, wk_h, wv_h, wo_h, cot_h, pick_h, pick8_h,
+    s_out, t_out, all_sums,
+    target_rows, source_rows, t_gain, s_gain, wk, wv, cot, pick, pick8, loads,
     pair, kv_all, stats, out, qa, t_all, pair_all, w_all,
     halves, rows_all, part, part_all, block, blocks, m, l, o, said, heard,
     dq, mine, ring_out, ring_in, w_ring_out, w_ring_in, outs, dq_block, dqs, o_part, swapped,
-    mine_sum, all_sums, upstream_s, kv_grad, grads2, parts, d_parts, s_in, t_in,
+    mine_sum, kv_grad, grads2, parts, d_parts, s_in, t_in,
     row_s, row_r, wy_s, wy_r, wx_s, wx_r, ya_s, ya_r, xb_s, xb_r, xa_s, xa_r, yb_s, yb_r, pair_s, pair_r,
     part_s, part_r, q_s, q_r, z_s, z_r, ss, sr,
     o_s, o_r, dq_s, dq_r, sw_s, sw_r, g_s, g_r, h_s, h_r, back_s, back_r,
@@ -579,6 +580,16 @@
     z, y, x, c = (lax.axis_index(a) for a in "zyxc")
     met = greet(("y", "x", "c")) + reach_greet(nz)
 
+    staged = (
+        (source_rows_h, source_rows), (s_gain_h, s_gain), (wk_h, wk), (wv_h, wv),
+        (target_rows_h, target_rows), (t_gain_h, t_gain), (cot_h, cot),
+        (wq_h, pair.at[pl.ds(0, HD)]), (wo_h, pair.at[pl.ds(HD, HD)]), (pick_h, pick), (pick8_h, pick8),
+    )
+    copies = [pltpu.make_async_copy(a, b, loads.at[i]) for i, (a, b) in enumerate(staged)]
+    for copy in copies:
+        copy.start()
+    for copy in copies[:2]:
+        copy.wait()
     normed = unit_rows(source_rows[...], s_gain[...])
     low = lanes_below((32, 128), HD)
     for j in range(8):
@@ -586,8 +597,8 @@
         first, second = (normed[:, 128 * i : 128 * i + 128] for i in (chip, chip + 4))
         halves[0, :, 128 * j : 128 * j + 128] = jnp.where(low, first, swap_halves(second)).astype(BF16)
         halves[1, :, 128 * j : 128 * j + 128] = jnp.where(low, swap_halves(first), second).astype(BF16)
-    pair[:HD] = jnp.transpose(wq[...].astype(F32)).astype(BF16)
-    pair[HD:] = wo[...]
+    for copy in copies[2:]:
+        copy.wait()
     greeted(met)
 
     by_rows = RowGather(halves, rows_all, row_s, row_r)
@@ -629,6 +640,12 @@
     for p in range(2):
         by_xb.relay(p)
         by_ya.relay(p)
+    for p in range(2):
+        by_xb.arrive(p)
+        by_ya.arrive(p)
+    for p in range(4):
+        by_xa.start(p)
+        by_yb.start(p)
     by_rows.arrive()
     for p in range(4):
         by_wx.arrive(p)
@@ -641,12 +658,6 @@
     part[1] = jnp.where(wide_low, swap_halves(k2), v2)
     by_part = Exchange(("c",), part, part_all, part_s, part_r, lambda at, i: i)
     by_part.start()
-    for p in range(2):
-        by_xb.arrive(p)
-        by_ya.arrive(p)
-    for p in range(4):
-        by_xa.start(p)
-        by_yb.start(p)
     by_part.arrive()
     kv_all[z] = (part_all[0] + part_all[1]).astype(BF16)
 
@@ -661,13 +672,14 @@
         by_xa.arrive(p)
         by_yb.arrive(p)
     everything = t_all[...].reshape(256, 2048)
-    scale = jnp.where(lanes_below((256, 128), HD), HD**-0.5, 1.0)
+    wide = lax.broadcasted_iota(jnp.int32, (256, 256), 1)
+    scale = jnp.where(lax.rem(wide, 128) < HD, HD**-0.5, 1.0)
+    projected = contract(everything, pair_all[...].reshape(256, 2048), 1, 1) * scale
+    chosen = jnp.dot(pick[...], projected.astype(BF16), preferred_element_type=F32)
+    narrow = lanes_below((96, 128), HD)
     for a in range(2):
-        both = (contract(everything, pair_all[a], 1, 1) * scale).astype(BF16)
-        chosen = jnp.dot(pick[...], both, preferred_element_type=F32)
-        block[96 * a : 96 * a + 96] = jnp.where(
-            lanes_below((96, 128), HD), chosen[:96], chosen[96:]
-        ).astype(BF16)
+        at = slice(128 * a, 128 * a + 128)
+        block[96 * a : 96 * a + 96] = jnp.where(narrow, chosen[:96, at], chosen[96:, at]).astype(BF16)
     by_q = ToReaders(block, blocks, q_s, q_r)
     by_q.start()
     by_z.relay(4)
@@ -677,8 +689,11 @@
     by_q.arrive()
     qa[...] = blocks[...].reshape(qa.shape)
 
-    def attend(at):
-        block = kv_all[at]
+    def blocks_of(planes):
+        return jnp.concatenate([kv_all[at] for at in planes], axis=0)
+
+    def attend(*planes):
+        block = blocks_of(planes)
         keys = jnp.where(lanes_below(block.shape, HD), block, jnp.zeros_like(block))
         scores = contract(keys, qa[...], 1, 1)
         top = jnp.maximum(m[...], jnp.max(scores, axis=0, keepdims=True))
@@ -689,23 +704,22 @@
         o[...] = o[...] * old + contract(block, weights.astype(BF16), 0, 0)[HD:]
 
     def attend_from(low, high):
-        def one(i, carry):
-            d = low + i // 2
-            attend(lax.rem(z + nz + jnp.where(lax.rem(i, 2) == 0, d, -d), nz))
+        def one(d, carry):
+            attend(lax.rem(z + d, nz), lax.rem(z + nz - d, nz))
             return carry
 
-        lax.fori_loop(0, 2 * (high - low + 1), one, 0)
+        lax.fori_loop(low, high + 1, one, 0)
 
     attend(z)
+    by_z.relay(6)
     by_z.arrive(1)
-    attend_from(1, 2)
-    by_z.relay(6)
     by_z.arrive(3)
+    attend_from(1, 4)
     by_z.arrive(5)
-    attend_from(3, 6)
+    attend_from(5, 6)
     by_z.arrive(7)
+    by_z.arrive(8)
     attend_from(7, 7)
-    by_z.arrive(8)
     attend(lax.rem(z + nz // 2, nz))
     upright = jnp.transpose(qa[...].astype(F32))
     delta = jnp.sum(upright[HD:] * o[...], axis=0, keepdims=True)
@@ -731,12 +745,11 @@
     dq[...] = jnp.zeros(dq.shape, F32)
 
     def plane_of(side, j):
-        offset = jnp.where(side == 0, j - nz // 2, nz // 2 - 1 - j)
+        offset = nz // 2 - 1 - j if side else j - nz // 2
         return lax.rem(z + nz + offset, nz)
 
-    def grads(side, j):
-        at = plane_of(side, j)
-        block = kv_all[at]
+    def grads(*terms):
+        block = blocks_of([plane_of(side, j) for side, j in terms])
         low = lanes_below(block.shape, HD)
         none = jnp.zeros_like(block)
         scores = contract(jnp.where(low, block, none), qa[...], 1, 1)
@@ -746,15 +759,16 @@
         for_v = contract(probs.astype(BF16), qa[...], 1, 0)
         for_k = contract(d_scores, qa[...], 1, 0)
         dq[...] += contract(block, d_scores, 0, 0)[:HD]
-        mine[side, j] = jnp.where(lanes_below(for_k.shape, HD), for_k, for_v)
+        both = jnp.where(low, for_k, for_v)
+        for i, (side, j) in enumerate(terms):
+            mine[side, j] = both[256 * i : 256 * i + 256]
 
     def both_grads(low, high):
-        def one(i, carry):
-            side = lax.rem(i, 2)
-            grads(side, low + i // 2 - side)
+        def one(j, carry):
+            grads((0, j), (1, j - 1))
             return carry
 
-        lax.fori_loop(0, 2 * (high - low + 1), one, 0)
+        lax.fori_loop(low, high + 1, one, 0)
 
     main = StrideSum(nz, lambda side, j, at: mine[side, j, at], ring_out, ring_in, g_s, g_r, PIECES)
 
@@ -768,10 +782,14 @@
         ring.step(0, j)
         ring.step(1, j - 1)
 
-    grads(jnp.int32(0), jnp.int32(0))
+    grads((0, 0))
     main.step(0, 0)
     both_grads(1, 1)
     two(main, 1)
+    both_grads(2, 2)
+    two(main, 2)
+    both_grads(3, 3)
+    two(main, 3)
     by_o.arrive()
     attended = jnp.sum(outs[...].astype(F32), axis=0).astype(BF16)
     for a in range(2):
@@ -781,26 +799,22 @@
             o_part[a, i] = product[:, 128 * i : 128 * i + 128]
     swap = Exchange(("c",), o_part, swapped, sw_s, sw_r, lambda at, i: i)
     swap.start()
-    both_grads(2, 3)
-    two(main, 3)
-    two(main, 2)
+    both_grads(4, 5)
     swap.arrive()
     weight.step(0, 0)
-    for j in range(1, nz // 2, 2):
-        two(weight, j)
-    both_grads(4, 5)
+    two(weight, 1)
+    two(main, 4)
     two(main, 5)
-    two(main, 4)
     both_grads(6, 7)
-    two(main, 7)
-    two(weight, 2)
-    grads(jnp.int32(1), jnp.int32(7))
+    grads((1, nz // 2 - 1))
     upright = jnp.concatenate([dq[...], jnp.zeros_like(dq[...])], axis=0) * HD**-0.5
     dq_block[...] = jnp.transpose(upright).astype(BF16).reshape(4, 192, 128)
     by_dq = ToOwners(dq_block, dqs, dq_s, dq_r)
     by_dq.start()
+    two(weight, 2)
+    two(weight, 3)
     two(main, 6)
-    two(weight, 4)
+    two(main, 7)
     by_dq.arrive()
     query_grad = jnp.sum(dqs[...].astype(F32), axis=0).astype(BF16)
     d_target = jnp.zeros((128, 2048), F32)
@@ -810,12 +824,15 @@
     d_parts[...] = d_target.astype(BF16).reshape(16, 8, 2048)
     by_t = Exchange(("x", "y"), d_parts, t_in, t_s, t_r, lambda at, i: i)
     by_t.start()
+    two(weight, 4)
+    two(weight, 5)
     piece = 256 // PIECES
     for p in range(PIECES):
         kv_grad[pl.ds(p * piece, piece)] = main.total(p).astype(BF16)
     by_kv = Exchange(("c",), kv_grad, grads2, kv_s, kv_r)
     by_kv.start()
     two(weight, 6)
+    two(weight, 7)
     by_kv.arrive()
     g0, g1 = grads2[0].astype(F32), grads2[1].astype(F32)
     k2 = jnp.where(wide_low, g0, swap_halves(g1)).astype(BF16)
@@ -829,8 +846,7 @@
     back = FarGather(nz, mine_sum, all_sums, back_s, back_r)
     back.start()
     by_t.arrive()
-    upstream = jnp.sum(t_in[...].astype(F32), axis=0)[:6]
-    t_out[...] = cot[...].astype(F32) + norm_back(target_rows[...], t_gain[...], upstream)
+    t_out[...] = jnp.sum(t_in[...].astype(F32), axis=0)
     back.relay()
     by_s.arrive()
     got = []
@@ -842,12 +858,9 @@
     for j in range(8):
         chip = (2 * j % 4) * 4 + j // 2
         a, b = (g[:, 128 * j : 128 * j + 128] for g in got)
-        upstream_s[:, 128 * chip : 128 * chip + 128] = jnp.where(low, a, swap_halves(b))
-        upstream_s[:, 128 * chip + 512 : 128 * chip + 640] = jnp.where(low, swap_halves(a), b)
-    s_out[...] = norm_back(source_rows[...], s_gain[...], upstream_s[...])
+        s_out[:, 128 * chip : 128 * chip + 128] = jnp.where(low, a, swap_halves(b))
+        s_out[:, 128 * chip + 512 : 128 * chip + 640] = jnp.where(low, swap_halves(a), b)
     back.arrive()
-    for i in range(nz):
-        w_out[:, 128 * i : 128 * i + 128] = all_sums[i].astype(F32)
     for by in (by_rows, by_wy, by_wx, by_ya, by_xb, by_xa, by_yb, by_pair, by_part, by_q, by_z, by_stats):
         by.drain()
     for by in (by_o, by_dq, swap, back, by_kv, by_s, by_t, main, weight):
@@ -868,12 +881,14 @@
         functools.partial(kernel, nz),
         out_shape=(
             jax.ShapeDtypeStruct((32, 2048), F32),
-            jax.ShapeDtypeStruct((6, 2048), F32),
-            jax.ShapeDtypeStruct((64, 2048), F32),
+            jax.ShapeDtypeStruct((8, 2048), F32),
+            jax.ShapeDtypeStruct((nz, HD, 128), BF16),
         ),
-        in_specs=[VMEM] * len(args),
+        in_specs=[pl.BlockSpec(memory_space=pl.ANY)] * len(args),
         out_specs=(VMEM,) * 3,
         scratch_shapes=[
+            bf16(6, 2048), bf16(32, 2048), f32(1, 2048), f32(1, 2048), bf16(64, 512), bf16(64, 512),
+            bf16(6, 2048), bf16(192, 256), bf16(96, 128), dma(len(args)),
             bf16(128, 2048), bf16(nz, 256, 128), f32(8, t), bf16(4, 192, 128), bf16(t, 128),
             bf16(4, 4, 16, 2048), bf16(2, 128, 2048), bf16(4, 4, 2, 64, 128),
             bf16(2, 32, 1024), bf16(4, 2, 32, 1024), f32(2, 256, 128), f32(2, 256, 128),
@@ -881,8 +896,7 @@
             f32(HD, t), f32(2, half, 256, 128), bf16(2, half, 256, 128), bf16(2, half, 256, 128),
             bf16(2, half, HD, 128), bf16(2, half, HD, 128),
             bf16(4, 192, 128), bf16(4, 192, 128), bf16(4, 192, 128),
-            bf16(2, nz, HD, 128), bf16(2, nz, HD, 128), bf16(HD, 128), bf16(nz, HD, 128),
-            f32(32, 2048), bf16(256, 128), bf16(2, 256, 128), bf16(8, 32, 1024), bf16(16, 8, 2048),
+            bf16(2, nz, HD, 128), bf16(2, nz, HD, 128), bf16(HD, 128), bf16(256, 128), bf16(2, 256, 128), bf16(8, 32, 1024), bf16(16, 8, 2048),
             bf16(8, 32, 1024), bf16(16, 8, 2048),
             sems(5, 2), sems(5, 2), dma(1), dma(1), dma(1), sems(3, 4),
             dma(1), sems(3, 2), dma(1), sems(3, 2), dma(1), sems(3, 4), dma(1), sems(3, 4), dma(1), dma(1),
@@ -895,6 +909,28 @@
     )(*args)
 
 
+def finish_kernel(
+    d_source, d_target, sums, target_rows, source_rows, t_gain, s_gain, cot, t_out, s_out, w_out
+):
+    t_out[...] = cot[...].astype(F32) + norm_back(target_rows[...], t_gain[...], d_target[:6])
+    s_out[...] = norm_back(source_rows[...], s_gain[...], d_source[...])
+    for i in range(sums.shape[0]):
+        w_out[:, 128 * i : 128 * i + 128] = sums[i].astype(F32)
+
+
+def finish(*args):
+    return pl.pallas_call(
+        finish_kernel,
+        out_shape=(
+            jax.ShapeDtypeStruct((6, 2048), F32),
+            jax.ShapeDtypeStruct((32, 2048), F32),
+            jax.ShapeDtypeStruct((64, 2048), F32),
+        ),
+        in_specs=[VMEM] * len(args),
+        out_specs=(VMEM,) * 3,
+    )(*args)
+
+
 def picks():
     r = np.arange(96)
     at = 16 * (r // 6) + r % 6
@@ -904,9 +940,11 @@
 
 
 def body(nz, target_rows, source_rows, t_gain, s_gain, wq, wk, wv, wo, cot):
-    args = (target_rows, source_rows, t_gain[None], s_gain[None], wq, wk, wv, wo, cot, *picks())
-    source_grad, target_grad, o_grad = whole(args, nz)
-    return target_grad, source_grad, o_grad
+    gains = (t_gain[None], s_gain[None])
+    d_source, d_target, sums = whole(
+        (target_rows, source_rows, *gains, wq.T, wk, wv, wo, cot, *picks()), nz
+    )
+    return finish(d_source, d_target, sums, target_rows, source_rows, *gains, cot)
 
 
 def solution(mesh):

time: 110 us -> 99 us (0.900)
  the two profiles are of different devices: /device:TPU:8 before, /device:TPU:1 now
where the time goes in v5:
time: 99 us; the launch traced here: 97.3 us
  Pallas kernels  96.7 us (98%)
    pallas_call x1, Pallas kernels, whole(): pl.pallas_call(functools.partial(kernel, nz), out_shape=(jax.ShapeDtypeSt...  94.5 us
    pallas_call x1, Pallas kernels, finish(): pl.pallas_call(finish_kernel, out_shape=(jax.ShapeDtypeStruct((6, 2048),...  2.22 us

profile of v5, /device:TPU:1, one launch (start us, length us, event | category | flops | bytes accessed | tf_op | source)
XLA Modules:
  0.0 97.3 jit_solution(749646504599416992)
XLA Ops:
  0.6 94.5 %shard_map.130 = (f32[32,2048]{1,0:T(8,128)}, f32[8,2048]{1,0:T(8,128)}, bf16[16,64,128]{2,1,0:T(8,128)(2,1)}) custom-call(bf16[6,2048]{1,0:T(8,128)(2,1)} %target_rows.1, bf16[32,2048]{1,0:T(8,128)(2,1)} %source_rows.1, f32[1,2048]{1,0:T(1,128)} %bitcast.4, f32[1,2048]{1,0:T(1,128)} %bitcast.6, bf16[64,2048]{1,0:T(8,128)(2,1)} %bitcast.3, ...), custom_call_target="tpu_custom_call" | custom-call | tf_op jit(solution)/shard_map/pallas_call | solution.py:880
  95.1 2.2 %shard_map.131 = (f32[6,2048]{1,0:T(8,128)}, f32[32,2048]{1,0:T(8,128)}, f32[64,2048]{1,0:T(8,128)}) custom-call(f32[32,2048]{1,0:T(8,128)} %get-tuple-element.6.d_source, f32[8,2048]{1,0:T(8,128)} %get-tuple-element.7.d_target, bf16[16,64,128]{2,1,0:T(8,128)(2,1)} %get-tuple-element.8.sums, bf16[6,2048]{1,0:T(8,128)(2,1)} %target_rows.1, ...), custom_call_target="tpu_custom_call" | custom-call | tf_op jit(solution)/shard_map/pallas_call | solution.py:922

commit v6 on v5

--- a/solution.py
+++ b/solution.py
@@ -349,7 +349,7 @@
         to = lax.rem(self.y + k, 4)
         return pltpu.make_async_remote_copy(
             src_ref=self.parts[i].at[:, self.lanes(to)],
-            dst_ref=self.out.at[self.x, slot_y, i],
+            dst_ref=self.out.at[to, self.x, slot_y, :, pl.ds(128 * i, 128)],
             send_sem=self.send.at[0],
             recv_sem=self.recv.at[0],
             device_id={"y": to},
@@ -361,10 +361,11 @@
             for i in range(2):
                 self.copy(k, i, self.y).start()
         for i in range(2):
-            self.out[self.x, self.y, i] = self.parts[i][:, self.lanes(self.y)]
+            block = self.parts[i][:, self.lanes(self.y)]
+            self.out[self.y, self.x, self.y, :, 128 * i : 128 * i + 128] = block
 
     def others(self):
-        return bulk(self.out.at[self.x, pl.ds(0, 3)], self.send, self.recv)
+        return bulk(self.out.at[0, 0, pl.ds(0, 3)], self.send, self.recv)
 
     def arrive(self):
         self.others().wait_recv()
@@ -571,8 +572,8 @@
     pair, kv_all, stats, out, qa, t_all, pair_all, w_all,
     halves, rows_all, part, part_all, block, blocks, m, l, o, said, heard,
     dq, mine, ring_out, ring_in, w_ring_out, w_ring_in, outs, dq_block, dqs, o_part, swapped,
-    mine_sum, kv_grad, grads2, parts, d_parts, s_in, t_in,
-    row_s, row_r, wy_s, wy_r, wx_s, wx_r, ya_s, ya_r, xb_s, xb_r, xa_s, xa_r, yb_s, yb_r, pair_s, pair_r,
+    mine_sum, kv_grad, grads8, parts, d_parts, s_in, t_in,
+    row_s, row_r, wy_s, wy_r, wx_s, wx_r, wf_s, wf_r, ya_s, ya_r, xb_s, xb_r, xa_s, xa_r, yb_s, yb_r, pair_s, pair_r,
     part_s, part_r, q_s, q_r, z_s, z_r, ss, sr,
     o_s, o_r, dq_s, dq_r, sw_s, sw_r, g_s, g_r, h_s, h_r, back_s, back_r,
     kv_s, kv_r, s_s, s_r, t_s, t_r,
@@ -603,7 +604,10 @@
 
     by_rows = RowGather(halves, rows_all, row_s, row_r)
     by_wy = WeightColumn(wk, wv, w_all, wy_s, wy_r)
-    by_wx = RingGather("x", lambda slot, p: w_all.at[slot, p], 4, w_all.at[pl.ds(0, 3)], wx_s, wx_r)
+    by_wx = RingGather(
+        "x", lambda slot, p: w_all.at[y, slot, p], 4, w_all.at[y, pl.ds(0, 3)], wx_s, wx_r
+    )
+    by_wf = RingGather("y", lambda slot, p: w_all.at[slot, p], 4, w_all.at[pl.ds(0, 3)], wf_s, wf_r)
     three, first, second = pl.ds(0, 3), pl.ds(0, 1024), pl.ds(1024, 1024)
     by_ya = RingGather(
         "y", lambda slot, p: t_all.at[x, slot, :, pl.ds(512 * p, 512)], 2,
@@ -651,8 +655,8 @@
         by_wx.arrive(p)
 
     rows = rows_all[...].reshape(256, 1024)
-    k2 = jnp.dot(rows, w_all[:, :, 0].reshape(1024, 128), preferred_element_type=F32)
-    v2 = jnp.dot(rows, w_all[:, :, 1].reshape(1024, 128), preferred_element_type=F32)
+    kv2 = jnp.dot(rows, w_all[y].reshape(1024, 256), preferred_element_type=F32)
+    k2, v2 = kv2[:, :128], kv2[:, 128:]
     wide_low = lanes_below((256, 128), HD)
     part[0] = jnp.where(wide_low, k2, swap_halves(v2))
     part[1] = jnp.where(wide_low, swap_halves(k2), v2)
@@ -666,6 +670,8 @@
     for p in range(4):
         by_xa.relay(p)
         by_yb.relay(p)
+    for p in range(4):
+        by_wf.start(p)
     by_z.relay(2)
     by_pair.arrive()
     for p in range(4):
@@ -711,12 +717,12 @@
         lax.fori_loop(low, high + 1, one, 0)
 
     attend(z)
+    by_z.arrive(1)
+    attend_from(1, 2)
     by_z.relay(6)
-    by_z.arrive(1)
     by_z.arrive(3)
-    attend_from(1, 4)
     by_z.arrive(5)
-    attend_from(5, 6)
+    attend_from(3, 6)
     by_z.arrive(7)
     by_z.arrive(8)
     attend_from(7, 7)
@@ -727,6 +733,19 @@
     said[...] = jnp.where(row == 0, m[...], jnp.where(row == 1, l[...], delta))
     by_stats = Exchange(("x",), said, heard, ss, sr)
     by_stats.start()
+    log_sum = m[...] + jnp.log(l[...])
+    high = log_sum.astype(BF16)
+    rest = log_sum - high.astype(F32)
+    middle = rest.astype(BF16)
+    low_part = rest - middle.astype(F32)
+    line = lax.broadcasted_iota(jnp.int32, (HD, qa.shape[0]), 0)
+    parts3 = jnp.where(line == 0, high.astype(F32), jnp.where(line == 1, middle.astype(F32), low_part))
+    upright = jnp.concatenate([o[...] / l[...], jnp.where(line < 3, parts3, 0.0)], axis=0)
+    out[...] = jnp.transpose(upright).astype(BF16).reshape(out.shape)
+    by_o = ToOwners(out, outs, o_s, o_r)
+    by_o.start()
+    for p in range(4):
+        by_wf.relay(p)
     by_stats.arrive()
     top = jnp.max(heard[:, 0:1], axis=0)
     total = jnp.zeros_like(top)
@@ -736,12 +755,6 @@
         total = total + w * heard[j, 1:2]
         both = both + w * heard[j, 2:3]
     stats[...] = jnp.where(row == 0, top + jnp.log(total), both / total)
-    scaled = o[...] * (jnp.exp(m[...] - top) / total)
-    upright = jnp.concatenate([scaled, jnp.zeros_like(scaled)], axis=0)
-    out[...] = jnp.transpose(upright).astype(BF16).reshape(out.shape)
-
-    by_o = ToOwners(out, outs, o_s, o_r)
-    by_o.start()
     dq[...] = jnp.zeros(dq.shape, F32)
 
     def plane_of(side, j):
@@ -784,14 +797,17 @@
 
     grads((0, 0))
     main.step(0, 0)
-    both_grads(1, 1)
-    two(main, 1)
-    both_grads(2, 2)
-    two(main, 2)
-    both_grads(3, 3)
-    two(main, 3)
     by_o.arrive()
-    attended = jnp.sum(outs[...].astype(F32), axis=0).astype(BF16)
+    lanes = lax.broadcasted_iota(jnp.int32, (192, 128), 1)
+    given = [outs[i].astype(F32) for i in range(4)]
+    log_sums = [
+        jnp.sum(jnp.where(jnp.logical_and(lanes >= HD, lanes < HD + 3), g, 0.0), axis=1, keepdims=True)
+        for g in given
+    ]
+    largest = functools.reduce(jnp.maximum, log_sums)
+    shares = [jnp.exp(part_sum - largest) for part_sum in log_sums]
+    whole_sum = sum(g * w for g, w in zip(given, shares)) / sum(shares)
+    attended = jnp.where(lanes < HD, whole_sum, 0.0).astype(BF16)
     for a in range(2):
         spread = contract(pick[96:], attended[96 * a : 96 * a + 96], 0, 0).astype(BF16)
         product = contract(spread, t_all[...].reshape(256, 2048), 0, 0)[:HD].astype(BF16)
@@ -799,10 +815,17 @@
             o_part[a, i] = product[:, 128 * i : 128 * i + 128]
     swap = Exchange(("c",), o_part, swapped, sw_s, sw_r, lambda at, i: i)
     swap.start()
-    both_grads(4, 5)
+    both_grads(1, 1)
+    two(main, 1)
     swap.arrive()
     weight.step(0, 0)
     two(weight, 1)
+    both_grads(2, 3)
+    two(main, 2)
+    two(main, 3)
+    both_grads(4, 5)
+    two(weight, 2)
+    two(weight, 3)
     two(main, 4)
     two(main, 5)
     both_grads(6, 7)
@@ -811,8 +834,8 @@
     dq_block[...] = jnp.transpose(upright).astype(BF16).reshape(4, 192, 128)
     by_dq = ToOwners(dq_block, dqs, dq_s, dq_r)
     by_dq.start()
-    two(weight, 2)
-    two(weight, 3)
+    two(weight, 4)
+    two(weight, 5)
     two(main, 6)
     two(main, 7)
     by_dq.arrive()
@@ -824,44 +847,42 @@
     d_parts[...] = d_target.astype(BF16).reshape(16, 8, 2048)
     by_t = Exchange(("x", "y"), d_parts, t_in, t_s, t_r, lambda at, i: i)
     by_t.start()
-    two(weight, 4)
-    two(weight, 5)
-    piece = 256 // PIECES
-    for p in range(PIECES):
-        kv_grad[pl.ds(p * piece, piece)] = main.total(p).astype(BF16)
-    by_kv = Exchange(("c",), kv_grad, grads2, kv_s, kv_r)
-    by_kv.start()
     two(weight, 6)
     two(weight, 7)
-    by_kv.arrive()
-    g0, g1 = grads2[0].astype(F32), grads2[1].astype(F32)
-    k2 = jnp.where(wide_low, g0, swap_halves(g1)).astype(BF16)
-    v2 = jnp.where(wide_low, swap_halves(g0), g1).astype(BF16)
-    d_rows = contract(k2, w_all[:, :, 0].reshape(1024, 128), 1, 1)
-    d_rows = d_rows + contract(v2, w_all[:, :, 1].reshape(1024, 128), 1, 1)
-    parts[...] = d_rows.astype(BF16).reshape(8, 32, 1024)
-    by_s = Exchange(("y", "c"), parts, s_in, s_s, s_r, lambda at, i: i)
-    by_s.start()
+    for p in range(4):
+        by_wf.arrive(p)
     mine_sum[...] = weight.total(0).astype(BF16)
     back = FarGather(nz, mine_sum, all_sums, back_s, back_r)
     back.start()
+    piece = 256 // PIECES
+    for p in range(PIECES):
+        kv_grad[2 * p : 2 * p + 2] = main.total(p).astype(BF16).reshape(2, 64, 128)
+    by_kv = Exchange(("y", "c"), kv_grad, grads8, kv_s, kv_r, lambda at, i: at["y"])
+    by_kv.start()
     by_t.arrive()
     t_out[...] = jnp.sum(t_in[...].astype(F32), axis=0)
+    by_kv.arrive()
+    narrow = lanes_below((64, 128), HD)
+    d_rows = jnp.zeros((64, 1024), F32)
+    for i in range(4):
+        g0, g1 = grads8[2 * i].astype(F32), grads8[2 * i + 1].astype(F32)
+        k2 = jnp.where(narrow, g0, swap_halves(g1)).astype(BF16)
+        v2 = jnp.where(narrow, swap_halves(g0), g1).astype(BF16)
+        kv2 = jnp.concatenate([k2, v2], axis=1)
+        d_rows = d_rows + contract(kv2, w_all[i].reshape(1024, 256), 1, 1)
+    parts[...] = d_rows.astype(BF16).reshape(2, 32, 1024)
+    by_s = Exchange(("c",), parts, s_in, s_s, s_r, lambda at, i: i)
+    by_s.start()
     back.relay()
     by_s.arrive()
-    got = []
-    for core in range(2):
-        total = s_in[core].astype(F32)
-        for i in range(1, 4):
-            total = total + s_in[2 * i + core].astype(F32)
-        got.append(total)
+    got = [s_in[core].astype(F32) for core in range(2)]
     for j in range(8):
         chip = (2 * j % 4) * 4 + j // 2
         a, b = (g[:, 128 * j : 128 * j + 128] for g in got)
         s_out[:, 128 * chip : 128 * chip + 128] = jnp.where(low, a, swap_halves(b))
         s_out[:, 128 * chip + 512 : 128 * chip + 640] = jnp.where(low, swap_halves(a), b)
     back.arrive()
-    for by in (by_rows, by_wy, by_wx, by_ya, by_xb, by_xa, by_yb, by_pair, by_part, by_q, by_z, by_stats):
+    for by in (by_rows, by_wy, by_wx, by_wf, by_ya, by_xb, by_xa, by_yb, by_pair, by_part, by_q, by_z, by_stats):
         by.drain()
     for by in (by_o, by_dq, swap, back, by_kv, by_s, by_t, main, weight):
         by.drain()
@@ -890,15 +911,15 @@
             bf16(6, 2048), bf16(32, 2048), f32(1, 2048), f32(1, 2048), bf16(64, 512), bf16(64, 512),
             bf16(6, 2048), bf16(192, 256), bf16(96, 128), dma(len(args)),
             bf16(128, 2048), bf16(nz, 256, 128), f32(8, t), bf16(4, 192, 128), bf16(t, 128),
-            bf16(4, 4, 16, 2048), bf16(2, 128, 2048), bf16(4, 4, 2, 64, 128),
+            bf16(4, 4, 16, 2048), bf16(2, 128, 2048), bf16(4, 4, 4, 64, 256),
             bf16(2, 32, 1024), bf16(4, 2, 32, 1024), f32(2, 256, 128), f32(2, 256, 128),
             bf16(192, 128), bf16(4, 192, 128), f32(1, t), f32(1, t), f32(HD, t), f32(8, t), f32(4, 8, t),
             f32(HD, t), f32(2, half, 256, 128), bf16(2, half, 256, 128), bf16(2, half, 256, 128),
             bf16(2, half, HD, 128), bf16(2, half, HD, 128),
             bf16(4, 192, 128), bf16(4, 192, 128), bf16(4, 192, 128),
-            bf16(2, nz, HD, 128), bf16(2, nz, HD, 128), bf16(HD, 128), bf16(256, 128), bf16(2, 256, 128), bf16(8, 32, 1024), bf16(16, 8, 2048),
-            bf16(8, 32, 1024), bf16(16, 8, 2048),
-            sems(5, 2), sems(5, 2), dma(1), dma(1), dma(1), sems(3, 4),
+            bf16(2, nz, HD, 128), bf16(2, nz, HD, 128), bf16(HD, 128), bf16(4, 64, 128), bf16(8, 64, 128), bf16(2, 32, 1024), bf16(16, 8, 2048),
+            bf16(2, 32, 1024), bf16(16, 8, 2048),
+            sems(5, 2), sems(5, 2), dma(1), dma(1), dma(1), sems(3, 4), dma(1), sems(3, 4),
             dma(1), sems(3, 2), dma(1), sems(3, 2), dma(1), sems(3, 4), dma(1), sems(3, 4), dma(1), dma(1),
             dma(1), dma(1), dma(4), dma(4), dma(1), sems(2, half, PIECES), dma(1), dma(1),
             dma(4), dma(4), dma(4), dma(4), dma(1), dma(1),

time: 99 us -> 103 us (1.040)
  Pallas kernels: 96.7 us -> 102 us
    pallas_call x1, Pallas kernels: 94.5 us -> 99.5 us  [whole(): pl.pallas_call(functools.partial(kernel, nz), out_shape=(jax.ShapeDtypeSt...]
where the time goes in v6:
time: 103 us; the launch traced here: 102 us
  Pallas kernels  102 us (99%)
    pallas_call x1, Pallas kernels, whole(): pl.pallas_call(functools.partial(kernel, nz), out_shape=(jax.ShapeDtypeSt...  99.5 us
    pallas_call x1, Pallas kernels, finish(): pl.pallas_call(finish_kernel, out_shape=(jax.ShapeDtypeStruct((6, 2048),...  2.22 us

profile of v6, /device:TPU:1, one launch (start us, length us, event | category | flops | bytes accessed | tf_op | source)
XLA Modules:
  0.0 102.4 jit_solution(7392355779799398035)
XLA Ops:
  0.6 99.5 %shard_map.130 = (f32[32,2048]{1,0:T(8,128)}, f32[8,2048]{1,0:T(8,128)}, bf16[16,64,128]{2,1,0:T(8,128)(2,1)}) custom-call(bf16[6,2048]{1,0:T(8,128)(2,1)} %target_rows.1, bf16[32,2048]{1,0:T(8,128)(2,1)} %source_rows.1, f32[1,2048]{1,0:T(1,128)} %bitcast.4, f32[1,2048]{1,0:T(1,128)} %bitcast.6, bf16[64,2048]{1,0:T(8,128)(2,1)} %bitcast.3, ...), custom_call_target="tpu_custom_call" | custom-call | tf_op jit(solution)/shard_map/pallas_call | solution.py:901
  100.1 2.2 %shard_map.131 = (f32[6,2048]{1,0:T(8,128)}, f32[32,2048]{1,0:T(8,128)}, f32[64,2048]{1,0:T(8,128)}) custom-call(f32[32,2048]{1,0:T(8,128)} %get-tuple-element.6.d_source, f32[8,2048]{1,0:T(8,128)} %get-tuple-element.7.d_target, bf16[16,64,128]{2,1,0:T(8,128)(2,1)} %get-tuple-element.8.sums, bf16[6,2048]{1,0:T(8,128)(2,1)} %target_rows.1, ...), custom_call_target="tpu_custom_call" | custom-call | tf_op jit(solution)/shard_map/pallas_call | solution.py:943

commit v7 on v6

--- a/solution.py
+++ b/solution.py
@@ -389,10 +389,16 @@
         self.nz, self.blocks, self.send, self.recv = nz, blocks, send, recv
         self.z = lax.axis_index("z")
         self.rows = blocks.shape[1] // PIECES
-        self.far = {1: nz // 2, -1: nz - 1 - nz // 2}
+        self.far = nz // 2
 
     def at(self, offset):
         return lax.rem(self.z + offset + self.nz, self.nz)
+
+    def pieces(self, sign, distance):
+        if distance < self.far:
+            return range(PIECES)
+        half = PIECES // 2
+        return range(half) if sign > 0 else range(half, PIECES)
 
     def copy(self, sign, distance, d, p):
         ref = self.blocks.at[self.at(-sign * distance), pl.ds(p * self.rows, self.rows)]
@@ -425,42 +431,40 @@
     def relay(self, distance):
         for p in range(PIECES):
             for sign in (1, -1):
-                if distance <= self.far[sign]:
-                    self.arrived(sign, distance, p).wait_recv()
-                if distance + 2 <= self.far[sign]:
+                self.arrived(sign, distance, p).wait_recv()
+                if p in self.pieces(sign, distance + 2):
                     self.copy(sign, distance, 2, p).start()
         for p in range(PIECES):
             for sign in (1, -1):
-                if distance + 1 <= self.far[sign]:
-                    self.copy(sign, distance, 1, p).start()
+                self.copy(sign, distance, 1, p).start()
 
     def arrive(self, distance):
         for sign in (1, -1):
-            if distance <= self.far[sign]:
-                for p in range(PIECES):
-                    self.arrived(sign, distance, p).wait_recv()
+            for p in self.pieces(sign, distance):
+                self.arrived(sign, distance, p).wait_recv()
 
     def drain(self):
         bulk(self.blocks.at[pl.ds(0, self.nz - 1)], self.send, self.send).wait_send()
 
 
 class StrideSum:
-    def __init__(self, nz, term, out, arrived, send, recv, pieces):
+    def __init__(self, nz, term, out, arrived, send, recv):
         self.nz, self.term, self.out, self.arrived = nz, term, out, arrived
-        self.send, self.recv, self.pieces = send, recv, pieces
-        self.rows = out.shape[2] // pieces
+        self.send, self.recv = send, recv
+        self.rows = out.shape[2] // PIECES
         self.z = lax.axis_index("z")
 
-    def chained(self, side, j):
-        return (j + side) % 2 == 0
+    def pieces(self, side, j):
+        half = PIECES // 2
+        return range(PIECES) if j else range(side * half, side * half + half)
 
     def hop(self, side, j, p):
         at = pl.ds(p * self.rows, self.rows)
-        d = (2 if self.chained(side, j) else 1) * (1 if side else -1)
+        d = (1 if j % 2 else 2) * (1 if side else -1)
         return pltpu.make_async_remote_copy(
             src_ref=self.out.at[side, j, at],
             dst_ref=self.arrived.at[side, j, at],
-            send_sem=self.send.at[side],
+            send_sem=self.send.at[side if j else 2 + side],
             recv_sem=self.recv.at[side, j, p],
             device_id={"z": lax.rem(self.z + d + self.nz, self.nz)},
             device_id_type=MESH,
@@ -469,31 +473,34 @@
     def joined(self, side, j, p, value):
         at = pl.ds(p * self.rows, self.rows)
         for i in (j - 1, j - 2):
-            if i >= 0:
+            if i >= 0 and p in self.pieces(side, i):
                 self.hop(side, i, p).wait_recv()
                 value = value + self.arrived[side, i, at].astype(F32)
         return value
 
-    def step(self, side, j):
-        for p in range(self.pieces):
-            at = pl.ds(p * self.rows, self.rows)
-            value = self.term(side, j, at)
-            if self.chained(side, j):
-                value = self.joined(side, j, p, value)
-            self.out[side, j, at] = value.astype(BF16)
-            self.hop(side, j, p).start()
+    def step(self, j):
+        for p in range(PIECES):
+            for side in range(2):
+                if p in self.pieces(side, j):
+                    at = pl.ds(p * self.rows, self.rows)
+                    value = self.term(side, j, at)
+                    if j % 2 == 0:
+                        value = self.joined(side, j, p, value)
+                    self.out[side, j, at] = value.astype(BF16)
+                    self.hop(side, j, p).start()
 
     def total(self, p):
         half = self.nz // 2
-        at = pl.ds(p * self.rows, self.rows)
-        value = self.joined(1, half - 1, p, self.term(1, half - 1, at))
-        return self.joined(0, half, p, value)
+        value = self.term(0, half, pl.ds(p * self.rows, self.rows))
+        return self.joined(1, half, p, self.joined(0, half, p, value))
 
     def drain(self):
         half = self.nz // 2
         for side in range(2):
             sem = self.send.at[pl.ds(side, 1)]
-            bulk(self.out.at[side, pl.ds(0, half - side)], sem, sem).wait_send()
+            bulk(self.out.at[side, pl.ds(0, half - 1)], sem, sem).wait_send()
+            sem = self.send.at[pl.ds(2 + side, 1)]
+            bulk(self.out.at[side, 0, pl.ds(0, self.rows * (PIECES // 2))], sem, sem).wait_send()
 
 
 class FarGather:
@@ -758,7 +765,7 @@
     dq[...] = jnp.zeros(dq.shape, F32)
 
     def plane_of(side, j):
-        offset = nz // 2 - 1 - j if side else j - nz // 2
+        offset = nz // 2 - j if side else j - nz // 2
         return lax.rem(z + nz + offset, nz)
 
     def grads(*terms):
@@ -774,29 +781,27 @@
         dq[...] += contract(block, d_scores, 0, 0)[:HD]
         both = jnp.where(low, for_k, for_v)
         for i, (side, j) in enumerate(terms):
-            mine[side, j] = both[256 * i : 256 * i + 256]
+            mine[j, side] = both[256 * i : 256 * i + 256]
 
     def both_grads(low, high):
         def one(j, carry):
-            grads((0, j), (1, j - 1))
+            grads((0, j), (1, j))
             return carry
 
         lax.fori_loop(low, high + 1, one, 0)
 
-    main = StrideSum(nz, lambda side, j, at: mine[side, j, at], ring_out, ring_in, g_s, g_r, PIECES)
+    main = StrideSum(
+        nz, lambda side, j, at: mine[j, side if j else 0, at], ring_out, ring_in, g_s, g_r
+    )
 
     def own_weight(side, j, at):
         to = plane_of(side, j)
         return swapped[0, to, at].astype(F32) + swapped[1, to, at].astype(F32)
 
-    weight = StrideSum(nz, own_weight, w_ring_out, w_ring_in, h_s, h_r, 1)
-
-    def two(ring, j):
-        ring.step(0, j)
-        ring.step(1, j - 1)
+    weight = StrideSum(nz, own_weight, w_ring_out, w_ring_in, h_s, h_r)
 
     grads((0, 0))
-    main.step(0, 0)
+    main.step(0)
     by_o.arrive()
     lanes = lax.broadcasted_iota(jnp.int32, (192, 128), 1)
     given = [outs[i].astype(F32) for i in range(4)]
@@ -816,51 +821,51 @@
     swap = Exchange(("c",), o_part, swapped, sw_s, sw_r, lambda at, i: i)
     swap.start()
     both_grads(1, 1)
-    two(main, 1)
+    main.step(1)
     swap.arrive()
-    weight.step(0, 0)
-    two(weight, 1)
+    weight.step(0)
+    weight.step(1)
     both_grads(2, 3)
-    two(main, 2)
-    two(main, 3)
-    both_grads(4, 5)
-    two(weight, 2)
-    two(weight, 3)
-    two(main, 4)
-    two(main, 5)
-    both_grads(6, 7)
-    grads((1, nz // 2 - 1))
+    weight.step(2)
+    main.step(2)
+    weight.step(3)
+    main.step(3)
+    both_grads(4, 7)
+    grads((0, nz // 2))
     upright = jnp.concatenate([dq[...], jnp.zeros_like(dq[...])], axis=0) * HD**-0.5
-    dq_block[...] = jnp.transpose(upright).astype(BF16).reshape(4, 192, 128)
+    straight = jnp.transpose(upright)
+    for i in range(4):
+        first_head, second_head = (straight[192 * i + 96 * a : 192 * i + 96 * a + 96] for a in range(2))
+        dq_block[i] = (first_head + swap_halves(second_head)).astype(BF16)
     by_dq = ToOwners(dq_block, dqs, dq_s, dq_r)
     by_dq.start()
-    two(weight, 4)
-    two(weight, 5)
-    two(main, 6)
-    two(main, 7)
+    weight.step(4)
+    main.step(4)
+    weight.step(5)
+    main.step(5)
     by_dq.arrive()
     query_grad = jnp.sum(dqs[...].astype(F32), axis=0).astype(BF16)
-    d_target = jnp.zeros((128, 2048), F32)
-    for a in range(2):
-        spread = contract(pick8[...], query_grad[96 * a : 96 * a + 96], 0, 0).astype(BF16)
-        d_target = d_target + jnp.dot(spread, pair_all[a], preferred_element_type=F32)
+    spread = contract(pick8[...], query_grad, 0, 0).astype(BF16)
+    heads = jnp.concatenate([pair_all[a, :HD] for a in range(2)], axis=0)
+    d_target = jnp.dot(spread, heads, preferred_element_type=F32)
     d_parts[...] = d_target.astype(BF16).reshape(16, 8, 2048)
     by_t = Exchange(("x", "y"), d_parts, t_in, t_s, t_r, lambda at, i: i)
     by_t.start()
-    two(weight, 6)
-    two(weight, 7)
+    weight.step(6)
+    weight.step(7)
+    main.step(6)
+    main.step(7)
+    for p in range(PIECES):
+        mine_sum[pl.ds(32 * p, 32)] = weight.total(p).astype(BF16)
+    back = FarGather(nz, mine_sum, all_sums, back_s, back_r)
+    back.start()
     for p in range(4):
         by_wf.arrive(p)
-    mine_sum[...] = weight.total(0).astype(BF16)
-    back = FarGather(nz, mine_sum, all_sums, back_s, back_r)
-    back.start()
-    piece = 256 // PIECES
     for p in range(PIECES):
         kv_grad[2 * p : 2 * p + 2] = main.total(p).astype(BF16).reshape(2, 64, 128)
     by_kv = Exchange(("y", "c"), kv_grad, grads8, kv_s, kv_r, lambda at, i: at["y"])
     by_kv.start()
-    by_t.arrive()
-    t_out[...] = jnp.sum(t_in[...].astype(F32), axis=0)
+    back.relay()
     by_kv.arrive()
     narrow = lanes_below((64, 128), HD)
     d_rows = jnp.zeros((64, 1024), F32)
@@ -873,7 +878,8 @@
     parts[...] = d_rows.astype(BF16).reshape(2, 32, 1024)
     by_s = Exchange(("c",), parts, s_in, s_s, s_r, lambda at, i: i)
     by_s.start()
-    back.relay()
+    by_t.arrive()
+    t_out[...] = jnp.sum(t_in[...].astype(F32), axis=0)
     by_s.arrive()
     got = [s_in[core].astype(F32) for core in range(2)]
     for j in range(8):
@@ -914,16 +920,16 @@
             bf16(4, 4, 16, 2048), bf16(2, 128, 2048), bf16(4, 4, 4, 64, 256),
             bf16(2, 32, 1024), bf16(4, 2, 32, 1024), f32(2, 256, 128), f32(2, 256, 128),
             bf16(192, 128), bf16(4, 192, 128), f32(1, t), f32(1, t), f32(HD, t), f32(8, t), f32(4, 8, t),
-            f32(HD, t), f32(2, half, 256, 128), bf16(2, half, 256, 128), bf16(2, half, 256, 128),
+            f32(HD, t), f32(half + 1, 2, 256, 128), bf16(2, half, 256, 128), bf16(2, half, 256, 128),
             bf16(2, half, HD, 128), bf16(2, half, HD, 128),
-            bf16(4, 192, 128), bf16(4, 192, 128), bf16(4, 192, 128),
+            bf16(4, 192, 128), bf16(4, 96, 128), bf16(4, 96, 128),
             bf16(2, nz, HD, 128), bf16(2, nz, HD, 128), bf16(HD, 128), bf16(4, 64, 128), bf16(8, 64, 128), bf16(2, 32, 1024), bf16(16, 8, 2048),
             bf16(2, 32, 1024), bf16(16, 8, 2048),
             sems(5, 2), sems(5, 2), dma(1), dma(1), dma(1), sems(3, 4), dma(1), sems(3, 4),
             dma(1), sems(3, 2), dma(1), sems(3, 2), dma(1), sems(3, 4), dma(1), sems(3, 4), dma(1), dma(1),
             dma(1), dma(1), dma(4), dma(4), dma(1), sems(2, half, PIECES), dma(1), dma(1),
             dma(4), dma(4), dma(4), dma(4), dma(1), dma(1),
-            dma(2), sems(2, half, PIECES), dma(2), sems(2, half, 1),
+            dma(4), sems(2, half, PIECES), dma(4), sems(2, half, PIECES),
             dma(1), dma(4), dma(1), dma(1), dma(1), dma(1), dma(1), dma(1),
         ],
         compiler_params=params(0),

time: 103 us -> 97.7 us (0.949)
  Pallas kernels: 102 us -> 96.9 us
    pallas_call x1, Pallas kernels: 99.5 us -> 94.7 us  [whole(): pl.pallas_call(functools.partial(kernel, nz), out_shape=(jax.ShapeDtypeSt...]
where the time goes in v7:
time: 97.7 us; the launch traced here: 97.5 us
  Pallas kernels  96.9 us (99%)
    pallas_call x1, Pallas kernels, whole(): pl.pallas_call(functools.partial(kernel, nz), out_shape=(jax.ShapeDtypeSt...  94.7 us
    pallas_call x1, Pallas kernels, finish(): pl.pallas_call(finish_kernel, out_shape=(jax.ShapeDtypeStruct((6, 2048),...  2.22 us

profile of v7, /device:TPU:1, one launch (start us, length us, event | category | flops | bytes accessed | tf_op | source)
XLA Modules:
  0.0 97.5 jit_solution(5124409112559304937)
XLA Ops:
  0.6 94.7 %shard_map.130 = (f32[32,2048]{1,0:T(8,128)}, f32[8,2048]{1,0:T(8,128)}, bf16[16,64,128]{2,1,0:T(8,128)(2,1)}) custom-call(bf16[6,2048]{1,0:T(8,128)(2,1)} %target_rows.1, bf16[32,2048]{1,0:T(8,128)(2,1)} %source_rows.1, f32[1,2048]{1,0:T(1,128)} %bitcast.4, f32[1,2048]{1,0:T(1,128)} %bitcast.6, bf16[64,2048]{1,0:T(8,128)(2,1)} %bitcast.3, ...), custom_call_target="tpu_custom_call" | custom-call | tf_op jit(solution)/shard_map/pallas_call | solution.py:907
  95.3 2.2 %shard_map.131 = (f32[6,2048]{1,0:T(8,128)}, f32[32,2048]{1,0:T(8,128)}, f32[64,2048]{1,0:T(8,128)}) custom-call(f32[32,2048]{1,0:T(8,128)} %get-tuple-element.6.d_source, f32[8,2048]{1,0:T(8,128)} %get-tuple-element.7.d_target, bf16[16,64,128]{2,1,0:T(8,128)(2,1)} %get-tuple-element.8.sums, bf16[6,2048]{1,0:T(8,128)(2,1)} %target_rows.1, ...), custom_call_target="tpu_custom_call" | custom-call | tf_op jit(solution)/shard_map/pallas_call | solution.py:949

commit v8 on v7

--- a/solution.py
+++ b/solution.py
@@ -822,15 +822,20 @@
     swap.start()
     both_grads(1, 1)
     main.step(1)
+    both_grads(2, 2)
     swap.arrive()
-    weight.step(0)
-    weight.step(1)
-    both_grads(2, 3)
+    for j in (0, 1, 3, 5, 7):
+        weight.step(j)
+    both_grads(3, 3)
+    main.step(2)
+    main.step(3)
+    both_grads(5, 5)
+    main.step(5)
     weight.step(2)
-    main.step(2)
-    weight.step(3)
-    main.step(3)
-    both_grads(4, 7)
+    both_grads(7, 7)
+    main.step(7)
+    both_grads(4, 4)
+    both_grads(6, 6)
     grads((0, nz // 2))
     upright = jnp.concatenate([dq[...], jnp.zeros_like(dq[...])], axis=0) * HD**-0.5
     straight = jnp.transpose(upright)
@@ -839,10 +844,10 @@
         dq_block[i] = (first_head + swap_halves(second_head)).astype(BF16)
     by_dq = ToOwners(dq_block, dqs, dq_s, dq_r)
     by_dq.start()
+    main.step(4)
     weight.step(4)
-    main.step(4)
-    weight.step(5)
-    main.step(5)
+    main.step(6)
+    weight.step(6)
     by_dq.arrive()
     query_grad = jnp.sum(dqs[...].astype(F32), axis=0).astype(BF16)
     spread = contract(pick8[...], query_grad, 0, 0).astype(BF16)
@@ -851,10 +856,6 @@
     d_parts[...] = d_target.astype(BF16).reshape(16, 8, 2048)
     by_t = Exchange(("x", "y"), d_parts, t_in, t_s, t_r, lambda at, i: i)
     by_t.start()
-    weight.step(6)
-    weight.step(7)
-    main.step(6)
-    main.step(7)
     for p in range(PIECES):
         mine_sum[pl.ds(32 * p, 32)] = weight.total(p).astype(BF16)
     back = FarGather(nz, mine_sum, all_sums, back_s, back_r)

time: 97.7 us -> 96.1 us (0.984)
  Pallas kernels: 96.9 us -> 94.4 us
    pallas_call x1, Pallas kernels: 94.7 us -> 92.2 us  [whole(): pl.pallas_call(functools.partial(kernel, nz), out_shape=(jax.ShapeDtypeSt...]
where the time goes in v8:
time: 96.1 us; the launch traced here: 95.1 us
  Pallas kernels  94.4 us (98%)
    pallas_call x1, Pallas kernels, whole(): pl.pallas_call(functools.partial(kernel, nz), out_shape=(jax.ShapeDtypeSt...  92.2 us
    pallas_call x1, Pallas kernels, finish(): pl.pallas_call(finish_kernel, out_shape=(jax.ShapeDtypeStruct((6, 2048),...  2.22 us

profile of v8, /device:TPU:1, one launch (start us, length us, event | category | flops | bytes accessed | tf_op | source)
XLA Modules:
  0.0 95.1 jit_solution(9226079299336376097)
XLA Ops:
  0.6 92.2 %shard_map.130 = (f32[32,2048]{1,0:T(8,128)}, f32[8,2048]{1,0:T(8,128)}, bf16[16,64,128]{2,1,0:T(8,128)(2,1)}) custom-call(bf16[6,2048]{1,0:T(8,128)(2,1)} %target_rows.1, bf16[32,2048]{1,0:T(8,128)(2,1)} %source_rows.1, f32[1,2048]{1,0:T(1,128)} %bitcast.4, f32[1,2048]{1,0:T(1,128)} %bitcast.6, bf16[64,2048]{1,0:T(8,128)(2,1)} %bitcast.3, ...), custom_call_target="tpu_custom_call" | custom-call | tf_op jit(solution)/shard_map/pallas_call | solution.py:908
  92.8 2.2 %shard_map.131 = (f32[6,2048]{1,0:T(8,128)}, f32[32,2048]{1,0:T(8,128)}, f32[64,2048]{1,0:T(8,128)}) custom-call(f32[32,2048]{1,0:T(8,128)} %get-tuple-element.6.d_source, f32[8,2048]{1,0:T(8,128)} %get-tuple-element.7.d_target, bf16[16,64,128]{2,1,0:T(8,128)(2,1)} %get-tuple-element.8.sums, bf16[6,2048]{1,0:T(8,128)(2,1)} %target_rows.1, ...), custom_call_target="tpu_custom_call" | custom-call | tf_op jit(solution)/shard_map/pallas_call | solution.py:950

commit v9 on v8

--- a/solution.py
+++ b/solution.py
@@ -732,8 +732,7 @@
     attend_from(3, 6)
     by_z.arrive(7)
     by_z.arrive(8)
-    attend_from(7, 7)
-    attend(lax.rem(z + nz // 2, nz))
+    attend(*(lax.rem(z + nz + d, nz) for d in (7, -7, nz // 2)))
     upright = jnp.transpose(qa[...].astype(F32))
     delta = jnp.sum(upright[HD:] * o[...], axis=0, keepdims=True)
     row = lax.broadcasted_iota(jnp.int32, (8, qa.shape[0]), 0)
@@ -866,6 +865,8 @@
         kv_grad[2 * p : 2 * p + 2] = main.total(p).astype(BF16).reshape(2, 64, 128)
     by_kv = Exchange(("y", "c"), kv_grad, grads8, kv_s, kv_r, lambda at, i: at["y"])
     by_kv.start()
+    for by in (by_rows, by_wy, by_wx, by_wf, by_ya, by_xb, by_xa, by_yb, by_pair, by_part, by_q, by_z, by_stats):
+        by.drain()
     back.relay()
     by_kv.arrive()
     narrow = lanes_below((64, 128), HD)
@@ -889,8 +890,6 @@
         s_out[:, 128 * chip : 128 * chip + 128] = jnp.where(low, a, swap_halves(b))
         s_out[:, 128 * chip + 512 : 128 * chip + 640] = jnp.where(low, swap_halves(a), b)
     back.arrive()
-    for by in (by_rows, by_wy, by_wx, by_wf, by_ya, by_xb, by_xa, by_yb, by_pair, by_part, by_q, by_z, by_stats):
-        by.drain()
     for by in (by_o, by_dq, swap, back, by_kv, by_s, by_t, main, weight):
         by.drain()
 

time: 96.1 us -> 95.9 us (level)
  no operation moved by 1% of the time
where the time goes in v9:
time: 95.9 us; the launch traced here: 94.6 us
  Pallas kernels  94 us (98%)
    pallas_call x1, Pallas kernels, whole(): pl.pallas_call(functools.partial(kernel, nz), out_shape=(jax.ShapeDtypeSt...  91.7 us
    pallas_call x1, Pallas kernels, finish(): pl.pallas_call(finish_kernel, out_shape=(jax.ShapeDtypeStruct((6, 2048),...  2.22 us

profile of v9, /device:TPU:1, one launch (start us, length us, event | category | flops | bytes accessed | tf_op | source)
XLA Modules:
  0.0 94.6 jit_solution(4916990851018601114)
XLA Ops:
  0.6 91.7 %shard_map.130 = (f32[32,2048]{1,0:T(8,128)}, f32[8,2048]{1,0:T(8,128)}, bf16[16,64,128]{2,1,0:T(8,128)(2,1)}) custom-call(bf16[6,2048]{1,0:T(8,128)(2,1)} %target_rows.1, bf16[32,2048]{1,0:T(8,128)(2,1)} %source_rows.1, f32[1,2048]{1,0:T(1,128)} %bitcast.4, f32[1,2048]{1,0:T(1,128)} %bitcast.6, bf16[64,2048]{1,0:T(8,128)(2,1)} %bitcast.3, ...), custom_call_target="tpu_custom_call" | custom-call | tf_op jit(solution)/shard_map/pallas_call | solution.py:907
  92.4 2.2 %shard_map.131 = (f32[6,2048]{1,0:T(8,128)}, f32[32,2048]{1,0:T(8,128)}, f32[64,2048]{1,0:T(8,128)}) custom-call(f32[32,2048]{1,0:T(8,128)} %get-tuple-element.6.d_source, f32[8,2048]{1,0:T(8,128)} %get-tuple-element.7.d_target, bf16[16,64,128]{2,1,0:T(8,128)(2,1)} %get-tuple-element.8.sums, bf16[6,2048]{1,0:T(8,128)(2,1)} %target_rows.1, ...), custom_call_target="tpu_custom_call" | custom-call | tf_op jit(solution)/shard_map/pallas_call | solution.py:949
